TPU v7x, 256 devices: a whole 4x4x8 slice. The times are simulated.
256 devices in a mesh: ep: 64 (over z, y, core), tp: 4 (over x).
Axes of the slice: x: 4, y: 4, z: 8, core: 2. Of those that a mesh axis runs over, the one named last changes fastest.
Arguments:
- queries: bfloat16 [16384, 1024], P('ep', 'tp'), may hold values from -200 to 200
- keys: bfloat16 [16384, 512], P('ep', 'tp'), may hold values from -5 to 5
- values: bfloat16 [16384, 512], P('ep', 'tp'), may hold values from -6 to 6
- log_gates: float32 [16384, 16], P('ep', 'tp'), may hold values from -16384 to 0, as said below
- out_weight: bfloat16 [1024, 2048], P('tp'), may hold values from -0.1875 to 0.1875
- moe_rows: bfloat16 [16384, 2048], P('ep'), may hold values from -6 to 6
- norm_gain: float32 [2048], replicated, may hold values from 0.1 to 1.9
- experts: int32 [16384, 2], P('ep'), may hold values from 0 to 63, all different within a row; in each aligned block of 256 rows (0 to 255, 256 to 511, ...) at most 16 rows name the same one
- expert_weights: float32 [16384, 2], P('ep'), may hold values from 0.2 to 1
- w_gate: bfloat16 [64, 2048, 1024], P('ep', None, 'tp'), may hold values from -0.125 to 0.125
- w_up: bfloat16 [64, 2048, 1024], P('ep', None, 'tp'), may hold values from -0.125 to 0.125
- w_down: bfloat16 [64, 1024, 2048], P('ep', 'tp'), may hold values from -0.1875 to 0.1875
Outputs:
- mixed: bfloat16 [16384, 2048], P(('ep', 'tp'))
- moe_out: bfloat16 [16384, 2048], P('ep', 'tp')
Inputs may be any that keep to these rules, and one draw needn't show every extreme that they name: Each token names 2 different experts; within the rows of one index of ep (aligned blocks of 256 rows) no expert is named more than 16 times, a bound that some block reaches. `log_gates`: Non-increasing along positions in every head.
All inputs are finite; a program needn't handle non-finite values.
Results may differ from a plain program's by a relative error of at most 0.01195.
Values may be sent and summed in bfloat16 or wider, within the bound.
No kernel may reach another device: no remote copies, remote signals or barrier semaphores. Data moves between devices by JAX's collectives and lax.ppermute only.
A program may use at most 128 MiB of HBM per device.

v0:
```python
import math

import jax
import jax.numpy as jnp
from jax import lax
from jax.sharding import PartitionSpec as P

D = 2048
HD = 64


EPSILON = 1e-06
MASKED = -1e30


def prepare_group(query_rows, gate_rows, positions, kv_here, group):
    rows = query_rows.shape[0]
    query_heads = query_rows.reshape(rows, kv_here, group, HD)
    query_gates = jnp.transpose(gate_rows.reshape(rows, kv_here, group), (1, 2, 0))
    return (query_heads, query_gates, positions)


def empty_state(rows, kv_here, group):
    return (
        jnp.full((kv_here, group, rows), MASKED, jnp.float32),
        jnp.zeros((kv_here, group, rows), jnp.float32),
        jnp.zeros((kv_here, group, rows, HD), jnp.float32),
    )


def attend_group(prepared, state, key_part, value_part, gate_part, offset, kv_here, group):
    query_heads, query_gates, query_position = prepared
    length = key_part.shape[0]
    key_span = math.gcd(length, 512)

    def run_blocks(start_state):

        def one_block(turn_index, inner):
            running_max, running_sum, weighted = inner
            first = turn_index * key_span
            key_block = lax.dynamic_slice_in_dim(key_part, first, key_span, 0).reshape(
                key_span, kv_here, HD
            )
            value_block = lax.dynamic_slice_in_dim(value_part, first, key_span, 0).reshape(
                key_span, kv_here, HD
            )
            gate_block = lax.dynamic_slice_in_dim(gate_part, first, key_span, 0).reshape(
                key_span, kv_here, group
            )
            scores = jnp.einsum(
                "qgrd,kgd->grqk", query_heads, key_block, preferred_element_type=jnp.float32
            ) * HD ** (-0.5)
            scores = (
                scores
                + query_gates[..., None]
                - jnp.transpose(gate_block, (1, 2, 0))[:, :, None, :]
            )
            key_position = first + jnp.arange(key_span, dtype=jnp.int32)
            scores = jnp.where(key_position[None, :] <= query_position[:, None], scores, MASKED)
            new_max = jnp.maximum(running_max, jnp.max(scores, axis=-1))
            weights = jnp.exp(scores - new_max[..., None])
            rescale = jnp.exp(running_max - new_max)
            running_sum = running_sum * rescale + jnp.sum(weights, axis=-1)
            weighted = weighted * rescale[..., None] + jnp.einsum(
                "grqk,kgd->grqd",
                weights.astype(jnp.bfloat16),
                value_block,
                preferred_element_type=jnp.float32,
            )
            return (new_max, running_sum, weighted)

        return lax.fori_loop(0, length // key_span, one_block, start_state)

    def keep_state(start_state):
        return start_state

    return lax.cond(offset <= query_position[-1], run_blocks, keep_state, state)


def finish_group(state, heads_here):
    running_max, running_sum, weighted = state
    rows = weighted.shape[2]
    attended = weighted / running_sum[..., None]
    return jnp.transpose(attended, (2, 0, 1, 3)).reshape(rows, heads_here * HD).astype(jnp.bfloat16)


def mixer_half(queries, keys, values, log_gates, out_weight):
    tok_rows = queries.shape[0]
    heads_here = log_gates.shape[1]
    kv_here = keys.shape[1] // HD
    group = heads_here // kv_here
    own_index = lax.axis_index("ep")
    positions = own_index * tok_rows + jnp.arange(tok_rows, dtype=jnp.int32)
    groups = [prepare_group(queries, log_gates, positions, kv_here, group)]
    initial = tuple((empty_state(entry[0].shape[0], kv_here, group) for entry in groups))
    offset = jnp.int32(0)
    key_part = lax.all_gather(keys.astype(jnp.float32), "ep", axis=0, tiled=True).astype(
        jnp.bfloat16
    )
    value_part = lax.all_gather(values.astype(jnp.float32), "ep", axis=0, tiled=True).astype(
        jnp.bfloat16
    )
    gate_part = lax.all_gather(log_gates, "ep", axis=0, tiled=True)
    states = tuple(
        (
            attend_group(
                groups[number],
                initial[number],
                key_part,
                value_part,
                gate_part,
                offset,
                kv_here,
                group,
            )
            for number in range(len(groups))
        )
    )
    finished = [finish_group(state, heads_here) for state in states]
    attended = finished[0]
    return lax.psum_scatter(
        jnp.dot(attended, out_weight, preferred_element_type=jnp.float32).astype(jnp.bfloat16),
        "tp",
        scatter_dimension=0,
        tiled=True,
    )


def experts_half(moe_rows, norm_gain, experts, expert_weights, w_gate, w_up, w_down):
    rows_here = moe_rows.shape[0]
    topk = experts.shape[1]
    experts_all = lax.axis_size("ep")
    capacity = 4 * rows_here // experts_all
    rows_float = moe_rows.astype(jnp.float32)
    normed = (
        rows_float
        * lax.rsqrt(jnp.mean(rows_float * rows_float, axis=-1, keepdims=True) + EPSILON)
        * norm_gain
    ).astype(jnp.bfloat16)
    expert_ids = experts.reshape(-1)
    one_hot = (expert_ids[:, None] == jnp.arange(experts_all, dtype=jnp.int32)[None, :]).astype(
        jnp.int32
    )
    ranks = jnp.cumsum(one_hot, axis=0) - 1
    slot_index = jnp.sum(one_hot * ranks, axis=1)
    destination = expert_ids * capacity + slot_index
    token_index = jnp.arange(rows_here * topk, dtype=jnp.int32) // topk
    outgoing = jnp.zeros((experts_all * capacity, normed.shape[1]), jnp.bfloat16)
    outgoing = (
        outgoing.at[destination]
        .set(normed[token_index])
        .reshape(experts_all, capacity, normed.shape[1])
    )
    arrived = lax.all_to_all(outgoing, "ep", split_axis=0, concat_axis=0, tiled=True)
    slots = arrived.shape[1]
    flat_rows = arrived.reshape(-1, D)
    gate_part = jnp.dot(flat_rows, w_gate[0], preferred_element_type=jnp.float32)
    up_part = jnp.dot(flat_rows, w_up[0], preferred_element_type=jnp.float32)
    hidden = (jax.nn.silu(gate_part) * up_part).astype(jnp.bfloat16)
    partial_out = jnp.dot(hidden, w_down[0], preferred_element_type=jnp.float32).reshape(
        experts_all, slots, D
    )
    summed = lax.psum_scatter(
        partial_out.astype(jnp.bfloat16), "tp", scatter_dimension=2, tiled=True
    )
    returned = lax.all_to_all(summed, "ep", split_axis=0, concat_axis=0, tiled=True)
    picked = returned.reshape(experts_all * capacity, -1)[destination].reshape(rows_here, topk, -1)
    return jnp.einsum("tk,tkd->td", expert_weights, picked.astype(jnp.float32)).astype(jnp.bfloat16)


def per_device(
    queries,
    keys,
    values,
    log_gates,
    out_weight,
    moe_rows,
    norm_gain,
    experts,
    expert_weights,
    w_gate,
    w_up,
    w_down,
):
    mixed = mixer_half(queries, keys, values, log_gates, out_weight)
    moe_out = experts_half(moe_rows, norm_gain, experts, expert_weights, w_gate, w_up, w_down)
    return (mixed, moe_out)


def solution(mesh):
    placed = (
        P("ep", "tp"),
        P("ep", "tp"),
        P("ep", "tp"),
        P("ep", "tp"),
        P("tp", None),
        P("ep", None),
        P(),
        P("ep", None),
        P("ep", None),
        P("ep", None, "tp"),
        P("ep", None, "tp"),
        P("ep", "tp", None),
    )
    return jax.shard_map(
        per_device,
        mesh=mesh,
        in_specs=placed,
        out_specs=(P(("ep", "tp"), None), P("ep", "tp")),
        check_vma=False,
    )
```

profile of v0, /device:TPU:1, one launch (start us, length us, event | category | flops | bytes accessed | tf_op | source)
XLA Modules:
  0.0 483.3 jit_solution(13519128477922005688)
XLA Ops:
  14.2 12.8 %scatter_custom_fusion = bf16[1024,2048]{1,0:T(8,128)(2,1)} fusion(s32[512]{0:T(512)S(1)} %bitcast.95, bf16[256,2048]{1,0:T(8,128)(2,1)S(1)} %fusion.10, s32[1024]{0:T(1024)S(1)} %pad_clamp_fusion.1, bf16[]{:T(256)} %constant.103.clone.1), kind=kCustom, calls=%fused_computation.29 | custom fusion | bytes 4194306 | tf_op jit(solution)/shard_map/scatter | solution.py:151
  27.0 13.5 %all-to-all-start = ((bf16[64,16,2048]{2,1,0:T(8,128)(2,1)}), bf16[64,16,2048]{2,1,0:T(8,128)(2,1)}, u32[]{:S(2)}, u32[]{:S(2)}) async-start(bf16[64,16,2048]{2,1,0:T(8,128)(2,1)} %bitcast.86), calls=%async_computation.1 | async-start | bytes 8388608 | tf_op jit(solution)/shard_map/all_to_all | solution.py:154
  41.4 104.0 %all-to-all-done = bf16[64,16,2048]{2,1,0:T(8,128)(2,1)} async-done(((bf16[64,16,2048]{2,1,0:T(8,128)(2,1)}), bf16[64,16,2048]{2,1,0:T(8,128)(2,1)}, u32[]{:S(2)}, u32[]{:S(2)}) %all-to-all-start) | async-done | bytes 4194336 | tf_op jit(solution)/shard_map/all_to_all | solution.py:154
  145.4 3.5 fusion.17
  148.9 3.5 fusion.14
  152.4 3.2 convolution_convert_fusion
  158.7 44.5 %all_gather.10 = f32[16384,4]{0,1:T(4,128)S(1)} all-gather(f32[256,4]{0,1:T(4,128)S(1)} %copy-done.5), channel_id=1, replica_groups=mesh['ep'=64,'tp'=4] {'ep'}, dimensions={0}, use_global_device_ids=true | all-gather | bytes 266240 | tf_op jit(solution)/shard_map/all_gather | solution.py:103
  203.2 4.8 all-gather.5.cloned.1.call-done
  208.0 226.4 %conditional.1 = (f32[2,2,256]{2,1,0:T(2,128)}, f32[2,2,256,64]{2,3,1,0:T(8,128)}) conditional(s32[]{:T(128)} %bitcast.1, () %tuple.30, (bf16[256,256]{1,0:T(8,128)(2,1)S(1)}, s32[256]{0:T(256)}, bf16[16384,128]{0,1:T(8,128)(2,1)}, f32[2,2,256]{2,1,0:T(2,128)}, f32[16384,4]{0,1:T(4,128)S(1)}, /*index=5*/bf16[16384,128]{0,1:T(8,128)(2,1)}) %tuple.71), branch_computations={%region_0.0_spmd, %region_1.6_spmd} | conditional | flops 139269632 | bytes 8373595 | solution.py:77
  208.8 225.7 %while.17 = (s32[]{:T(128)}, f32[2,2,256]{2,1,0:T(2,128)S(1)}, f32[2,2,256]{2,1,0:T(2,128)}, f32[2,2,256,64]{2,3,1,0:T(8,128)}, s32[256]{0:T(256)}, /*index=5*/b...) while((s32[]{:T(128)}, f32[2,2,256]{2,1,0:T(2,128)S(1)}, ...), condition=%wide.region_5.5_spmd.clone, body=%wide.region_2.4_spmd.clone.sunk | while | flops 139269632 | bytes 8111315 | solution.py:72
  226.4 2.1 convolution_add_fusion.2
  233.5 2.1 convolution_add_fusion.2
  240.6 2.1 convolution_add_fusion.2
  261.9 2.1 convolution_add_fusion.2
  276.1 2.1 convolution_add_fusion.2
  283.2 2.1 convolution_add_fusion.2
  290.3 2.1 convolution_add_fusion.2
  297.4 2.1 convolution_add_fusion.2
  311.6 2.1 convolution_add_fusion.2
  318.7 2.1 convolution_add_fusion.2
  332.9 2.1 convolution_add_fusion.2
  340.0 2.1 convolution_add_fusion.2
  347.1 2.1 convolution_add_fusion.2
  354.2 2.1 convolution_add_fusion.2
  368.4 2.1 convolution_add_fusion.2
  389.7 2.1 convolution_add_fusion.2
  403.9 2.1 convolution_add_fusion.2
  411.1 2.1 convolution_add_fusion.2
  418.2 2.1 convolution_add_fusion.2
  425.3 2.1 convolution_add_fusion.2
  435.6 8.5 %all-to-all-start.1 = ((bf16[64,16,512]{2,1,0:T(8,128)(2,1)}), bf16[64,16,512]{2,1,0:T(8,128)(2,1)S(1)}, u32[]{:S(2)}, u32[]{:S(2)}) async-start(bf16[64,16,512]{2,1,0:T(8,128)(2,1)} %reduce-scatter.5.cloned.1.call-done), calls=%async_computation.3 | async-start | bytes 2097152 | tf_op jit(solution)/shard_map/all_to_all | solution.py:166
  445.9 26.4 %all-to-all-done.1 = bf16[64,16,512]{2,1,0:T(8,128)(2,1)S(1)} async-done(((bf16[64,16,512]{2,1,0:T(8,128)(2,1)}), bf16[64,16,512]{2,1,0:T(8,128)(2,1)S(1)}, u32[]{:S(2)}, u32[]{:S(2)}) %all-to-all-start.1) | async-done | bytes 1048608 | tf_op jit(solution)/shard_map/all_to_all | solution.py:166
  (402 shorter events, 198.7 us)
Async XLA Ops:
  8.0 144.4 %copy-start = (bf16[1,256,2048]{2,1,0:T(8,128)(2,1)S(1)}, bf16[1,256,2048]{2,1,0:T(8,128)(2,1)}, u32[]{:S(2)}) copy-start(bf16[1,256,2048]{2,1,0:T(8,128)(2,1)} %param.27) | copy-start | bytes 3145732
  8.0 5.5 %copy-start.1 = (bf16[256,2048]{1,0:T(8,128)(2,1)S(1)}, bf16[256,2048]{1,0:T(8,128)(2,1)}, u32[]{:S(2)}) copy-start(bf16[256,2048]{1,0:T(8,128)(2,1)} %param.21) | copy-start | bytes 3145732
  8.0 5.8 %copy-start.6 = (f32[2048]{0:T(1024)S(1)}, f32[2048]{0:T(1024)}, u32[]{:S(2)}) copy-start(f32[2048]{0:T(1024)} %param.22) | copy-start | bytes 24580
  8.0 195.2 %all-gather.3.cloned.1.call-start = ((), (), s32[]{:S(2)}) async-start(), calls=%async_computation.4 | async-start | bytes 4259840 | tf_op jit(solution)/shard_map/all_gather | solution.py:97
  13.9 13.1 %copy-start.7 = (s32[512,1]{0,1:T(1,128)}, s32[512,1]{0,1:T(1,128)S(1)}, u32[]{:S(2)}) copy-start(s32[512,1]{0,1:T(1,128)S(1)} %compare_select_fusion.1) | copy-start | bytes 6148
  27.0 13.5 %copy-start.4 = (bf16[256,128]{1,0:T(8,128)(2,1)S(1)}, bf16[256,128]{1,0:T(8,128)(2,1)}, u32[]{:S(2)}) copy-start(bf16[256,128]{1,0:T(8,128)(2,1)} %param.18) | copy-start | bytes 196612
  27.0 118.3 %copy-start.10 = (bf16[1,2048,256]{2,1,0:T(8,128)(2,1)S(1)}, bf16[1,2048,256]{2,1,0:T(8,128)(2,1)}, u32[]{:S(2)}) copy-start(bf16[1,2048,256]{2,1,0:T(8,128)(2,1)} %param.25) | copy-start | bytes 3145732
  27.0 118.3 %all-to-all-start = ((bf16[64,16,2048]{2,1,0:T(8,128)(2,1)}), bf16[64,16,2048]{2,1,0:T(8,128)(2,1)}, u32[]{:S(2)}, u32[]{:S(2)}) async-start(bf16[64,16,2048]{2,1,0:T(8,128)(2,1)} %bitcast.86), calls=%async_computation.1 | async-start | bytes 8388608 | tf_op jit(solution)/shard_map/all_to_all | solution.py:154
  40.5 167.5 %all-gather.5.cloned.1.call-start = ((), (), s32[]{:S(2)}) async-start(), calls=%async_computation.5 | async-start | bytes 4259840 | tf_op jit(solution)/shard_map/all_gather | solution.py:100
  41.3 394.2 %reduce-scatter.5.cloned.1.call-start = ((), (), s32[]{:S(2)}) async-start(), calls=%async_computation.7 | async-start | bytes 5242880 | tf_op jit(solution)/shard_map/reduce_scatter | solution.py:163
  145.4 3.5 copy-start.11
  155.6 2.5 copy-start.5
  155.6 52.4 %copy-start.3 = (bf16[256,256]{1,0:T(8,128)(2,1)S(1)}, bf16[256,256]{1,0:T(8,128)(2,1)}, u32[]{:S(2)}) copy-start(bf16[256,256]{1,0:T(8,128)(2,1)} %param.16) | copy-start | bytes 393220
  434.5 9.7 %copy-start.2 = (bf16[256,2048]{1,0:T(8,128)(2,1)S(1)}, bf16[256,2048]{1,0:T(8,128)(2,1)}, u32[]{:S(2)}) copy-start(bf16[256,2048]{1,0:T(8,128)(2,1)} %param.20) | copy-start | bytes 3145732
  435.6 36.7 %all-to-all-start.1 = ((bf16[64,16,512]{2,1,0:T(8,128)(2,1)}), bf16[64,16,512]{2,1,0:T(8,128)(2,1)S(1)}, u32[]{:S(2)}, u32[]{:S(2)}) async-start(bf16[64,16,512]{2,1,0:T(8,128)(2,1)} %reduce-scatter.5.cloned.1.call-done), calls=%async_computation.3 | async-start | bytes 2097152 | tf_op jit(solution)/shard_map/all_to_all | solution.py:166
  444.1 1.5 copy-start.9
  444.1 1.7 copy-start.8
  444.1 31.8 %reduce-scatter.3.cloned.1.call-start = ((), (), s32[]{:S(2)}) async-start(), calls=%async_computation.6 | async-start | bytes 1310720 | tf_op jit(solution)/shard_map/reduce_scatter | solution.py:121
Sparse Core Ops, SparseCore 0:
  12.1 118.5 all-gather.2
  133.9 74.1 all-gather.4
Sparse Core Ops, SparseCore 1:
  155.7 47.2 reduce-scatter.4
  447.8 25.6 reduce-scatter.2
where the time goes:
time: 487 us; the launch traced here: 483 us
  waiting for transfers between devices  135 us (28%)
  matrix products  130 us (27%)
  other arithmetic  79 us (16%)
  local copies, waits for them, and re-layouts  54.9 us (11%)
  blocking collectives  44.5 us (9%)
  starting transfers between devices  22.2 us (5%)
  between operations  16.4 us (3%)
    all_to_all x1, waiting for transfers between devices, experts_half(): lax.all_to_all(outgoing, 'ep', split_axis=0, concat_axis=0, tiled=True)  104 us
    dot_general x32, matrix products, one_block(): jnp.einsum('grqk,kgd->grqd', weights.astype(jnp.bfloat16), value_block, p...  66.6 us
    dot_general x32, matrix products, one_block(): jnp.einsum('qgrd,kgd->grqk', query_heads, key_block, preferred_element_ty...  50.8 us
    all_gather x1, blocking collectives, mixer_half(): gate_part = lax.all_gather(log_gates, 'ep', axis=0, tiled=True)  44.5 us
    add x32, other arithmetic, one_block(): running_sum = running_sum * rescale + jnp.sum(weights, axis=-1)  40.5 us
    dynamic_slice x32, local copies, waits for them, and re-layouts, one_block(): lax.dynamic_slice_in_dim(value_part, first, key_span, 0)  31.6 us
    all_to_all x1, waiting for transfers between devices, experts_half(): lax.all_to_all(summed, 'ep', split_axis=0, concat_axis=0, tiled=True)  26.4 us
    le x32, other arithmetic, one_block(): key_position[None, :] <= query_position[:, None]  24.3 us
  transfers between devices with their start and end apart: 6, of which 3 were waited for; matrix products, arithmetic and copies ran while one was open for 54% of the time, Pallas kernels for 0%

commit v1 on v0

v1 whole, which is shorter than its diff:
```python
import functools

import jax
import jax.numpy as jnp
from jax import lax
from jax.experimental import pallas as pl
from jax.experimental.pallas import tpu as pltpu
from jax.sharding import PartitionSpec as P

HD = 64
EPSILON = 1e-06
MASKED = -1e30
F32 = jnp.float32
BF16 = jnp.bfloat16
HEAD_ROWS = 80


def whole(shape):
    return pl.BlockSpec(shape, lambda *_: (0,) * len(shape))


def pack_body(keys_ref, values_ref, gates_ref, out_ref):
    rows = keys_ref.shape[0]
    half = rows // 2
    keys_t = keys_ref[...].astype(F32).T
    gates = gates_ref[...]
    high = gates.astype(BF16).astype(F32)
    rest = gates - high
    mid = rest.astype(BF16).astype(F32)
    low = rest - mid
    pad = jnp.zeros((10, rows), F32)
    for g in range(2):
        pieces = []
        for r in range(2):
            h = 2 * g + r
            pieces += [high[h : h + 1], mid[h : h + 1], low[h : h + 1]]
        block = jnp.concatenate([keys_t[g * HD : (g + 1) * HD]] + pieces + [pad], axis=0)
        out_ref[pl.ds(g * HEAD_ROWS, HEAD_ROWS), :] = block.astype(BF16)
    out_ref[pl.ds(2 * HEAD_ROWS, half), pl.ds(0, 128)] = values_ref[pl.ds(0, half), :]
    out_ref[pl.ds(2 * HEAD_ROWS, half), pl.ds(128, 128)] = values_ref[pl.ds(half, half), :]


def pack_keys(keys, values, gates_t):
    rows = keys.shape[0]
    height = 2 * HEAD_ROWS + rows // 2
    return pl.pallas_call(
        pack_body,
        out_shape=jax.ShapeDtypeStruct((height, rows), BF16),
        name="pack_keys",
    )(keys, values, gates_t)


def attention_body(index_ref, q_ref, kv_ref, w_ref, o_ref, qa_ref, acc_ref, max_ref, *, per_step):
    step = pl.program_id(0)
    own = index_ref[0]
    last = own // per_step
    rows = q_ref.shape[0]
    span = per_step * rows

    @pl.when(step == 0)
    def _():
        column = lax.broadcasted_iota(jnp.int32, (rows, 16), 1)
        for g in range(2):
            for r in range(2):
                h = 2 * g + r
                scaled = q_ref[:, h * HD : (h + 1) * HD].astype(F32) * HD ** (-0.5)
                picks = jnp.where((column >= 3 * r) & (column < 3 * r + 3), -1.0, 0.0)
                qa_ref[g, pl.ds(r * rows, rows), :] = jnp.concatenate(
                    [scaled, picks.astype(F32)], axis=1
                ).astype(BF16)
        acc_ref[...] = jnp.zeros_like(acc_ref)
        max_ref[...] = jnp.full_like(max_ref, MASKED)

    def run(masked):
        values = []
        for c in range(per_step):
            packed = kv_ref[c, pl.ds(2 * HEAD_ROWS, rows // 2), :]
            values += [packed[:, :128], packed[:, 128:]]
        values = jnp.concatenate(values, axis=0)
        values = jnp.concatenate([values, jnp.ones_like(values)], axis=1)
        for g in range(2):
            keys = jnp.concatenate(
                [kv_ref[c, pl.ds(g * HEAD_ROWS, HEAD_ROWS), :] for c in range(per_step)], axis=1
            )
            scores = jnp.dot(qa_ref[g], keys, preferred_element_type=F32)
            if masked:
                key_at = step * span + lax.broadcasted_iota(jnp.int32, scores.shape, 1)
                query_at = own * rows + lax.broadcasted_iota(jnp.int32, scores.shape, 0) % rows
                scores = jnp.where(key_at <= query_at, scores, MASKED)
            old = max_ref[g]
            new = jnp.maximum(old, jnp.max(scores, axis=1, keepdims=True))
            weights = jnp.exp(scores - new[:, :1]).astype(BF16)
            rescale = jnp.exp(old - new)
            max_ref[g] = new
            acc_ref[g] = acc_ref[g] * jnp.concatenate([rescale, rescale], axis=1) + jnp.dot(
                weights, values, preferred_element_type=F32
            )

    @pl.when(step < last)
    def _():
        run(False)

    @pl.when(step == last)
    def _():
        run(True)
        heads = []
        for g in range(2):
            done = acc_ref[g, :, :128] / acc_ref[g, :, 128:]
            for r in range(2):
                heads.append(done[r * rows : (r + 1) * rows, g * HD : (g + 1) * HD])
        attended = jnp.concatenate(heads, axis=1).astype(BF16)
        o_ref[...] = jnp.dot(attended, w_ref[...], preferred_element_type=F32).astype(BF16)


def attention(own_index, queries, packed, out_weight):
    parts, height, rows = packed.shape
    per_step = 4
    steps = parts // per_step
    wide = out_weight.shape[1]
    return pl.pallas_call(
        functools.partial(attention_body, per_step=per_step),
        grid_spec=pltpu.PrefetchScalarGridSpec(
            num_scalar_prefetch=1,
            grid=(steps,),
            in_specs=[
                whole(queries.shape),
                pl.BlockSpec(
                    (per_step, height, rows),
                    lambda s, own: (jnp.minimum(s, own[0] // per_step), 0, 0),
                ),
                whole(out_weight.shape),
            ],
            out_specs=whole((rows, wide)),
            scratch_shapes=[
                pltpu.VMEM((2, 2 * rows, HEAD_ROWS), BF16),
                pltpu.VMEM((2, 2 * rows, 256), F32),
                pltpu.VMEM((2, 2 * rows, 128), F32),
            ],
        ),
        out_shape=jax.ShapeDtypeStruct((rows, wide), BF16),
        compiler_params=pltpu.CompilerParams(dimension_semantics=("arbitrary",)),
        cost_estimate=pl.CostEstimate(
            flops=20_000_000_000, transcendentals=17_000_000, bytes_accessed=11_000_000
        ),
        name="attention",
    )(own_index, queries, packed, out_weight)


def mixer_half(queries, keys, values, log_gates, out_weight):
    packed = pack_keys(keys, values, log_gates.T)
    gathered = lax.all_gather(packed, "ep", axis=0, tiled=False)
    own_index = lax.axis_index("ep").astype(jnp.int32).reshape(1)
    partial = attention(own_index, queries, gathered, out_weight)
    return lax.psum_scatter(partial, "tp", scatter_dimension=0, tiled=True)


def dispatch_body(
    index_ref, rows_ref, part_ref, gain_ref, experts_t_ref, experts_ref, send_ref, slot_ref, *, cap
):
    tokens = rows_ref.shape[0]
    slots = send_ref.shape[0]
    count = slots // cap
    rows = rows_ref[...].astype(F32)
    scale = lax.rsqrt(jnp.mean(rows * rows, axis=1, keepdims=True) + EPSILON)
    normed = (part_ref[...].astype(F32) * scale * gain_ref[...]).astype(BF16)
    expert_at = lax.broadcasted_iota(jnp.int32, (count, tokens), 0)
    first = (expert_at == experts_t_ref[0:1, :]).astype(F32)
    second = (expert_at == experts_t_ref[1:2, :]).astype(F32)
    earlier = (
        lax.broadcasted_iota(jnp.int32, (tokens, tokens), 0)
        < lax.broadcasted_iota(jnp.int32, (tokens, tokens), 1)
    ).astype(BF16)
    base = (expert_at * cap).astype(F32)
    before_first = jnp.dot(first.astype(BF16), earlier, preferred_element_type=F32)
    before_second = jnp.dot(second.astype(BF16), earlier, preferred_element_type=F32) + jnp.sum(
        first, axis=1, keepdims=True
    )
    to_first = jnp.sum(first * (base + before_first), axis=0, keepdims=True).astype(jnp.int32)
    to_second = jnp.sum(second * (base + before_second), axis=0, keepdims=True).astype(jnp.int32)
    slot_at = lax.broadcasted_iota(jnp.int32, (slots, tokens), 0)
    chosen = ((slot_at == to_first) | (slot_at == to_second)).astype(F32).astype(BF16)
    send_ref[...] = jnp.dot(chosen, normed, preferred_element_type=F32).astype(BF16)
    expert_at = lax.broadcasted_iota(jnp.int32, (tokens, count), 1)
    first = (expert_at == experts_ref[:, 0:1]).astype(F32)
    second = (expert_at == experts_ref[:, 1:2]).astype(F32)
    earlier = (
        lax.broadcasted_iota(jnp.int32, (tokens, tokens), 1)
        < lax.broadcasted_iota(jnp.int32, (tokens, tokens), 0)
    ).astype(BF16)
    base = (expert_at * cap).astype(F32)
    before_first = jnp.dot(earlier, first.astype(BF16), preferred_element_type=F32)
    before_second = jnp.dot(earlier, second.astype(BF16), preferred_element_type=F32) + jnp.sum(
        first, axis=0, keepdims=True
    )
    to_first = jnp.sum(first * (base + before_first), axis=1, keepdims=True)
    to_second = jnp.sum(second * (base + before_second), axis=1, keepdims=True)
    slot_ref[:, 0:1] = to_first.astype(jnp.int32)
    slot_ref[:, 1:2] = to_second.astype(jnp.int32)


def dispatch(tp_index, moe_rows, norm_gain, experts, count, tp):
    tokens, width = moe_rows.shape
    cap = 4 * tokens // count
    part = width // tp
    return pl.pallas_call(
        functools.partial(dispatch_body, cap=cap),
        grid_spec=pltpu.PrefetchScalarGridSpec(
            num_scalar_prefetch=1,
            grid=(1,),
            in_specs=[
                whole(moe_rows.shape),
                pl.BlockSpec((tokens, part), lambda s, own: (0, own[0])),
                pl.BlockSpec((1, part), lambda s, own: (0, own[0])),
                whole((2, tokens)),
                whole((tokens, 2)),
            ],
            out_specs=[whole((count * cap, part)), whole((tokens, 2))],
        ),
        out_shape=[
            jax.ShapeDtypeStruct((count * cap, part), BF16),
            jax.ShapeDtypeStruct((tokens, 2), jnp.int32),
        ],
        name="dispatch",
    )(tp_index, moe_rows, moe_rows, norm_gain.reshape(1, -1), experts.T, experts)


def gather_over_tp(own):
    size = lax.axis_size("tp")
    up = [(n, (n + 1) % size) for n in range(size)]
    down = [(n, (n - 1) % size) for n in range(size)]
    half = own.shape[0] // 2
    previous = lax.ppermute(own, "tp", up)
    following = lax.ppermute(own, "tp", down)
    far_low = lax.ppermute(previous[:half], "tp", up)
    far_high = lax.ppermute(following[half:], "tp", down)
    return own, previous, following, far_low, far_high


def pick_parts(index_ref, refs, steps):
    own, previous, following, far_low, far_high = refs
    low = pl.program_id(0) < steps // 2
    tp = index_ref[0]
    return (
        (tp, own[...]),
        (lax.rem(tp + 3, 4), previous[...]),
        (lax.rem(tp + 1, 4), following[...]),
        (lax.rem(tp + 2, 4), jnp.where(low, far_low[...], far_high[...])),
    )


def part_specs(tall, wide, steps):
    block = tall // steps
    half = steps // 2
    straight = pl.BlockSpec((block, wide), lambda s, own: (s, 0))
    return [
        straight,
        straight,
        straight,
        pl.BlockSpec((block, wide), lambda s, own: (jnp.minimum(s, half - 1), 0)),
        pl.BlockSpec((block, wide), lambda s, own: (jnp.maximum(s - half, 0), 0)),
    ]


def up_body(index_ref, a, b, c, d, e, gate_ref, up_ref, out_ref, *, steps):
    gate = up = None
    for number, rows in pick_parts(index_ref, (a, b, c, d, e), steps):
        to_gate = jnp.dot(rows, gate_ref[number], preferred_element_type=F32)
        to_up = jnp.dot(rows, up_ref[number], preferred_element_type=F32)
        gate = to_gate if gate is None else gate + to_gate
        up = to_up if up is None else up + to_up
    out_ref[...] = (gate / (1.0 + jnp.exp(-gate)) * up).astype(BF16)


def up_projections(tp_index, parts, w_gate, w_up, tp):
    tall, wide = parts[0].shape
    steps = 4
    hidden = w_gate.shape[1]
    return pl.pallas_call(
        functools.partial(up_body, steps=steps),
        grid_spec=pltpu.PrefetchScalarGridSpec(
            num_scalar_prefetch=1,
            grid=(steps,),
            in_specs=part_specs(tall, wide, steps)
            + [whole((tp, wide, hidden)), whole((tp, wide, hidden))],
            out_specs=pl.BlockSpec((tall // steps, hidden), lambda s, own: (s, 0)),
        ),
        out_shape=jax.ShapeDtypeStruct((tall, hidden), BF16),
        cost_estimate=pl.CostEstimate(
            flops=2_200_000_000, transcendentals=262_144, bytes_accessed=6_800_000
        ),
        name="up_projections",
    )(tp_index, *parts, w_gate.reshape(tp, wide, hidden), w_up.reshape(tp, wide, hidden))


def down_body(index_ref, a, b, c, d, e, down_ref, out_ref, *, steps):
    total = None
    for number, rows in pick_parts(index_ref, (a, b, c, d, e), steps):
        term = jnp.dot(rows, down_ref[number], preferred_element_type=F32)
        total = term if total is None else total + term
    out_ref[...] = total.astype(BF16)


def down_projection(tp_index, parts, w_down, tp):
    tall, wide = parts[0].shape
    steps = 4
    columns = w_down.shape[1]
    return pl.pallas_call(
        functools.partial(down_body, steps=steps),
        grid_spec=pltpu.PrefetchScalarGridSpec(
            num_scalar_prefetch=1,
            grid=(steps,),
            in_specs=part_specs(tall, wide, steps) + [whole((tp, wide, columns))],
            out_specs=pl.BlockSpec((tall // steps, columns), lambda s, own: (s, 0)),
        ),
        out_shape=jax.ShapeDtypeStruct((tall, columns), BF16),
        cost_estimate=pl.CostEstimate(
            flops=1_100_000_000, transcendentals=0, bytes_accessed=4_200_000
        ),
        name="down_projection",
    )(tp_index, *parts, w_down.reshape(tp, wide, columns))


def combine_body(slot_ref, weight_ref, rows_ref, out_ref):
    slots = rows_ref.shape[0]
    tokens = slot_ref.shape[0]
    slot_at = lax.broadcasted_iota(jnp.int32, (tokens, slots), 1)
    total = None
    for k in range(2):
        chosen = (slot_at == slot_ref[:, k : k + 1]).astype(F32).astype(BF16)
        picked = jnp.dot(chosen, rows_ref[...], preferred_element_type=F32)
        term = picked * weight_ref[:, k : k + 1]
        total = term if total is None else total + term
    out_ref[...] = total.astype(BF16)


def combine(slots, expert_weights, rows):
    return pl.pallas_call(
        combine_body,
        out_shape=jax.ShapeDtypeStruct((slots.shape[0], rows.shape[1]), BF16),
        name="combine",
    )(slots, expert_weights, rows)


def experts_half(moe_rows, norm_gain, experts, expert_weights, w_gate, w_up, w_down):
    count = lax.axis_size("ep")
    tp = lax.axis_size("tp")
    tp_index = lax.axis_index("tp").astype(jnp.int32).reshape(1)
    down_columns = lax.all_to_all(w_down[0], "tp", split_axis=1, concat_axis=0, tiled=True)
    outgoing, slots = dispatch(tp_index, moe_rows, norm_gain, experts, count, tp)
    part = outgoing.shape[1]
    arrived = lax.all_to_all(
        outgoing.reshape(count, -1, part), "ep", split_axis=0, concat_axis=0, tiled=True
    ).reshape(-1, part)
    hidden = up_projections(tp_index, gather_over_tp(arrived), w_gate[0], w_up[0], tp)
    result = down_projection(tp_index, gather_over_tp(hidden), down_columns, tp)
    returned = lax.all_to_all(
        result.reshape(count, -1, part), "ep", split_axis=0, concat_axis=0, tiled=True
    ).reshape(-1, part)
    return combine(slots, expert_weights, returned)


def per_device(
    queries,
    keys,
    values,
    log_gates,
    out_weight,
    moe_rows,
    norm_gain,
    experts,
    expert_weights,
    w_gate,
    w_up,
    w_down,
):
    mixed = mixer_half(queries, keys, values, log_gates, out_weight)
    moe_out = experts_half(moe_rows, norm_gain, experts, expert_weights, w_gate, w_up, w_down)
    return (mixed, moe_out)


def solution(mesh):
    placed = (
        P("ep", "tp"),
        P("ep", "tp"),
        P("ep", "tp"),
        P("ep", "tp"),
        P("tp", None),
        P("ep", None),
        P(),
        P("ep", None),
        P("ep", None),
        P("ep", None, "tp"),
        P("ep", None, "tp"),
        P("ep", "tp", None),
    )
    return jax.shard_map(
        per_device,
        mesh=mesh,
        in_specs=placed,
        out_specs=(P(("ep", "tp"), None), P("ep", "tp")),
        check_vma=False,
    )
```

time: 487 us -> 228 us (0.47)
  matrix products: 130 us -> 0 us
  other arithmetic: 79 us -> 0 us
  waiting for transfers between devices: 135 us -> 71 us
  local copies, waits for them, and re-layouts: 54.9 us -> 6.88 us
  starting transfers between devices: 22.2 us -> 63.5 us
  Pallas kernels: 0 us -> 25 us
    dot_general x69 -> x0, matrix products: 130 us -> none  [the longest x32 66.6 us: one_block(): jnp.einsum('grqk,kgd->grqd', weights.astype(jnp.bfloat16), value_block, p...]
    all_to_all x2, waiting for transfers between devices: 130 us -> 29.7 us  [the longest x1 27.4 us: experts_half(): lax.all_to_all(result.reshape(count, -1, part), 'ep', split_axis=0, conca...]
    all_to_all x0 -> x1, blocking collectives: none -> 47 us  [experts_half(): lax.all_to_all(outgoing.reshape(count, -1, part), 'ep', split_axis=0, con...]
    all_gather x1 -> x0, blocking collectives: 44.5 us -> none  [mixer_half(): gate_part = lax.all_gather(log_gates, 'ep', axis=0, tiled=True)]
    ppermute x0 -> x8, waiting for transfers between devices: none -> 41.2 us  [the longest x2 26.7 us: gather_over_tp(): previous = lax.ppermute(own, 'tp', up)]
    add x65 -> x0, other arithmetic: 41.2 us -> none  [the longest x32 40.5 us: one_block(): running_sum = running_sum * rescale + jnp.sum(weights, axis=-1)]
    dynamic_slice x64 -> x0, local copies, waits for them, and re-layouts: 31.6 us -> none  [the longest x32 31.6 us: one_block(): lax.dynamic_slice_in_dim(value_part, first, key_span, 0)]
    all_to_all x2, starting transfers between devices: 22 us -> 52.3 us  [the longest x1 48.8 us: experts_half(): lax.all_to_all(result.reshape(count, -1, part), 'ep', split_axis=0, conca...]
  transfers between devices with their start and end apart: 6 -> 12, of which waited for: 3 -> 7; matrix products, arithmetic and copies ran while one was open for 54% -> 2% of each run, Pallas kernels for 0% -> 10%
where the time goes in v1:
time: 228 us
  waiting for transfers between devices  71 us (31%)
  starting transfers between devices  63.5 us (28%)
  blocking collectives  47 us (21%)
  Pallas kernels  25 us (11%)
  between operations  14.2 us (6%)
  local copies, waits for them, and re-layouts  6.88 us (3%)
    all_to_all x1, starting transfers between devices, experts_half(): lax.all_to_all(result.reshape(count, -1, part), 'ep', split_axis=0, conca...  48.8 us
    all_to_all x1, blocking collectives, experts_half(): lax.all_to_all(outgoing.reshape(count, -1, part), 'ep', split_axis=0, con...  47 us
    all_to_all x1, waiting for transfers between devices, experts_half(): lax.all_to_all(result.reshape(count, -1, part), 'ep', split_axis=0, conca...  27.4 us
    ppermute x2, waiting for transfers between devices, gather_over_tp(): previous = lax.ppermute(own, 'tp', up)  26.7 us
    ppermute x2, waiting for transfers between devices, gather_over_tp(): far_low = lax.ppermute(previous[:half], 'tp', up)  14.2 us
    pallas_call x1, Pallas kernels, up_projections(): pl.pallas_call(functools.partial(up_body, steps=steps), grid_spec=pltpu.P...  6.32 us
    pallas_call x1, Pallas kernels, attention(): pl.pallas_call(functools.partial(attention_body, per_step=per_step), grid...  6.06 us
    ppermute x2, starting transfers between devices, gather_over_tp(): far_high = lax.ppermute(following[half:], 'tp', down)  5.62 us
  transfers between devices with their start and end apart: 12, of which 7 were waited for; matrix products, arithmetic and copies ran while one was open for 2% of the time, Pallas kernels for 10%

profile of v1, /device:TPU:1, one launch (start us, length us, event | category | flops | bytes accessed | tf_op | source)
XLA Modules:
  0.0 227.6 jit_solution(9225971107453707084)
XLA Ops:
  7.2 1.7 pack_keys.1
  9.0 1.5 copy.16.experts_ref
  10.4 3.1 %dispatch.1 = (bf16[1024,512]{1,0:T(8,128)(2,1)}, s32[256,2]{1,0:T(8,128)}) custom-call(s32[1]{0:T(128)} %bitcast.3.index_ref, bf16[256,2048]{1,0:T(8,128)(2,1)} %part_ref.1, bf16[256,2048]{1,0:T(8,128)(2,1)} %part_ref.1, f32[1,2048]{1,0:T(1,128)} %bitcast.22, s32[2,256]{1,0:T(2,128)} %bitcast.23, s32[256,2]{1,0:T(8,128)} %copy.16.experts_ref), custom_call_target="tpu_custom_call" | custom-call | tf_op jit(solution)/shard_map/dispatch/pallas_call | solution.py:205
  13.6 47.0 %all_to_all.26 = bf16[64,16,512]{2,1,0:T(8,128)(2,1)S(1)} all-to-all(bf16[64,16,512]{2,1,0:T(8,128)(2,1)} %bitcast.21), channel_id=1, replica_groups=mesh['ep'=64,'tp'=4] {'ep'}, dimensions={0} | all-to-all | bytes 2097152 | tf_op jit(solution)/shard_map/all_to_all | solution.py:351
  60.5 1.2 collective-permute-start
  61.7 1.5 collective-permute-start.1
  63.2 22.4 %collective-permute-done.b = bf16[1024,512]{1,0:T(8,128)(2,1)S(1)} collective-permute-done((bf16[1024,512]{1,0:T(8,128)(2,1)S(1)}, bf16[1024,512]{1,0:T(8,128)(2,1)S(1)}, u32[]{:S(2)}, u32[]{:S(2)}) %collective-permute-start) | collective-permute-done | bytes 1048608 | tf_op jit(solution)/shard_map/ppermute | solution.py:232
  85.7 0.1 collective-permute-start.2
  85.8 2.7 %collective-permute-start.3 = (bf16[512,512]{1,0:T(8,128)(2,1)S(1)}, bf16[512,512]{1,0:T(8,128)(2,1)S(1)}, u32[]{:S(2)}, u32[]{:S(2)}) collective-permute-start(bf16[512,512]{1,0:T(8,128)(2,1)S(1)} %slice.17), channel_id=1, source_target_pairs={{0,3},{1,0},{2,1},{3,2},{4,7},{5,4},{6,5},{7,6},{8,11},{9,8},{10,9... | collective-permute-start | bytes 1572872 | tf_op jit(solution)/shard_map/ppermute | solution.py:235
  88.6 10.3 %collective-permute-done.2.d = bf16[512,512]{1,0:T(8,128)(2,1)S(1)} collective-permute-done((bf16[512,512]{1,0:T(8,128)(2,1)S(1)}, bf16[512,512]{1,0:T(8,128)(2,1)S(1)}, u32[]{:S(2)}, u32[]{:S(2)}) %collective-permute-start.2) | collective-permute-done | bytes 524320 | tf_op jit(solution)/shard_map/ppermute | solution.py:234
  98.9 0.8 copy-done.11
  99.7 0.2 copy-done.12
  99.9 6.3 %up_projections.1.a = bf16[1024,256]{1,0:T(8,128)(2,1)} custom-call(s32[1]{0:T(128)} %bitcast.3.index_ref, bf16[1024,512]{1,0:T(8,128)(2,1)} %bitcast.20, bf16[1024,512]{1,0:T(8,128)(2,1)} %copy-done.8, bf16[1024,512]{1,0:T(8,128)(2,1)} %copy-done.9, bf16[512,512]{1,0:T(8,128)(2,1)} %copy-done.11, bf16[512,512]{1,0:T(8,128)(2,1)} %copy-done.12, ...), custom_call_target="tpu_custom_call" | custom-call | flops 2200000000 | bytes 6800000 | tf_op jit(solution)/shard_map/up_projections/pallas_call | solution.py:278
  106.2 0.2 collective-permute-start.4
  106.3 2.5 %collective-permute-start.5 = (bf16[1024,256]{1,0:T(8,128)(2,1)}, bf16[1024,256]{1,0:T(8,128)(2,1)S(1)}, u32[]{:S(2)}, u32[]{:S(2)}) collective-permute-start(bf16[1024,256]{1,0:T(8,128)(2,1)} %up_projections.1.a), channel_id=1, source_target_pairs={{0,3},{1,0},{2,1},{3,2},{4,7},{5,4},{6,5},{7,6},{8,11},{9,8},{10,9... | collective-permute-start | bytes 1572872 | tf_op jit(solution)/shard_map/ppermute | solution.py:233
  108.9 0.5 copy.17
  109.4 1.3 copy.18
  110.7 3.5 %all-to-all-start.1 = ((bf16[256,4,512]{2,0,1:T(8,128)(2,1)}), bf16[256,4,512]{2,0,1:T(8,128)(2,1)S(1)}, u32[]{:S(2)}, u32[]{:S(2)}) async-start(bf16[256,4,512]{2,0,1:T(8,128)(2,1)} %copy.18), calls=%async_computation.2 | async-start | bytes 2097152 | tf_op jit(solution)/shard_map/all_to_all | solution.py:348
  114.3 4.3 %collective-permute-done.4.b = bf16[1024,256]{1,0:T(8,128)(2,1)S(1)} collective-permute-done((bf16[1024,256]{1,0:T(8,128)(2,1)}, bf16[1024,256]{1,0:T(8,128)(2,1)S(1)}, u32[]{:S(2)}, u32[]{:S(2)}) %collective-permute-start.4) | collective-permute-done | bytes 524320 | tf_op jit(solution)/shard_map/ppermute | solution.py:232
  118.7 2.9 %collective-permute-start.7 = (bf16[512,256]{1,0:T(8,128)(2,1)S(1)}, bf16[512,256]{1,0:T(8,128)(2,1)S(1)}, u32[]{:S(2)}, u32[]{:S(2)}) collective-permute-start(bf16[512,256]{1,0:T(8,128)(2,1)S(1)} %slice.19), channel_id=1, source_target_pairs={{0,3},{1,0},{2,1},{3,2},{4,7},{5,4},{6,5},{7,6},{8,11},{9,8},{10,9... | collective-permute-start | bytes 786440 | tf_op jit(solution)/shard_map/ppermute | solution.py:235
  121.6 6.1 %attention.1 = bf16[256,2048]{1,0:T(8,128)(2,1)} custom-call(s32[1]{0:T(128)} %bitcast.index_ref, bf16[256,256]{1,0:T(8,128)(2,1)} %q_ref.1, bf16[64,288,256]{2,1,0:T(8,128)(2,1)} %bitcast.25, bf16[256,2048]{1,0:T(8,128)(2,1)} %w_ref.1), custom_call_target="tpu_custom_call" | custom-call | flops 20000000000 | bytes 11000000 | tf_op jit(solution)/shard_map/attention/pallas_call | solution.py:120
  127.7 2.4 %all-to-all-done.1 = bf16[256,4,512]{2,0,1:T(8,128)(2,1)S(1)} async-done(((bf16[256,4,512]{2,0,1:T(8,128)(2,1)}), bf16[256,4,512]{2,0,1:T(8,128)(2,1)S(1)}, u32[]{:S(2)}, u32[]{:S(2)}) %all-to-all-start.1) | async-done | bytes 1048608 | tf_op jit(solution)/shard_map/all_to_all | solution.py:348
  130.1 3.8 %collective-permute-done.6.d = bf16[512,256]{1,0:T(8,128)(2,1)S(1)} collective-permute-done((bf16[512,256]{1,0:T(8,128)(2,1)S(1)}, bf16[512,256]{1,0:T(8,128)(2,1)S(1)}, u32[]{:S(2)}, u32[]{:S(2)}) %collective-permute-start.6) | collective-permute-done | bytes 262176 | tf_op jit(solution)/shard_map/ppermute | solution.py:234
  133.9 0.3 collective-permute-done.7.e
  134.3 0.4 copy-done.6
  134.6 0.3 copy-done.7
  135.0 5.0 %down_projection.1 = bf16[1024,512]{1,0:T(8,128)(2,1)} custom-call(s32[1]{0:T(128)} %bitcast.3.index_ref, bf16[1024,256]{1,0:T(8,128)(2,1)} %up_projections.1.a, bf16[1024,256]{1,0:T(8,128)(2,1)} %copy-done.2, bf16[1024,256]{1,0:T(8,128)(2,1)} %copy-done.3, bf16[512,256]{1,0:T(8,128)(2,1)} %copy-done.6, bf16[512,256]{1,0:T(8,128)(2,1)} %copy-done.7, ...), custom_call_target="tpu_custom_call" | custom-call | flops 1100000000 | bytes 4200000 | tf_op jit(solution)/shard_map/down_projection/pallas_call | solution.py:307
  140.0 48.8 %all-to-all-start.2 = ((bf16[64,16,512]{2,1,0:T(8,128)(2,1)}), bf16[64,16,512]{2,1,0:T(8,128)(2,1)S(1)}, u32[]{:S(2)}, u32[]{:S(2)}) async-start(bf16[64,16,512]{2,1,0:T(8,128)(2,1)} %bitcast.15), calls=%async_computation.3 | async-start | bytes 2097152 | tf_op jit(solution)/shard_map/all_to_all | solution.py:356
  188.7 0.8 copy.19.weight_ref
  189.5 27.4 %all-to-all-done.2 = bf16[64,16,512]{2,1,0:T(8,128)(2,1)S(1)} async-done(((bf16[64,16,512]{2,1,0:T(8,128)(2,1)}), bf16[64,16,512]{2,1,0:T(8,128)(2,1)S(1)}, u32[]{:S(2)}, u32[]{:S(2)}) %all-to-all-start.2) | async-done | bytes 1048608 | tf_op jit(solution)/shard_map/all_to_all | solution.py:356
  216.9 1.0 copy-done.1
  217.9 2.8 %combine.1 = bf16[256,512]{1,0:T(8,128)(2,1)} custom-call(s32[256,2]{1,0:T(8,128)} %get-tuple-element.4.slot_ref, f32[256,2]{1,0:T(8,128)} %copy.19.weight_ref, bf16[1024,512]{1,0:T(8,128)(2,1)} %bitcast.16), custom_call_target="tpu_custom_call" | custom-call | tf_op jit(solution)/shard_map/combine/pallas_call | solution.py:337
  (35 shorter events, 0.4 us)
Async XLA Ops:
  7.2 101.7 %copy-start.4 = (bf16[1,256,2048]{2,1,0:T(8,128)(2,1)S(1)}, bf16[1,256,2048]{2,1,0:T(8,128)(2,1)}, u32[]{:S(2)}) copy-start(bf16[1,256,2048]{2,1,0:T(8,128)(2,1)} %param.23) | copy-start | bytes 3145732
  7.2 114.5 %all-gather.3.cloned.1.call-start = ((), (), s32[]{:S(2)}) async-start(), calls=%async_computation.5 | async-start | bytes 9584640 | tf_op jit(solution)/shard_map/all_gather | solution.py:151
  60.5 39.3 %copy-start.5 = (bf16[64,16,512]{2,1,0:T(8,128)(2,1)}, bf16[64,16,512]{2,1,0:T(8,128)(2,1)S(1)}, u32[]{:S(2)}) copy-start(bf16[64,16,512]{2,1,0:T(8,128)(2,1)S(1)} %all_to_all.26) | copy-start | bytes 3145732
  60.5 25.1 %collective-permute-start = (bf16[1024,512]{1,0:T(8,128)(2,1)S(1)}, bf16[1024,512]{1,0:T(8,128)(2,1)S(1)}, u32[]{:S(2)}, u32[]{:S(2)}) collective-permute-start(bf16[1024,512]{1,0:T(8,128)(2,1)S(1)} %bitcast.18), channel_id=1, source_target_pairs={{0,1},{1,2},{2,3},{3,0},{4,5},{5,6},{6,7},{7,4},{8,9},{9,10},{10,1... | collective-permute-start | bytes 3145736 | tf_op jit(solution)/shard_map/ppermute | solution.py:232
  61.7 24.0 %collective-permute-start.1 = (bf16[1024,512]{1,0:T(8,128)(2,1)S(1)}, bf16[1024,512]{1,0:T(8,128)(2,1)S(1)}, u32[]{:S(2)}, u32[]{:S(2)}) collective-permute-start(bf16[1024,512]{1,0:T(8,128)(2,1)S(1)} %bitcast.19), channel_id=1, source_target_pairs={{0,3},{1,0},{2,1},{3,2},{4,7},{5,4},{6,5},{7,6},{8,11},{9,8},{10,9... | collective-permute-start | bytes 3145736 | tf_op jit(solution)/shard_map/ppermute | solution.py:233
  85.6 14.2 %copy-start.8 = (bf16[1024,512]{1,0:T(8,128)(2,1)}, bf16[1024,512]{1,0:T(8,128)(2,1)S(1)}, u32[]{:S(2)}) copy-start(bf16[1024,512]{1,0:T(8,128)(2,1)S(1)} %collective-permute-done.b) | copy-start | bytes 3145732
  85.7 13.2 %collective-permute-start.2 = (bf16[512,512]{1,0:T(8,128)(2,1)S(1)}, bf16[512,512]{1,0:T(8,128)(2,1)S(1)}, u32[]{:S(2)}, u32[]{:S(2)}) collective-permute-start(bf16[512,512]{1,0:T(8,128)(2,1)S(1)} %slice.16), channel_id=1, source_target_pairs={{0,1},{1,2},{2,3},{3,0},{4,5},{5,6},{6,7},{7,4},{8,9},{9,10},{10,1... | collective-permute-start | bytes 1572872 | tf_op jit(solution)/shard_map/ppermute | solution.py:234
  85.8 13.1 %copy-start.9 = (bf16[1024,512]{1,0:T(8,128)(2,1)}, bf16[1024,512]{1,0:T(8,128)(2,1)S(1)}, u32[]{:S(2)}) copy-start(bf16[1024,512]{1,0:T(8,128)(2,1)S(1)} %collective-permute-done.1.c) | copy-start | bytes 3145732
  85.8 13.0 %collective-permute-start.3 = (bf16[512,512]{1,0:T(8,128)(2,1)S(1)}, bf16[512,512]{1,0:T(8,128)(2,1)S(1)}, u32[]{:S(2)}, u32[]{:S(2)}) collective-permute-start(bf16[512,512]{1,0:T(8,128)(2,1)S(1)} %slice.17), channel_id=1, source_target_pairs={{0,3},{1,0},{2,1},{3,2},{4,7},{5,4},{6,5},{7,6},{8,11},{9,8},{10,9... | collective-permute-start | bytes 1572872 | tf_op jit(solution)/shard_map/ppermute | solution.py:235
  98.9 0.8 copy-start.11
  98.9 1.0 copy-start.12
  106.2 12.4 %collective-permute-start.4 = (bf16[1024,256]{1,0:T(8,128)(2,1)}, bf16[1024,256]{1,0:T(8,128)(2,1)S(1)}, u32[]{:S(2)}, u32[]{:S(2)}) collective-permute-start(bf16[1024,256]{1,0:T(8,128)(2,1)} %up_projections.1.a), channel_id=1, source_target_pairs={{0,1},{1,2},{2,3},{3,0},{4,5},{5,6},{6,7},{7,4},{8,9},{9,10},{10,1... | collective-permute-start | bytes 1572872 | tf_op jit(solution)/shard_map/ppermute | solution.py:232
  106.3 12.3 %collective-permute-start.5 = (bf16[1024,256]{1,0:T(8,128)(2,1)}, bf16[1024,256]{1,0:T(8,128)(2,1)S(1)}, u32[]{:S(2)}, u32[]{:S(2)}) collective-permute-start(bf16[1024,256]{1,0:T(8,128)(2,1)} %up_projections.1.a), channel_id=1, source_target_pairs={{0,3},{1,0},{2,1},{3,2},{4,7},{5,4},{6,5},{7,6},{8,11},{9,8},{10,9... | collective-permute-start | bytes 1572872 | tf_op jit(solution)/shard_map/ppermute | solution.py:233
  110.7 19.4 %all-to-all-start.1 = ((bf16[256,4,512]{2,0,1:T(8,128)(2,1)}), bf16[256,4,512]{2,0,1:T(8,128)(2,1)S(1)}, u32[]{:S(2)}, u32[]{:S(2)}) async-start(bf16[256,4,512]{2,0,1:T(8,128)(2,1)} %copy.18), calls=%async_computation.2 | async-start | bytes 2097152 | tf_op jit(solution)/shard_map/all_to_all | solution.py:348
  114.2 106.5 %reduce-scatter.2.cloned.1.call-start = ((), (), s32[]{:S(2)}) async-start(), calls=%async_computation.4 | async-start | bytes 1310720 | tf_op jit(solution)/shard_map/reduce_scatter | solution.py:154
  118.6 9.1 %copy-start.2 = (bf16[1024,256]{1,0:T(8,128)(2,1)}, bf16[1024,256]{1,0:T(8,128)(2,1)S(1)}, u32[]{:S(2)}) copy-start(bf16[1024,256]{1,0:T(8,128)(2,1)S(1)} %collective-permute-done.4.b) | copy-start | bytes 1572868
  118.6 15.4 %collective-permute-start.6 = (bf16[512,256]{1,0:T(8,128)(2,1)S(1)}, bf16[512,256]{1,0:T(8,128)(2,1)S(1)}, u32[]{:S(2)}, u32[]{:S(2)}) collective-permute-start(bf16[512,256]{1,0:T(8,128)(2,1)S(1)} %slice.18), channel_id=1, source_target_pairs={{0,1},{1,2},{2,3},{3,0},{4,5},{5,6},{6,7},{7,4},{8,9},{9,10},{10,1... | collective-permute-start | bytes 786440 | tf_op jit(solution)/shard_map/ppermute | solution.py:234
  118.7 9.0 %copy-start.3 = (bf16[1024,256]{1,0:T(8,128)(2,1)}, bf16[1024,256]{1,0:T(8,128)(2,1)S(1)}, u32[]{:S(2)}) copy-start(bf16[1024,256]{1,0:T(8,128)(2,1)S(1)} %collective-permute-done.5.c) | copy-start | bytes 1572868
  118.7 15.5 %collective-permute-start.7 = (bf16[512,256]{1,0:T(8,128)(2,1)S(1)}, bf16[512,256]{1,0:T(8,128)(2,1)S(1)}, u32[]{:S(2)}, u32[]{:S(2)}) collective-permute-start(bf16[512,256]{1,0:T(8,128)(2,1)S(1)} %slice.19), channel_id=1, source_target_pairs={{0,3},{1,0},{2,1},{3,2},{4,7},{5,4},{6,5},{7,6},{8,11},{9,8},{10,9... | collective-permute-start | bytes 786440 | tf_op jit(solution)/shard_map/ppermute | solution.py:235
  121.6 67.1 %copy-start.10 = (f32[256,2]{0,1:T(2,128)S(1)}, f32[256,2]{0,1:T(2,128)}, u32[]{:S(2)}) copy-start(f32[256,2]{0,1:T(2,128)} %param.20) | copy-start | bytes 6148
  130.1 4.2 %copy-start = (bf16[256,4,512]{2,0,1:T(8,128)(2,1)}, bf16[256,4,512]{2,0,1:T(8,128)(2,1)S(1)}, u32[]{:S(2)}) copy-start(bf16[256,4,512]{2,0,1:T(8,128)(2,1)S(1)} %all-to-all-done.1) | copy-start | bytes 3145732
  133.9 0.7 copy-start.6
  134.3 0.7 copy-start.7
  140.0 76.9 %all-to-all-start.2 = ((bf16[64,16,512]{2,1,0:T(8,128)(2,1)}), bf16[64,16,512]{2,1,0:T(8,128)(2,1)S(1)}, u32[]{:S(2)}, u32[]{:S(2)}) async-start(bf16[64,16,512]{2,1,0:T(8,128)(2,1)} %bitcast.15), calls=%async_computation.3 | async-start | bytes 2097152 | tf_op jit(solution)/shard_map/all_to_all | solution.py:356
  216.9 1.0 copy-start.1
Sparse Core Ops, SparseCore 0:
  11.3 92.8 all-gather.2
  127.8 67.8 reduce-scatter.1

commit v2 on v1

v2 whole, which is shorter than its diff:
```python
import functools

import jax
import jax.numpy as jnp
from jax import lax
from jax.experimental import pallas as pl
from jax.experimental.pallas import tpu as pltpu
from jax.sharding import PartitionSpec as P


HD = 64
EPSILON = 1e-06
MASKED = -1e30
F32 = jnp.float32
BF16 = jnp.bfloat16
HEAD_ROWS = 80


def whole(shape):
    return pl.BlockSpec(shape, lambda *_: (0,) * len(shape))


def mirror_pairs(size):
    return [(n, size - 1 - n) for n in range(size)]


def along_z(shift, size):
    return [(n, (n + 8 * shift) % size) for n in range(size)]


def along_y(shift, size):
    return [(n, n // 8 * 8 + (n // 2 + shift) % 4 * 2 + n % 2) for n in range(size)]


Y_STEPS = (0, -1, 1, 2)
Z_STEPS = (0, -1, 1, -2, 2, -3, 3)
KV_ROWS = HEAD_ROWS + HD


def pieces_of(value):
    high = value.astype(BF16).astype(F32)
    rest = value - high
    mid = rest.astype(BF16).astype(F32)
    return high, mid, rest - mid


def pack_body(own_ref, queries_ref, keys_ref, values_ref, gates_ref, keep_ref, send_ref):
    rows = keys_ref.shape[0]
    keys_t = keys_ref[...].astype(F32).T
    values_t = values_ref[...].astype(F32).T
    queries_t = (queries_ref[...].astype(F32) * HD ** (-0.5)).T
    split = pieces_of(gates_ref[...])
    pad = jnp.zeros((HEAD_ROWS - HD - 6, rows), F32)
    blocks = []
    for g in range(2):
        gates = [piece[2 * g + r : 2 * g + r + 1] for r in range(2) for piece in split]
        heads = slice(g * HD, (g + 1) * HD)
        parts = [keys_t[heads]] + gates + [pad, values_t[heads]]
        parts.append(queries_t[2 * g * HD : 2 * (g + 1) * HD])
        blocks.append(jnp.concatenate(parts, axis=0).astype(BF16))
    even = lax.rem(own_ref[0], 2) == 0

    @pl.when(even)
    def _():
        keep_ref[...] = blocks[0]
        send_ref[...] = blocks[1]

    @pl.when(jnp.logical_not(even))
    def _():
        keep_ref[...] = blocks[1]
        send_ref[...] = blocks[0]


def pack(own, queries, keys, values, gates_t):
    rows = keys.shape[0]
    shape = (KV_ROWS + 2 * HD, rows)
    return pl.pallas_call(
        pack_body,
        grid_spec=pltpu.PrefetchScalarGridSpec(
            num_scalar_prefetch=1,
            grid=(1,),
            in_specs=[whole(x.shape) for x in (queries, keys, values, gates_t)],
            out_specs=[whole(shape), whole(shape)],
        ),
        out_shape=[jax.ShapeDtypeStruct(shape, BF16)] * 2,
        name="pack",
    )(own, queries, keys, values, gates_t)


def assemble_body(own_ref, *refs):
    kv_refs, key_ref, value_ref = refs[:9], refs[9], refs[10]
    z = own_ref[0] // 8
    rows = kv_refs[0].shape[2]
    value_ref[:, pl.ds(HD, HEAD_ROWS - HD), :] = jnp.ones(
        (value_ref.shape[0], HEAD_ROWS - HD, 2 * rows), BF16
    )

    def place_keys(slab, at, block):
        turned = block[:HEAD_ROWS].astype(F32).T
        key_ref[slab, pl.ds(at * rows, rows), :] = turned.astype(BF16)
        value_ref[slab, pl.ds(0, HD), pl.ds(at * rows, rows)] = block[HEAD_ROWS:]

    for number, shift in enumerate(Z_STEPS):
        source = lax.rem(z + shift + 8, 8)
        place_keys(source, 0, kv_refs[number][0])
        place_keys(7 - source, 1, kv_refs[number][1])
    source = lax.rem(z + 4, 8)
    place_keys(source, 0, kv_refs[7][0])
    place_keys(7 - source, 1, kv_refs[8][0])


def assemble(own, kv_parts):
    rows = kv_parts[0].shape[2]
    shapes = [(8, 2 * rows, HEAD_ROWS), (8, HEAD_ROWS, 2 * rows)]
    return pl.pallas_call(
        assemble_body,
        grid_spec=pltpu.PrefetchScalarGridSpec(
            num_scalar_prefetch=1,
            grid=(1,),
            in_specs=[whole(x.shape) for x in kv_parts],
            out_specs=[whole(shape) for shape in shapes],
        ),
        out_shape=[jax.ShapeDtypeStruct(shape, BF16) for shape in shapes],
        name="assemble",
    )(own, *kv_parts)


def attention_body(own_ref, *refs, steps):
    count_y = len(steps)
    q_refs, (key_ref, value_ref) = refs[:count_y], refs[count_y : count_y + 2]
    o_refs = refs[count_y + 2 : 2 * count_y + 2]
    query_ref, acc_ref, max_ref = refs[2 * count_y + 2 :]
    z, y, core = own_ref[0] // 8, own_ref[0] // 2 % 4, own_ref[0] % 2
    rows = q_refs[0].shape[2]
    line = lax.broadcasted_iota(jnp.int32, (HEAD_ROWS - HD, rows), 0)
    for number, ref in enumerate(q_refs):
        for slot in range(2):
            for r in range(2):
                picks = jnp.where((line >= 3 * r) & (line < 3 * r + 3), -1.0, 0.0).astype(F32)
                heads = ref[slot, r * HD : (r + 1) * HD, :].astype(F32)
                query_ref[2 * number + slot, r] = jnp.concatenate([heads, picks], axis=0).astype(
                    BF16
                )
    low = jnp.minimum(z, 7 - z)
    offset = 2 * y + core

    def run_half(high, carry):
        count = jnp.where(high == 1, 7 - low, low)
        slot = jnp.where(count == z, 0, 1)
        acc_ref[...] = jnp.zeros_like(acc_ref)
        max_ref[...] = jnp.full_like(max_ref, MASKED)

        def one_slab(slab, masked):
            keys = key_ref[slab]
            values = value_ref[slab]
            for number, shift in enumerate(steps):
                for r in range(2):
                    scores = jnp.dot(
                        keys, query_ref[2 * number + slot, r], preferred_element_type=F32
                    )
                    if masked:
                        line = lax.broadcasted_iota(jnp.int32, scores.shape, 0)
                        key_at = line + jnp.where(
                            line < rows, offset * rows, (7 - offset) * rows - rows
                        )
                        own = 2 * lax.rem(y + shift + 4, 4) + core
                        own = jnp.where(slot == 0, own, 7 - own)
                        query_at = own * rows + lax.broadcasted_iota(jnp.int32, scores.shape, 1)
                        scores = jnp.where(key_at <= query_at, scores, MASKED)
                    old = max_ref[number, r]
                    new = jnp.maximum(old, jnp.max(scores, axis=0, keepdims=True))
                    weights = jnp.exp(scores - new[0:1]).astype(BF16)
                    max_ref[number, r] = new
                    acc_ref[number, r] = acc_ref[number, r] * jnp.exp(old - new)[0:1] + jnp.dot(
                        values, weights, preferred_element_type=F32
                    )

        def open_slab(slab, carry):
            one_slab(slab, False)
            return carry

        lax.fori_loop(0, count, open_slab, 0)
        one_slab(count, True)
        blank = jnp.zeros((HEAD_ROWS - HD - 3, rows), F32)
        for number in range(count_y):
            for r in range(2):
                total = acc_ref[number, r]
                weight = total[HD : HD + 1]
                stats = pieces_of(max_ref[number, r][0:1] + jnp.log(weight))
                o_refs[number][slot, pl.ds(r * HEAD_ROWS, HEAD_ROWS), :] = jnp.concatenate(
                    [total[:HD] / weight, *stats, blank], axis=0
                ).astype(BF16)
        return carry

    lax.fori_loop(0, 2, run_half, 0)


def attention(own, steps, query_parts, keys, values):
    rows = query_parts[0].shape[2]
    count_y = len(steps)
    shape = (2, 2 * HEAD_ROWS, rows)
    operands = (*query_parts, keys, values)
    return pl.pallas_call(
        functools.partial(attention_body, steps=steps),
        grid_spec=pltpu.PrefetchScalarGridSpec(
            num_scalar_prefetch=1,
            grid=(1,),
            in_specs=[whole(x.shape) for x in operands],
            out_specs=[whole(shape)] * count_y,
            scratch_shapes=[
                pltpu.VMEM((2 * count_y, 2, HEAD_ROWS, rows), BF16),
                pltpu.VMEM((count_y, 2, HEAD_ROWS, rows), F32),
                pltpu.VMEM((count_y, 2, 8, rows), F32),
            ],
        ),
        out_shape=[jax.ShapeDtypeStruct(shape, BF16)] * count_y,
        cost_estimate=pl.CostEstimate(
            flops=10_000_000_000, transcendentals=5_000_000, bytes_accessed=2_000_000
        ),
        name="attention",
    )(own, *operands)


def merge_body(a, b, c, d, keep_ref, send_ref):
    for slot, target in enumerate((keep_ref, send_ref)):
        heads = []
        for r in range(2):
            block = pl.ds(r * HEAD_ROWS, HEAD_ROWS)
            parts = [ref[slot, block, :].astype(F32) for ref in (a, b, c, d)]
            logs = [x[HD : HD + 1] + x[HD + 1 : HD + 2] + x[HD + 2 : HD + 3] for x in parts]
            highest = functools.reduce(jnp.maximum, logs)
            shares = [jnp.exp(x - highest) for x in logs]
            total = functools.reduce(jnp.add, shares)
            mixed = functools.reduce(
                jnp.add, [x[:HD] * share for x, share in zip(parts, shares)]
            )
            heads.append(mixed / total)
        target[...] = jnp.concatenate(heads, axis=0).T.astype(BF16)


def merge(parts):
    rows = parts[0].shape[2]
    return pl.pallas_call(
        merge_body,
        out_shape=[jax.ShapeDtypeStruct((rows, 2 * HD), BF16)] * 2,
        name="merge",
    )(*parts)


def project_body(own_ref, tp_ref, keep_ref, back_ref, w_ref, *out_refs):
    tp = len(out_refs)
    even = lax.rem(own_ref[0], 2) == 0
    rows = out_refs[0].shape[0]
    for shift, ref in enumerate(out_refs):
        at = pl.multiple_of(lax.rem(tp_ref[0] + shift, tp) * rows, rows)
        kept, back = keep_ref[pl.ds(at, rows), :], back_ref[pl.ds(at, rows), :]
        attended = jnp.concatenate(
            [jnp.where(even, kept, back), jnp.where(even, back, kept)], axis=1
        )
        ref[...] = jnp.dot(attended, w_ref[...], preferred_element_type=F32).astype(BF16)


def project(own, tp_index, keep, back, out_weight, tp):
    shape = (keep.shape[0] // tp, out_weight.shape[1])
    return pl.pallas_call(
        project_body,
        grid_spec=pltpu.PrefetchScalarGridSpec(
            num_scalar_prefetch=2,
            grid=(1,),
            in_specs=[whole(x.shape) for x in (keep, back, out_weight)],
            out_specs=[whole(shape)] * tp,
        ),
        out_shape=[jax.ShapeDtypeStruct(shape, BF16)] * tp,
        name="project",
    )(own, tp_index, keep, back, out_weight)


CHUNKS = 1


def slot_number(named, rank, expert_at, cap, chunk, axis):
    part = cap // CHUNKS
    base = (expert_at * part).astype(F32)
    number = base + rank
    for cut in range(1, CHUNKS):
        number = number + jnp.where(rank >= cut * part, float(chunk - part), 0.0)
    return jnp.sum(named * number, axis=axis, keepdims=True).astype(jnp.int32)


def dispatch_body(
    index_ref, rows_ref, part_ref, gain_ref, experts_t_ref, *send_refs, cap
):
    tokens = rows_ref.shape[0]
    chunk = send_refs[0].shape[0]
    slots = chunk * len(send_refs)
    count = slots // cap
    rows = rows_ref[...].astype(F32)
    scale = lax.rsqrt(jnp.mean(rows * rows, axis=1, keepdims=True) + EPSILON)
    normed = (part_ref[...].astype(F32) * scale * gain_ref[...]).astype(BF16)
    expert_at = lax.broadcasted_iota(jnp.int32, (count, tokens), 0)
    first = (expert_at == experts_t_ref[0:1, :]).astype(F32)
    second = (expert_at == experts_t_ref[1:2, :]).astype(F32)
    earlier = (
        lax.broadcasted_iota(jnp.int32, (tokens, tokens), 0)
        < lax.broadcasted_iota(jnp.int32, (tokens, tokens), 1)
    ).astype(BF16)
    before_first = jnp.dot(first.astype(BF16), earlier, preferred_element_type=F32)
    before_second = jnp.dot(second.astype(BF16), earlier, preferred_element_type=F32) + jnp.sum(
        first, axis=1, keepdims=True
    )
    to_first = slot_number(first, before_first, expert_at, cap, chunk, 0)
    to_second = slot_number(second, before_second, expert_at, cap, chunk, 0)
    slot_at = lax.broadcasted_iota(jnp.int32, (slots, tokens), 0)
    chosen = ((slot_at == to_first) | (slot_at == to_second)).astype(F32).astype(BF16)
    for number, ref in enumerate(send_refs):
        picks = chosen[number * chunk : (number + 1) * chunk]
        ref[...] = jnp.dot(picks, normed, preferred_element_type=F32).astype(BF16)


def dispatch(tp_index, moe_rows, norm_gain, experts, count, tp):
    tokens, width = moe_rows.shape
    cap = 4 * tokens // count
    part = width // tp
    return pl.pallas_call(
        functools.partial(dispatch_body, cap=cap),
        grid_spec=pltpu.PrefetchScalarGridSpec(
            num_scalar_prefetch=1,
            grid=(1,),
            in_specs=[
                whole(moe_rows.shape),
                pl.BlockSpec((tokens, part), lambda s, own: (0, own[0])),
                pl.BlockSpec((1, part), lambda s, own: (0, own[0])),
                whole((2, tokens)),
            ],
            out_specs=[whole((count * cap // CHUNKS, part))] * CHUNKS,
        ),
        out_shape=[jax.ShapeDtypeStruct((count * cap // CHUNKS, part), BF16)] * CHUNKS,
        name="dispatch",
    )(tp_index, moe_rows, moe_rows, norm_gain.reshape(1, -1), experts.T)


def way_back_body(experts_ref, slot_ref, *, count, cap):
    tokens = experts_ref.shape[0]
    expert_at = lax.broadcasted_iota(jnp.int32, (tokens, count), 1)
    first = (expert_at == experts_ref[:, 0:1]).astype(F32)
    second = (expert_at == experts_ref[:, 1:2]).astype(F32)
    earlier = (
        lax.broadcasted_iota(jnp.int32, (tokens, tokens), 1)
        < lax.broadcasted_iota(jnp.int32, (tokens, tokens), 0)
    ).astype(BF16)
    before_first = jnp.dot(earlier, first.astype(BF16), preferred_element_type=F32)
    before_second = jnp.dot(earlier, second.astype(BF16), preferred_element_type=F32) + jnp.sum(
        first, axis=0, keepdims=True
    )
    chunk = count * cap // CHUNKS
    slot_ref[:, 0:1] = slot_number(first, before_first, expert_at, cap, chunk, 1)
    slot_ref[:, 1:2] = slot_number(second, before_second, expert_at, cap, chunk, 1)


def way_back(experts, count):
    cap = 4 * experts.shape[0] // count
    return pl.pallas_call(
        functools.partial(way_back_body, count=count, cap=cap),
        out_shape=jax.ShapeDtypeStruct(experts.shape, jnp.int32),
        name="way_back",
    )(experts)


def pick_parts(index_ref, refs, steps):
    own, previous, following, far_low, far_high = refs
    low = pl.program_id(0) < steps // 2
    tp = index_ref[0]
    return (
        (tp, own[...]),
        (lax.rem(tp + 3, 4), previous[...]),
        (lax.rem(tp + 1, 4), following[...]),
        (lax.rem(tp + 2, 4), jnp.where(low, far_low[...], far_high[...])),
    )


def part_specs(tall, wide, steps):
    block = tall // steps
    half = steps // 2
    straight = pl.BlockSpec((block, wide), lambda s, own: (s, 0))
    return [
        straight,
        straight,
        straight,
        pl.BlockSpec((block, wide), lambda s, own: (jnp.minimum(s, half - 1), 0)),
        pl.BlockSpec((block, wide), lambda s, own: (jnp.maximum(s - half, 0), 0)),
    ]


def up_body(index_ref, a, b, c, d, e, gate_ref, up_ref, out_ref, *, steps):
    gate = up = None
    for number, rows in pick_parts(index_ref, (a, b, c, d, e), steps):
        to_gate = jnp.dot(rows, gate_ref[number], preferred_element_type=F32)
        to_up = jnp.dot(rows, up_ref[number], preferred_element_type=F32)
        gate = to_gate if gate is None else gate + to_gate
        up = to_up if up is None else up + to_up
    out_ref[...] = (gate / (1.0 + jnp.exp(-gate)) * up).astype(BF16)


def up_projections(tp_index, parts, w_gate, w_up, tp):
    tall, wide = parts[0].shape
    steps = 4
    hidden = w_gate.shape[1]
    return pl.pallas_call(
        functools.partial(up_body, steps=steps),
        grid_spec=pltpu.PrefetchScalarGridSpec(
            num_scalar_prefetch=1,
            grid=(steps,),
            in_specs=part_specs(tall, wide, steps)
            + [whole((tp, wide, hidden)), whole((tp, wide, hidden))],
            out_specs=pl.BlockSpec((tall // steps, hidden), lambda s, own: (s, 0)),
        ),
        out_shape=jax.ShapeDtypeStruct((tall, hidden), BF16),
        cost_estimate=pl.CostEstimate(
            flops=2_200_000_000, transcendentals=262_144, bytes_accessed=6_800_000
        ),
        name="up_projections",
    )(tp_index, *parts, w_gate.reshape(tp, wide, hidden), w_up.reshape(tp, wide, hidden))


def down_body(index_ref, a, b, c, d, e, own_w, previous_w, following_w, far_w, out_ref, *, steps):
    low = pl.program_id(0) < steps // 2
    far_rows = jnp.where(low, d[...], e[...])
    total = jnp.dot(a[...], own_w[...], preferred_element_type=F32)
    total = total + jnp.dot(b[...], previous_w[...], preferred_element_type=F32)
    total = total + jnp.dot(c[...], following_w[...], preferred_element_type=F32)
    total = total + jnp.dot(far_rows, far_w[...], preferred_element_type=F32)
    out_ref[...] = total.astype(BF16)


def down_projection(tp_index, parts, w_down, moved):
    tall, wide = parts[0].shape
    steps = 4
    columns = moved[0].shape[1]
    return pl.pallas_call(
        functools.partial(down_body, steps=steps),
        grid_spec=pltpu.PrefetchScalarGridSpec(
            num_scalar_prefetch=1,
            grid=(steps,),
            in_specs=part_specs(tall, wide, steps)
            + [pl.BlockSpec((wide, columns), lambda s, own: (0, own[0]))]
            + [whole((wide, columns))] * 3,
            out_specs=pl.BlockSpec((tall // steps, columns), lambda s, own: (s, 0)),
        ),
        out_shape=jax.ShapeDtypeStruct((tall, columns), BF16),
        cost_estimate=pl.CostEstimate(
            flops=1_100_000_000, transcendentals=0, bytes_accessed=4_200_000
        ),
        name="down_projection",
    )(tp_index, *parts, w_down, *moved)


def cut_body(index_ref, a, b, c, to_a, to_b, to_c):
    to_a[...] = a[...]
    to_b[...] = b[...]
    to_c[...] = c[...]


def cut_columns(tp_index, w_down, tp):
    wide, columns = w_down.shape[0], w_down.shape[1] // tp

    def block(shift):
        return pl.BlockSpec((wide, columns), lambda s, own: (0, lax.rem(own[0] + shift, tp)))

    return pl.pallas_call(
        cut_body,
        grid_spec=pltpu.PrefetchScalarGridSpec(
            num_scalar_prefetch=1,
            grid=(1,),
            in_specs=[block(1), block(tp - 1), block(2)],
            out_specs=[whole((wide, columns))] * 3,
        ),
        out_shape=[jax.ShapeDtypeStruct((wide, columns), BF16)] * 3,
        name="cut_columns",
    )(tp_index, w_down, w_down, w_down)


def combine_body(slot_ref, weight_ref, *refs):
    row_refs, out_ref = refs[:-1], refs[-1]
    chunk = row_refs[0].shape[0]
    tokens = slot_ref.shape[0]
    total = None
    for k in range(2):
        picked = None
        for number, ref in enumerate(row_refs):
            slot_at = number * chunk + lax.broadcasted_iota(jnp.int32, (tokens, chunk), 1)
            chosen = (slot_at == slot_ref[:, k : k + 1]).astype(F32).astype(BF16)
            found = jnp.dot(chosen, ref[...], preferred_element_type=F32)
            picked = found if picked is None else picked + found
        term = picked * weight_ref[:, k : k + 1]
        total = term if total is None else total + term
    out_ref[...] = total.astype(BF16)


def combine(slots, expert_weights, rows):
    return pl.pallas_call(
        combine_body,
        out_shape=jax.ShapeDtypeStruct((slots.shape[0], rows[0].shape[1]), BF16),
        name="combine",
    )(slots, expert_weights, *rows)


def per_device(
    queries,
    keys,
    values,
    log_gates,
    out_weight,
    moe_rows,
    norm_gain,
    experts,
    expert_weights,
    w_gate,
    w_up,
    w_down,
):
    size = lax.axis_size("ep")
    tp = lax.axis_size("tp")
    own = lax.axis_index("ep").astype(jnp.int32).reshape(1)
    tp_index = lax.axis_index("tp").astype(jnp.int32).reshape(1)
    up_ring = [(n, (n + 1) % tp) for n in range(tp)]
    down_ring = [(n, (n - 1) % tp) for n in range(tp)]

    def over_ep(x):
        wide = x.shape[1]
        moved = lax.all_to_all(
            x.reshape(size, -1, wide), "ep", split_axis=0, concat_axis=0, tiled=True
        )
        return moved.reshape(-1, wide)

    def near(x):
        return lax.ppermute(x, "tp", up_ring), lax.ppermute(x, "tp", down_ring)

    def far(pair):
        half = pair[0].shape[0] // 2
        low, high = pair[0][:half], pair[1][half:]
        return lax.ppermute(low, "tp", up_ring), lax.ppermute(high, "tp", down_ring)

    keep, send = pack(own, queries, keys, values, log_gates.T)
    mirrored = lax.ppermute(send, "ep", mirror_pairs(size))
    outgoing = dispatch(tp_index, moe_rows, norm_gain, experts, size, tp)
    arrived = []
    for rows in outgoing:
        arrived.append(over_ep(rows))
    both = jnp.stack([keep, mirrored])
    own_keys, own_queries = both[:, :KV_ROWS], both[:, KV_ROWS:]
    query_parts = [own_queries] + [
        lax.ppermute(own_queries, "ep", along_y(-step, size)) for step in Y_STEPS[1:]
    ]
    below2, above2, below, above = [
        lax.ppermute(own_keys, "ep", along_z(shift, size)) for shift in (2, -2, 1, -1)
    ]
    below3 = lax.ppermute(below2, "ep", along_z(1, size))
    above3 = lax.ppermute(above2, "ep", along_z(-1, size))
    far_low = lax.ppermute(below2[:1], "ep", along_z(2, size))
    far_high = lax.ppermute(above2[1:], "ep", along_z(-2, size))
    kv_parts = [own_keys, below, above, below2, above2, below3, above3, far_low, far_high]
    slab_keys, slab_values = assemble(own, kv_parts)
    far_ring = [(n, (n + 2) % tp) for n in range(tp)]
    cuts = cut_columns(tp_index, w_down[0], tp)
    moved = [
        lax.ppermute(cut, "tp", ring) for cut, ring in zip(cuts, (up_ring, down_ring, far_ring))
    ]
    slots = way_back(experts, size)
    x_near = [near(rows) for rows in arrived]
    x_far = [far(pair) for pair in x_near]
    partial = {}
    for picks in ((3, 1), (2, 0)):
        done = attention(
            own,
            tuple(Y_STEPS[n] for n in picks),
            [query_parts[n] for n in picks],
            slab_keys,
            slab_values,
        )
        for n, part in zip(picks, done):
            if n:
                part = lax.ppermute(part, "ep", along_y(Y_STEPS[n], size))
            partial[n] = part
    h_near, h_far, hidden = [], [], []
    for number in range(CHUNKS):
        hidden.append(
            up_projections(
                tp_index,
                (arrived[number],) + x_near[number] + x_far[number],
                w_gate[0],
                w_up[0],
                tp,
            )
        )
        h_near.append(near(hidden[number]))
        h_far.append(far(h_near[number]))
    kept, sent = merge([partial[n] for n in range(4)])
    back = lax.ppermute(sent, "ep", mirror_pairs(size))
    products = project(own, tp_index, kept, back, out_weight, tp)
    others = [
        lax.ppermute(product, "tp", ring)
        for product, ring in zip(products[1:], (up_ring, far_ring, down_ring))
    ]
    mixed = sum(part.astype(F32) for part in [products[0]] + others).astype(BF16)
    returned = []
    for number in range(CHUNKS):
        result = down_projection(
            tp_index, (hidden[number],) + h_near[number] + h_far[number], w_down[0], moved
        )
        returned.append(over_ep(result))
    moe_out = combine(slots, expert_weights, returned)
    return (mixed, moe_out)


def solution(mesh):
    placed = (
        P("ep", "tp"),
        P("ep", "tp"),
        P("ep", "tp"),
        P("ep", "tp"),
        P("tp", None),
        P("ep", None),
        P(),
        P("ep", None),
        P("ep", None),
        P("ep", None, "tp"),
        P("ep", None, "tp"),
        P("ep", "tp", None),
    )
    return jax.shard_map(
        per_device,
        mesh=mesh,
        in_specs=placed,
        out_specs=(P(("ep", "tp"), None), P("ep", "tp")),
        check_vma=False,
    )
```

time: 228 us -> 240 us (1.053)
  Pallas kernels: 25 us -> 65.3 us
  waiting for transfers between devices: 71 us -> 57.4 us
  between operations: 14.2 us -> 0.98 us
  blocking collectives: 47 us -> 41.3 us
    pallas_call x2 -> x8, Pallas kernels: 7.78 us -> 48.1 us  [the longest x2 34.5 us: attention(): pl.pallas_call(functools.partial(attention_body, steps=steps), grid_spec=...]
    all_to_all x2 -> x1, starting transfers between devices: 52.3 us -> 12.3 us  [over_ep(): lax.all_to_all(x.reshape(size, -1, wide), 'ep', split_axis=0, concat_axis...]
    ppermute x8 -> x30, starting transfers between devices: 11.1 us -> 50.1 us  [the longest x4 8.08 us: per_device(): lax.ppermute(own_keys, 'ep', along_z(shift, size))]
    all_to_all x2 -> x1, waiting for transfers between devices: 29.7 us -> 0.01 us  [over_ep(): lax.all_to_all(x.reshape(size, -1, wide), 'ep', split_axis=0, concat_axis...]
    ppermute x8 -> x30, waiting for transfers between devices: 41.2 us -> 57.4 us  [the longest x4 22.1 us: near(): return (lax.ppermute(x, 'tp', up_ring), lax.ppermute(x, 'tp', down_ring))]
    all_to_all x1, blocking collectives: 47 us -> 41.3 us  [over_ep(): lax.all_to_all(x.reshape(size, -1, wide), 'ep', split_axis=0, concat_axis...]
    unnamed x29 -> x74, local copies, waits for them, and re-layouts: 5.46 us -> 8.55 us
  transfers between devices with their start and end apart: 12 -> 31, of which waited for: 7 -> 12; matrix products, arithmetic and copies ran while one was open for 2% -> 1% of each run, Pallas kernels for 10% -> 22%
where the time goes in v2:
time: 240 us; the launch traced here: 238 us
  Pallas kernels  65.3 us (27%)
  starting transfers between devices  62.4 us (26%)
  waiting for transfers between devices  57.4 us (24%)
  blocking collectives  41.3 us (17%)
  local copies, waits for them, and re-layouts  8.66 us (4%)
    all_to_all x1, blocking collectives, over_ep(): lax.all_to_all(x.reshape(size, -1, wide), 'ep', split_axis=0, concat_axis...  41.3 us
    pallas_call x2, Pallas kernels, attention(): pl.pallas_call(functools.partial(attention_body, steps=steps), grid_spec=...  34.5 us
    ppermute x4, waiting for transfers between devices, near(): return (lax.ppermute(x, 'tp', up_ring), lax.ppermute(x, 'tp', down_ring))  22.1 us
    all_to_all x1, starting transfers between devices, over_ep(): lax.all_to_all(x.reshape(size, -1, wide), 'ep', split_axis=0, concat_axis...  12.3 us
    ppermute x2, waiting for transfers between devices, far(): lax.ppermute(low, 'tp', up_ring)  9.88 us
    unnamed x74, local copies, waits for them, and re-layouts  8.55 us
    ppermute x4, starting transfers between devices, per_device(): lax.ppermute(own_keys, 'ep', along_z(shift, size))  8.08 us
    ppermute x3, waiting for transfers between devices, per_device(): lax.ppermute(product, 'tp', ring)  8.06 us
  transfers between devices with their start and end apart: 31, of which 12 were waited for; matrix products, arithmetic and copies ran while one was open for 1% of the time, Pallas kernels for 22%

profile of v2, /device:TPU:1, one launch (start us, length us, event | category | flops | bytes accessed | tf_op | source)
XLA Modules:
  0.0 237.8 jit_solution(17293278434761049074)
XLA Ops:
  0.6 3.1 %dispatch.1 = bf16[1024,512]{1,0:T(8,128)(2,1)} custom-call(s32[1]{0:T(128)} %bitcast.1.tp_ref.index_ref, bf16[256,2048]{1,0:T(8,128)(2,1)} %part_ref.1, bf16[256,2048]{1,0:T(8,128)(2,1)} %part_ref.1, f32[1,2048]{1,0:T(1,128)} %bitcast.28, s32[2,256]{1,0:T(2,128)} %bitcast.29), custom_call_target="tpu_custom_call" | custom-call | tf_op jit(solution)/shard_map/dispatch/pallas_call | solution.py:324
  3.7 41.3 %all_to_all.10 = bf16[64,16,512]{2,1,0:T(8,128)(2,1)S(1)} all-to-all(bf16[64,16,512]{2,1,0:T(8,128)(2,1)} %bitcast.19), channel_id=1, replica_groups=mesh['ep'=64,'tp'=4] {'ep'}, dimensions={0} | all-to-all | bytes 2097152 | tf_op jit(solution)/shard_map/all_to_all | solution.py:530
  47.7 22.1 %collective-permute-done.19.b = bf16[1024,512]{1,0:T(8,128)(2,1)S(1)} collective-permute-done((bf16[1024,512]{1,0:T(8,128)(2,1)S(1)}, bf16[1024,512]{1,0:T(8,128)(2,1)S(1)}, u32[]{:S(2)}, u32[]{:S(2)}) %collective-permute-start.19) | collective-permute-done | bytes 1048608 | tf_op jit(solution)/shard_map/ppermute | solution.py:536
  70.0 2.7 %collective-permute-start.22 = (bf16[512,512]{1,0:T(8,128)(2,1)S(1)}, bf16[512,512]{1,0:T(8,128)(2,1)S(1)}, u32[]{:S(2)}, u32[]{:S(2)}) collective-permute-start(bf16[512,512]{1,0:T(8,128)(2,1)S(1)} %slice.35), channel_id=1, source_target_pairs={{0,3},{1,0},{2,1},{3,2},{4,7},{5,4},{6,5},{7,6},{8,11},{9,8},{10,9... | collective-permute-start | bytes 1572872 | tf_op jit(solution)/shard_map/ppermute | solution.py:541
  72.7 9.9 %collective-permute-done.21.d = bf16[512,512]{1,0:T(8,128)(2,1)S(1)} collective-permute-done((bf16[512,512]{1,0:T(8,128)(2,1)S(1)}, bf16[512,512]{1,0:T(8,128)(2,1)S(1)}, u32[]{:S(2)}, u32[]{:S(2)}) %collective-permute-start.21) | collective-permute-done | bytes 524320 | tf_op jit(solution)/shard_map/ppermute | solution.py:541
  83.6 6.3 %up_projections.1.a = bf16[1024,256]{1,0:T(8,128)(2,1)} custom-call(s32[1]{0:T(128)} %bitcast.1.tp_ref.index_ref, bf16[1024,512]{1,0:T(8,128)(2,1)} %bitcast.23, bf16[1024,512]{1,0:T(8,128)(2,1)} %copy-done.14, bf16[1024,512]{1,0:T(8,128)(2,1)} %copy-done.15, bf16[512,512]{1,0:T(8,128)(2,1)} %copy-done.29, bf16[512,512]{1,0:T(8,128)(2,1)} %copy-done.30, ...), custom_call_target="tpu_custom_call" | custom-call | flops 2200000000 | bytes 6800000 | tf_op jit(solution)/shard_map/up_projections/pallas_call | solution.py:408
  89.9 2.7 %collective-permute-start.24 = (bf16[1024,256]{1,0:T(8,128)(2,1)}, bf16[1024,256]{1,0:T(8,128)(2,1)S(1)}, u32[]{:S(2)}, u32[]{:S(2)}) collective-permute-start(bf16[1024,256]{1,0:T(8,128)(2,1)} %up_projections.1.a), channel_id=1, source_target_pairs={{0,3},{1,0},{2,1},{3,2},{4,7},{5,4},{6,5},{7,6},{8,11},{9,8},{10,9... | collective-permute-start | bytes 1572872 | tf_op jit(solution)/shard_map/ppermute | solution.py:536
  96.5 5.9 %collective-permute-start = (bf16[272,256]{1,0:T(8,128)(2,1)}, bf16[272,256]{1,0:T(8,128)(2,1)S(1)}, u32[]{:S(2)}, u32[]{:S(2)}) collective-permute-start(bf16[272,256]{1,0:T(8,128)(2,1)} %get-tuple-element.20), channel_id=1, source_target_pairs={{0,252},{4,248},{8,244},{12,240},{16,236},{20,232},{24,228},{28,22... | collective-permute-start | bytes 417800 | tf_op jit(solution)/shard_map/ppermute | solution.py:544
  102.4 2.9 %collective-permute-start.28 = (bf16[256,512]{1,0:T(8,128)(2,1)S(1)}, bf16[256,512]{1,0:T(8,128)(2,1)S(1)}, u32[]{:S(2)}, u32[]{:S(2)}) collective-permute-start(bf16[256,512]{1,0:T(8,128)(2,1)S(1)} %copy-done.32), channel_id=1, source_target_pairs={{0,3},{1,0},{2,1},{3,2},{4,7},{5,4},{6,5},{7,6},{8,11},{9,8},{10,9... | collective-permute-start | bytes 786440 | tf_op jit(solution)/shard_map/ppermute | solution.py:566
  105.3 2.4 %collective-permute-done = bf16[272,256]{1,0:T(8,128)(2,1)S(1)} collective-permute-done((bf16[272,256]{1,0:T(8,128)(2,1)}, bf16[272,256]{1,0:T(8,128)(2,1)S(1)}, u32[]{:S(2)}, u32[]{:S(2)}) %collective-permute-start) | collective-permute-done | bytes 139296 | tf_op jit(solution)/shard_map/ppermute | solution.py:544
  110.1 3.9 %collective-permute-start.5 = (bf16[2,144,256]{2,1,0:T(8,128)(2,1)S(1)}, bf16[2,144,256]{2,1,0:T(8,128)(2,1)S(1)}, u32[]{:S(2)}, u32[]{:S(2)}) collective-permute-start(bf16[2,144,256]{2,1,0:T(8,128)(2,1)S(1)} %pad_maximum_fusion.refs_0_), channel_id=1, source_target_pairs={{0,192},{4,196},{8,200},{12,204},{16,208},{20,212},{24,216},{28,22... | collective-permute-start | bytes 442376 | tf_op jit(solution)/shard_map/ppermute | solution.py:555
  114.1 2.7 %collective-permute-start.3 = (bf16[2,144,256]{2,1,0:T(8,128)(2,1)S(1)}, bf16[2,144,256]{2,1,0:T(8,128)(2,1)S(1)}, u32[]{:S(2)}, u32[]{:S(2)}) collective-permute-start(bf16[2,144,256]{2,1,0:T(8,128)(2,1)S(1)} %pad_maximum_fusion.refs_0_), channel_id=1, source_target_pairs={{0,224},{4,228},{8,232},{12,236},{16,240},{20,244},{24,248},{28,25... | collective-permute-start | bytes 442376 | tf_op jit(solution)/shard_map/ppermute | solution.py:555
  122.8 3.1 %collective-permute-start.9 = (bf16[1,144,256]{2,1,0:T(8,128)(2,1)S(1)}, bf16[1,144,256]{2,1,0:T(8,128)(2,1)S(1)}, u32[]{:S(2)}, u32[]{:S(2)}) collective-permute-start(bf16[1,144,256]{2,1,0:T(8,128)(2,1)S(1)} %slice.33), channel_id=1, source_target_pairs={{0,192},{4,196},{8,200},{12,204},{16,208},{20,212},{24,216},{28,22... | collective-permute-start | bytes 221192 | tf_op jit(solution)/shard_map/ppermute | solution.py:560
  125.9 2.0 collective-permute-done.8.refs_7_
  128.2 2.8 %collective-permute-start.7 = (bf16[2,144,256]{2,1,0:T(8,128)(2,1)S(1)}, bf16[2,144,256]{2,1,0:T(8,128)(2,1)S(1)}, u32[]{:S(2)}, u32[]{:S(2)}) collective-permute-start(bf16[2,144,256]{2,1,0:T(8,128)(2,1)S(1)} %collective-permute-done.5.refs_4_), channel_id=1, source_target_pairs={{0,224},{4,228},{8,232},{12,236},{16,240},{20,244},{24,248},{28,25... | collective-permute-start | bytes 442376 | tf_op jit(solution)/shard_map/ppermute | solution.py:558
  131.1 3.0 %collective-permute-done.6.refs_5_ = bf16[2,144,256]{2,1,0:T(8,128)(2,1)S(1)} collective-permute-done((bf16[2,144,256]{2,1,0:T(8,128)(2,1)S(1)}, bf16[2,144,256]{2,1,0:T(8,128)(2,1)S(1)}, u32[]{:S(2)}, u32[]{:S(2)}) %collective-permute-start.6) | collective-permute-done | bytes 147488 | tf_op jit(solution)/shard_map/ppermute | solution.py:557
  137.7 2.9 %assemble.1 = (bf16[8,512,80]{2,1,0:T(8,128)(2,1)}, bf16[8,80,512]{2,1,0:T(8,128)(2,1)}) custom-call(s32[1]{0:T(128)} %bitcast.own_ref, bf16[2,144,256]{2,1,0:T(8,128)(2,1)} %copy-done.4, bf16[2,144,256]{2,1,0:T(8,128)(2,1)} %copy-done.19, bf16[2,144,256]{2,1,0:T(8,128)(2,1)} %copy-done.20, bf16[2,144,256]{2,1,0:T(8,128)(2,1)} %copy-done.6, ...), custom_call_target="tpu_custom_call" | custom-call | tf_op jit(solution)/shard_map/assemble/pallas_call | solution.py:115
  142.9 5.0 %down_projection.1 = bf16[1024,512]{1,0:T(8,128)(2,1)} custom-call(s32[1]{0:T(128)} %bitcast.1.tp_ref.index_ref, bf16[1024,256]{1,0:T(8,128)(2,1)} %up_projections.1.a, bf16[1024,256]{1,0:T(8,128)(2,1)} %copy-done.1, bf16[1024,256]{1,0:T(8,128)(2,1)} %copy-done.2, bf16[512,256]{1,0:T(8,128)(2,1)} %copy-done.11, bf16[512,256]{1,0:T(8,128)(2,1)} %copy-done.12, ...), custom_call_target="tpu_custom_call" | custom-call | flops 1100000000 | bytes 4200000 | tf_op jit(solution)/shard_map/down_projection/pallas_call | solution.py:439
  147.9 12.3 %all-to-all-start.1 = ((bf16[64,16,512]{2,1,0:T(8,128)(2,1)}), bf16[64,16,512]{2,1,0:T(8,128)(2,1)S(1)}, u32[]{:S(2)}, u32[]{:S(2)}) async-start(bf16[64,16,512]{2,1,0:T(8,128)(2,1)} %bitcast.18), calls=%async_computation.1 | async-start | bytes 2097152 | tf_op jit(solution)/shard_map/all_to_all | solution.py:530
  160.9 17.2 %attention.3 = (bf16[2,160,256]{2,1,0:T(8,128)(2,1)}, bf16[2,160,256]{2,1,0:T(8,128)(2,1)}) custom-call(s32[1]{0:T(128)} %bitcast.own_ref, bf16[2,128,256]{2,1,0:T(8,128)(2,1)} %copy-done.33, bf16[2,128,256]{2,1,0:T(8,128)(2,1)} %copy-done.34, bf16[8,512,80]{2,1,0:T(8,128)(2,1)} %get-tuple-element.21.refs_2_, bf16[8,80,512]{2,1,0:T(8,128)(2,1)} %get-tuple-element.22.refs_3_), custom_call_target="tpu_custom_call" | custom-call | flops 10000000000 | bytes 2000000 | tf_op jit(solution)/shard_map/attention/pallas_call | solution.py:203
  178.1 2.6 %collective-permute-start.12 = (bf16[2,160,256]{2,1,0:T(8,128)(2,1)}, bf16[2,160,256]{2,1,0:T(8,128)(2,1)S(1)}, u32[]{:S(2)}, u32[]{:S(2)}) collective-permute-start(bf16[2,160,256]{2,1,0:T(8,128)(2,1)} %get-tuple-element.24), channel_id=1, source_target_pairs={{0,24},{4,28},{8,0},{12,4},{16,8},{20,12},{24,16},{28,20},{32,56},... | collective-permute-start | bytes 491528 | tf_op jit(solution)/shard_map/ppermute | solution.py:582
  181.9 17.2 %attention.2 = (bf16[2,160,256]{2,1,0:T(8,128)(2,1)}, bf16[2,160,256]{2,1,0:T(8,128)(2,1)}) custom-call(s32[1]{0:T(128)} %bitcast.own_ref, bf16[2,128,256]{2,1,0:T(8,128)(2,1)} %copy-done.35, bf16[2,128,256]{2,1,0:T(8,128)(2,1)} %copy-done.23, bf16[8,512,80]{2,1,0:T(8,128)(2,1)} %get-tuple-element.21.refs_2_, bf16[8,80,512]{2,1,0:T(8,128)(2,1)} %get-tuple-element.22.refs_3_), custom_call_target="tpu_custom_call" | custom-call | flops 10000000000 | bytes 2000000 | tf_op jit(solution)/shard_map/attention/pallas_call | solution.py:203
  199.7 5.6 %collective-permute-done.13.c = bf16[2,160,256]{2,1,0:T(8,128)(2,1)S(1)} collective-permute-done((bf16[2,160,256]{2,1,0:T(8,128)(2,1)}, bf16[2,160,256]{2,1,0:T(8,128)(2,1)S(1)}, u32[]{:S(2)}, u32[]{:S(2)}) %collective-permute-start.13) | collective-permute-done | bytes 163872 | tf_op jit(solution)/shard_map/ppermute | solution.py:582
  206.0 2.0 merge.1
  208.1 4.1 %collective-permute-start.15 = (bf16[256,128]{1,0:T(8,128)(2,1)}, bf16[256,128]{1,0:T(8,128)(2,1)S(1)}, u32[]{:S(2)}, u32[]{:S(2)}) collective-permute-start(bf16[256,128]{1,0:T(8,128)(2,1)} %get-tuple-element.28), channel_id=1, source_target_pairs={{0,252},{4,248},{8,244},{12,240},{16,236},{20,232},{24,228},{28,22... | collective-permute-start | bytes 196616 | tf_op jit(solution)/shard_map/ppermute | solution.py:598
  212.2 3.1 %collective-permute-done.15.back_ref = bf16[256,128]{1,0:T(8,128)(2,1)S(1)} collective-permute-done((bf16[256,128]{1,0:T(8,128)(2,1)}, bf16[256,128]{1,0:T(8,128)(2,1)S(1)}, u32[]{:S(2)}, u32[]{:S(2)}) %collective-permute-start.15) | collective-permute-done | bytes 65568 | tf_op jit(solution)/shard_map/ppermute | solution.py:598
  215.9 2.9 %project.1 = (bf16[64,2048]{1,0:T(8,128)(2,1)}, bf16[64,2048]{1,0:T(8,128)(2,1)}, bf16[64,2048]{1,0:T(8,128)(2,1)}, bf16[64,2048]{1,0:T(8,128)(2,1)}) custom-call(s32[1]{0:T(128)} %bitcast.own_ref, s32[1]{0:T(128)} %bitcast.1.tp_ref.index_ref, bf16[256,128]{1,0:T(8,128)(2,1)} %get-tuple-element.27.keep_ref, bf16[256,128]{1,0:T(8,128)(2,1)} %copy-done.26, ...), custom_call_target="tpu_custom_call" | custom-call | tf_op jit(solution)/shard_map/project/pallas_call | solution.py:265
  222.3 2.0 way_back.1.slot_ref
  225.1 2.1 collective-permute-done.16
  227.1 3.9 %collective-permute-done.17 = bf16[64,2048]{1,0:T(8,128)(2,1)S(1)} collective-permute-done((bf16[64,2048]{1,0:T(8,128)(2,1)}, bf16[64,2048]{1,0:T(8,128)(2,1)S(1)}, u32[]{:S(2)}, u32[]{:S(2)}) %collective-permute-start.17) | collective-permute-done | bytes 262176 | tf_op jit(solution)/shard_map/ppermute | solution.py:601
  231.0 2.1 collective-permute-done.18
  235.0 2.8 %combine.1 = bf16[256,512]{1,0:T(8,128)(2,1)} custom-call(s32[256,2]{1,0:T(8,128)} %way_back.1.slot_ref, f32[256,2]{1,0:T(8,128)} %copy.15.weight_ref, bf16[1024,512]{1,0:T(8,128)(2,1)} %bitcast.20), custom_call_target="tpu_custom_call" | custom-call | tf_op jit(solution)/shard_map/combine/pallas_call | solution.py:500
  (126 shorter events, 32.3 us)
Async XLA Ops:
  45.0 25.0 %copy-start.3 = (bf16[64,16,512]{2,1,0:T(8,128)(2,1)}, bf16[64,16,512]{2,1,0:T(8,128)(2,1)S(1)}, u32[]{:S(2)}) copy-start(bf16[64,16,512]{2,1,0:T(8,128)(2,1)S(1)} %all_to_all.10) | copy-start | bytes 3145732
  45.0 24.8 %collective-permute-start.19 = (bf16[1024,512]{1,0:T(8,128)(2,1)S(1)}, bf16[1024,512]{1,0:T(8,128)(2,1)S(1)}, u32[]{:S(2)}, u32[]{:S(2)}) collective-permute-start(bf16[1024,512]{1,0:T(8,128)(2,1)S(1)} %bitcast.21), channel_id=1, source_target_pairs={{0,1},{1,2},{2,3},{3,0},{4,5},{5,6},{6,7},{7,4},{8,9},{9,10},{10,1... | collective-permute-start | bytes 3145736 | tf_op jit(solution)/shard_map/ppermute | solution.py:536
  46.2 23.7 %collective-permute-start.20 = (bf16[1024,512]{1,0:T(8,128)(2,1)S(1)}, bf16[1024,512]{1,0:T(8,128)(2,1)S(1)}, u32[]{:S(2)}, u32[]{:S(2)}) collective-permute-start(bf16[1024,512]{1,0:T(8,128)(2,1)S(1)} %bitcast.22), channel_id=1, source_target_pairs={{0,3},{1,0},{2,1},{3,2},{4,7},{5,4},{6,5},{7,6},{8,11},{9,8},{10,9... | collective-permute-start | bytes 3145736 | tf_op jit(solution)/shard_map/ppermute | solution.py:536
  69.8 12.8 %collective-permute-start.21 = (bf16[512,512]{1,0:T(8,128)(2,1)S(1)}, bf16[512,512]{1,0:T(8,128)(2,1)S(1)}, u32[]{:S(2)}, u32[]{:S(2)}) collective-permute-start(bf16[512,512]{1,0:T(8,128)(2,1)S(1)} %slice.34), channel_id=1, source_target_pairs={{0,1},{1,2},{2,3},{3,0},{4,5},{5,6},{6,7},{7,4},{8,9},{9,10},{10,1... | collective-permute-start | bytes 1572872 | tf_op jit(solution)/shard_map/ppermute | solution.py:541
  70.0 12.6 %collective-permute-start.22 = (bf16[512,512]{1,0:T(8,128)(2,1)S(1)}, bf16[512,512]{1,0:T(8,128)(2,1)S(1)}, u32[]{:S(2)}, u32[]{:S(2)}) collective-permute-start(bf16[512,512]{1,0:T(8,128)(2,1)S(1)} %slice.35), channel_id=1, source_target_pairs={{0,3},{1,0},{2,1},{3,2},{4,7},{5,4},{6,5},{7,6},{8,11},{9,8},{10,9... | collective-permute-start | bytes 1572872 | tf_op jit(solution)/shard_map/ppermute | solution.py:541
  89.9 24.1 %collective-permute-start.23 = (bf16[1024,256]{1,0:T(8,128)(2,1)}, bf16[1024,256]{1,0:T(8,128)(2,1)S(1)}, u32[]{:S(2)}, u32[]{:S(2)}) collective-permute-start(bf16[1024,256]{1,0:T(8,128)(2,1)} %up_projections.1.a), channel_id=1, source_target_pairs={{0,1},{1,2},{2,3},{3,0},{4,5},{5,6},{6,7},{7,4},{8,9},{9,10},{10,1... | collective-permute-start | bytes 1572872 | tf_op jit(solution)/shard_map/ppermute | solution.py:536
  89.9 24.1 %collective-permute-start.24 = (bf16[1024,256]{1,0:T(8,128)(2,1)}, bf16[1024,256]{1,0:T(8,128)(2,1)S(1)}, u32[]{:S(2)}, u32[]{:S(2)}) collective-permute-start(bf16[1024,256]{1,0:T(8,128)(2,1)} %up_projections.1.a), channel_id=1, source_target_pairs={{0,3},{1,0},{2,1},{3,2},{4,7},{5,4},{6,5},{7,6},{8,11},{9,8},{10,9... | collective-permute-start | bytes 1572872 | tf_op jit(solution)/shard_map/ppermute | solution.py:536
  94.6 15.5 %collective-permute-start.27 = (bf16[256,512]{1,0:T(8,128)(2,1)}, bf16[256,512]{1,0:T(8,128)(2,1)S(1)}, u32[]{:S(2)}, u32[]{:S(2)}) collective-permute-start(bf16[256,512]{1,0:T(8,128)(2,1)} %get-tuple-element.33), channel_id=1, source_target_pairs={{0,1},{1,2},{2,3},{3,0},{4,5},{5,6},{6,7},{7,4},{8,9},{9,10},{10,1... | collective-permute-start | bytes 786440 | tf_op jit(solution)/shard_map/ppermute | solution.py:566
  96.5 11.2 %collective-permute-start = (bf16[272,256]{1,0:T(8,128)(2,1)}, bf16[272,256]{1,0:T(8,128)(2,1)S(1)}, u32[]{:S(2)}, u32[]{:S(2)}) collective-permute-start(bf16[272,256]{1,0:T(8,128)(2,1)} %get-tuple-element.20), channel_id=1, source_target_pairs={{0,252},{4,248},{8,244},{12,240},{16,236},{20,232},{24,228},{28,22... | collective-permute-start | bytes 417800 | tf_op jit(solution)/shard_map/ppermute | solution.py:544
  102.4 14.4 %collective-permute-start.28 = (bf16[256,512]{1,0:T(8,128)(2,1)S(1)}, bf16[256,512]{1,0:T(8,128)(2,1)S(1)}, u32[]{:S(2)}, u32[]{:S(2)}) collective-permute-start(bf16[256,512]{1,0:T(8,128)(2,1)S(1)} %copy-done.32), channel_id=1, source_target_pairs={{0,3},{1,0},{2,1},{3,2},{4,7},{5,4},{6,5},{7,6},{8,11},{9,8},{10,9... | collective-permute-start | bytes 786440 | tf_op jit(solution)/shard_map/ppermute | solution.py:566
  108.6 10.1 %collective-permute-start.4 = (bf16[2,144,256]{2,1,0:T(8,128)(2,1)S(1)}, bf16[2,144,256]{2,1,0:T(8,128)(2,1)S(1)}, u32[]{:S(2)}, u32[]{:S(2)}) collective-permute-start(bf16[2,144,256]{2,1,0:T(8,128)(2,1)S(1)} %pad_maximum_fusion.refs_0_), channel_id=1, source_target_pairs={{0,64},{4,68},{8,72},{12,76},{16,80},{20,84},{24,88},{28,92},{32,9... | collective-permute-start | bytes 442376 | tf_op jit(solution)/shard_map/ppermute | solution.py:555
  110.1 9.5 %collective-permute-start.5 = (bf16[2,144,256]{2,1,0:T(8,128)(2,1)S(1)}, bf16[2,144,256]{2,1,0:T(8,128)(2,1)S(1)}, u32[]{:S(2)}, u32[]{:S(2)}) collective-permute-start(bf16[2,144,256]{2,1,0:T(8,128)(2,1)S(1)} %pad_maximum_fusion.refs_0_), channel_id=1, source_target_pairs={{0,192},{4,196},{8,200},{12,204},{16,208},{20,212},{24,216},{28,22... | collective-permute-start | bytes 442376 | tf_op jit(solution)/shard_map/ppermute | solution.py:555
  114.0 8.3 %collective-permute-start.2 = (bf16[2,144,256]{2,1,0:T(8,128)(2,1)S(1)}, bf16[2,144,256]{2,1,0:T(8,128)(2,1)S(1)}, u32[]{:S(2)}, u32[]{:S(2)}) collective-permute-start(bf16[2,144,256]{2,1,0:T(8,128)(2,1)S(1)} %pad_maximum_fusion.refs_0_), channel_id=1, source_target_pairs={{0,32},{4,36},{8,40},{12,44},{16,48},{20,52},{24,56},{28,60},{32,6... | collective-permute-start | bytes 442376 | tf_op jit(solution)/shard_map/ppermute | solution.py:555
  114.1 8.7 %collective-permute-start.3 = (bf16[2,144,256]{2,1,0:T(8,128)(2,1)S(1)}, bf16[2,144,256]{2,1,0:T(8,128)(2,1)S(1)}, u32[]{:S(2)}, u32[]{:S(2)}) collective-permute-start(bf16[2,144,256]{2,1,0:T(8,128)(2,1)S(1)} %pad_maximum_fusion.refs_0_), channel_id=1, source_target_pairs={{0,224},{4,228},{8,232},{12,236},{16,240},{20,244},{24,248},{28,25... | collective-permute-start | bytes 442376 | tf_op jit(solution)/shard_map/ppermute | solution.py:555
  117.7 22.9 %collective-permute-start.29 = (bf16[256,512]{1,0:T(8,128)(2,1)S(1)}, bf16[256,512]{1,0:T(8,128)(2,1)S(1)}, u32[]{:S(2)}, u32[]{:S(2)}) collective-permute-start(bf16[256,512]{1,0:T(8,128)(2,1)S(1)} %copy-done.31), channel_id=1, source_target_pairs={{0,2},{1,3},{2,0},{3,1},{4,6},{5,7},{6,4},{7,5},{8,10},{9,11},{10,... | collective-permute-start | bytes 786440 | tf_op jit(solution)/shard_map/ppermute | solution.py:566
  118.7 22.8 %collective-permute-start.25 = (bf16[512,256]{1,0:T(8,128)(2,1)S(1)}, bf16[512,256]{1,0:T(8,128)(2,1)S(1)}, u32[]{:S(2)}, u32[]{:S(2)}) collective-permute-start(bf16[512,256]{1,0:T(8,128)(2,1)S(1)} %slice.36), channel_id=1, source_target_pairs={{0,1},{1,2},{2,3},{3,0},{4,5},{5,6},{6,7},{7,4},{8,9},{9,10},{10,1... | collective-permute-start | bytes 786440 | tf_op jit(solution)/shard_map/ppermute | solution.py:541
  119.6 21.9 %collective-permute-start.26 = (bf16[512,256]{1,0:T(8,128)(2,1)S(1)}, bf16[512,256]{1,0:T(8,128)(2,1)S(1)}, u32[]{:S(2)}, u32[]{:S(2)}) collective-permute-start(bf16[512,256]{1,0:T(8,128)(2,1)S(1)} %slice.37), channel_id=1, source_target_pairs={{0,3},{1,0},{2,1},{3,2},{4,7},{5,4},{6,5},{7,6},{8,11},{9,8},{10,9... | collective-permute-start | bytes 786440 | tf_op jit(solution)/shard_map/ppermute | solution.py:541
  122.3 5.6 %collective-permute-start.8 = (bf16[1,144,256]{2,1,0:T(8,128)(2,1)S(1)}, bf16[1,144,256]{2,1,0:T(8,128)(2,1)S(1)}, u32[]{:S(2)}, u32[]{:S(2)}) collective-permute-start(bf16[1,144,256]{2,1,0:T(8,128)(2,1)S(1)} %slice.32), channel_id=1, source_target_pairs={{0,64},{4,68},{8,72},{12,76},{16,80},{20,84},{24,88},{28,92},{32,9... | collective-permute-start | bytes 221192 | tf_op jit(solution)/shard_map/ppermute | solution.py:559
  122.8 5.4 %collective-permute-start.9 = (bf16[1,144,256]{2,1,0:T(8,128)(2,1)S(1)}, bf16[1,144,256]{2,1,0:T(8,128)(2,1)S(1)}, u32[]{:S(2)}, u32[]{:S(2)}) collective-permute-start(bf16[1,144,256]{2,1,0:T(8,128)(2,1)S(1)} %slice.33), channel_id=1, source_target_pairs={{0,192},{4,196},{8,200},{12,204},{16,208},{20,212},{24,216},{28,22... | collective-permute-start | bytes 221192 | tf_op jit(solution)/shard_map/ppermute | solution.py:560
  127.9 6.1 %collective-permute-start.6 = (bf16[2,144,256]{2,1,0:T(8,128)(2,1)S(1)}, bf16[2,144,256]{2,1,0:T(8,128)(2,1)S(1)}, u32[]{:S(2)}, u32[]{:S(2)}) collective-permute-start(bf16[2,144,256]{2,1,0:T(8,128)(2,1)S(1)} %collective-permute-done.4.refs_3_), channel_id=1, source_target_pairs={{0,32},{4,36},{8,40},{12,44},{16,48},{20,52},{24,56},{28,60},{32,6... | collective-permute-start | bytes 442376 | tf_op jit(solution)/shard_map/ppermute | solution.py:557
  128.2 7.6 %collective-permute-start.7 = (bf16[2,144,256]{2,1,0:T(8,128)(2,1)S(1)}, bf16[2,144,256]{2,1,0:T(8,128)(2,1)S(1)}, u32[]{:S(2)}, u32[]{:S(2)}) collective-permute-start(bf16[2,144,256]{2,1,0:T(8,128)(2,1)S(1)} %collective-permute-done.5.refs_4_), channel_id=1, source_target_pairs={{0,224},{4,228},{8,232},{12,236},{16,240},{20,244},{24,248},{28,25... | collective-permute-start | bytes 442376 | tf_op jit(solution)/shard_map/ppermute | solution.py:558
  134.0 26.1 %collective-permute-start.10 = (bf16[2,128,256]{2,1,0:T(8,128)(2,1)S(1)}, bf16[2,128,256]{2,1,0:T(8,128)(2,1)S(1)}, u32[]{:S(2)}, u32[]{:S(2)}) collective-permute-start(bf16[2,128,256]{2,1,0:T(8,128)(2,1)S(1)} %pad_maximum_fusion.1.refs_1_), channel_id=1, source_target_pairs={{0,16},{4,20},{8,24},{12,28},{16,0},{20,4},{24,8},{28,12},{32,48},... | collective-permute-start | bytes 393224 | tf_op jit(solution)/shard_map/ppermute | solution.py:552
  135.8 24.4 %collective-permute-start.11 = (bf16[2,128,256]{2,1,0:T(8,128)(2,1)S(1)}, bf16[2,128,256]{2,1,0:T(8,128)(2,1)S(1)}, u32[]{:S(2)}, u32[]{:S(2)}) collective-permute-start(bf16[2,128,256]{2,1,0:T(8,128)(2,1)S(1)} %pad_maximum_fusion.1.refs_1_), channel_id=1, source_target_pairs={{0,8},{4,12},{8,16},{12,20},{16,24},{20,28},{24,0},{28,4},{32,40},... | collective-permute-start | bytes 393224 | tf_op jit(solution)/shard_map/ppermute | solution.py:552
  140.6 40.7 %collective-permute-start.1 = (bf16[2,128,256]{2,1,0:T(8,128)(2,1)S(1)}, bf16[2,128,256]{2,1,0:T(8,128)(2,1)S(1)}, u32[]{:S(2)}, u32[]{:S(2)}) collective-permute-start(bf16[2,128,256]{2,1,0:T(8,128)(2,1)S(1)} %pad_maximum_fusion.1.refs_1_), channel_id=1, source_target_pairs={{0,24},{4,28},{8,0},{12,4},{16,8},{20,12},{24,16},{28,20},{32,56},... | collective-permute-start | bytes 393224 | tf_op jit(solution)/shard_map/ppermute | solution.py:552
  147.9 86.1 %all-to-all-start.1 = ((bf16[64,16,512]{2,1,0:T(8,128)(2,1)}), bf16[64,16,512]{2,1,0:T(8,128)(2,1)S(1)}, u32[]{:S(2)}, u32[]{:S(2)}) async-start(bf16[64,16,512]{2,1,0:T(8,128)(2,1)} %bitcast.18), calls=%async_computation.1 | async-start | bytes 2097152 | tf_op jit(solution)/shard_map/all_to_all | solution.py:530
  178.1 21.6 %collective-permute-start.12 = (bf16[2,160,256]{2,1,0:T(8,128)(2,1)}, bf16[2,160,256]{2,1,0:T(8,128)(2,1)S(1)}, u32[]{:S(2)}, u32[]{:S(2)}) collective-permute-start(bf16[2,160,256]{2,1,0:T(8,128)(2,1)} %get-tuple-element.24), channel_id=1, source_target_pairs={{0,24},{4,28},{8,0},{12,4},{16,8},{20,12},{24,16},{28,20},{32,56},... | collective-permute-start | bytes 491528 | tf_op jit(solution)/shard_map/ppermute | solution.py:582
  180.7 19.0 %collective-permute-start.14 = (bf16[2,160,256]{2,1,0:T(8,128)(2,1)}, bf16[2,160,256]{2,1,0:T(8,128)(2,1)S(1)}, u32[]{:S(2)}, u32[]{:S(2)}) collective-permute-start(bf16[2,160,256]{2,1,0:T(8,128)(2,1)} %get-tuple-element.26), channel_id=1, source_target_pairs={{0,16},{4,20},{8,24},{12,28},{16,0},{20,4},{24,8},{28,12},{32,48},... | collective-permute-start | bytes 491528 | tf_op jit(solution)/shard_map/ppermute | solution.py:582
  199.1 6.2 %collective-permute-start.13 = (bf16[2,160,256]{2,1,0:T(8,128)(2,1)}, bf16[2,160,256]{2,1,0:T(8,128)(2,1)S(1)}, u32[]{:S(2)}, u32[]{:S(2)}) collective-permute-start(bf16[2,160,256]{2,1,0:T(8,128)(2,1)} %get-tuple-element.25), channel_id=1, source_target_pairs={{0,8},{4,12},{8,16},{12,20},{16,24},{20,28},{24,0},{28,4},{32,40},... | collective-permute-start | bytes 491528 | tf_op jit(solution)/shard_map/ppermute | solution.py:582
  208.1 7.2 %collective-permute-start.15 = (bf16[256,128]{1,0:T(8,128)(2,1)}, bf16[256,128]{1,0:T(8,128)(2,1)S(1)}, u32[]{:S(2)}, u32[]{:S(2)}) collective-permute-start(bf16[256,128]{1,0:T(8,128)(2,1)} %get-tuple-element.28), channel_id=1, source_target_pairs={{0,252},{4,248},{8,244},{12,240},{16,236},{20,232},{24,228},{28,22... | collective-permute-start | bytes 196616 | tf_op jit(solution)/shard_map/ppermute | solution.py:598
  218.8 8.4 %collective-permute-start.16 = (bf16[64,2048]{1,0:T(8,128)(2,1)}, bf16[64,2048]{1,0:T(8,128)(2,1)S(1)}, u32[]{:S(2)}, u32[]{:S(2)}) collective-permute-start(bf16[64,2048]{1,0:T(8,128)(2,1)} %get-tuple-element.30), channel_id=1, source_target_pairs={{0,1},{1,2},{2,3},{3,0},{4,5},{5,6},{6,7},{7,4},{8,9},{9,10},{10,1... | collective-permute-start | bytes 786440 | tf_op jit(solution)/shard_map/ppermute | solution.py:601
  218.8 12.2 %collective-permute-start.17 = (bf16[64,2048]{1,0:T(8,128)(2,1)}, bf16[64,2048]{1,0:T(8,128)(2,1)S(1)}, u32[]{:S(2)}, u32[]{:S(2)}) collective-permute-start(bf16[64,2048]{1,0:T(8,128)(2,1)} %get-tuple-element.31), channel_id=1, source_target_pairs={{0,2},{1,3},{2,0},{3,1},{4,6},{5,7},{6,4},{7,5},{8,10},{9,11},{10,... | collective-permute-start | bytes 786440 | tf_op jit(solution)/shard_map/ppermute | solution.py:601
  220.5 12.6 %collective-permute-start.18 = (bf16[64,2048]{1,0:T(8,128)(2,1)}, bf16[64,2048]{1,0:T(8,128)(2,1)S(1)}, u32[]{:S(2)}, u32[]{:S(2)}) collective-permute-start(bf16[64,2048]{1,0:T(8,128)(2,1)} %get-tuple-element.32), channel_id=1, source_target_pairs={{0,3},{1,0},{2,1},{3,2},{4,7},{5,4},{6,5},{7,6},{8,11},{9,8},{10,9... | collective-permute-start | bytes 786440 | tf_op jit(solution)/shard_map/ppermute | solution.py:601
  (35 other events, 215.0 us)

commit v3 on v2

--- a/solution.py
+++ b/solution.py
@@ -46,18 +46,19 @@
 
 def pack_body(own_ref, queries_ref, keys_ref, values_ref, gates_ref, keep_ref, send_ref):
     rows = keys_ref.shape[0]
+    half = rows // 2
     keys_t = keys_ref[...].astype(F32).T
     values_t = values_ref[...].astype(F32).T
-    queries_t = (queries_ref[...].astype(F32) * HD ** (-0.5)).T
     split = pieces_of(gates_ref[...])
     pad = jnp.zeros((HEAD_ROWS - HD - 6, rows), F32)
     blocks = []
     for g in range(2):
         gates = [piece[2 * g + r : 2 * g + r + 1] for r in range(2) for piece in split]
         heads = slice(g * HD, (g + 1) * HD)
-        parts = [keys_t[heads]] + gates + [pad, values_t[heads]]
-        parts.append(queries_t[2 * g * HD : 2 * (g + 1) * HD])
-        blocks.append(jnp.concatenate(parts, axis=0).astype(BF16))
+        upper = jnp.concatenate([keys_t[heads]] + gates + [pad, values_t[heads]], axis=0)
+        wide = queries_ref[:, g * 128 : (g + 1) * 128].astype(F32)
+        lower = jnp.concatenate([wide[:half], wide[half:]], axis=1)
+        blocks.append(jnp.concatenate([upper, lower], axis=0).astype(BF16))
     even = lax.rem(own_ref[0], 2) == 0
 
     @pl.when(even)
@@ -73,7 +74,7 @@
 
 def pack(own, queries, keys, values, gates_t):
     rows = keys.shape[0]
-    shape = (KV_ROWS + 2 * HD, rows)
+    shape = (KV_ROWS + rows // 2, rows)
     return pl.pallas_call(
         pack_body,
         grid_spec=pltpu.PrefetchScalarGridSpec(
@@ -91,14 +92,14 @@
     kv_refs, key_ref, value_ref = refs[:9], refs[9], refs[10]
     z = own_ref[0] // 8
     rows = kv_refs[0].shape[2]
-    value_ref[:, pl.ds(HD, HEAD_ROWS - HD), :] = jnp.ones(
-        (value_ref.shape[0], HEAD_ROWS - HD, 2 * rows), BF16
-    )
+    ones = jnp.ones((rows, HD), F32)
 
     def place_keys(slab, at, block):
-        turned = block[:HEAD_ROWS].astype(F32).T
-        key_ref[slab, pl.ds(at * rows, rows), :] = turned.astype(BF16)
-        value_ref[slab, pl.ds(0, HD), pl.ds(at * rows, rows)] = block[HEAD_ROWS:]
+        key_ref[slab, :, pl.ds(at * rows, rows)] = block[:HEAD_ROWS]
+        turned = block[HEAD_ROWS:].astype(F32).T
+        value_ref[slab, pl.ds(at * rows, rows), :] = jnp.concatenate(
+            [turned, ones], axis=1
+        ).astype(BF16)
 
     for number, shift in enumerate(Z_STEPS):
         source = lax.rem(z + shift + 8, 8)
@@ -111,7 +112,7 @@
 
 def assemble(own, kv_parts):
     rows = kv_parts[0].shape[2]
-    shapes = [(8, 2 * rows, HEAD_ROWS), (8, HEAD_ROWS, 2 * rows)]
+    shapes = [(8, HEAD_ROWS, 2 * rows), (8, 2 * rows, 128)]
     return pl.pallas_call(
         assemble_body,
         grid_spec=pltpu.PrefetchScalarGridSpec(
@@ -129,76 +130,96 @@
     count_y = len(steps)
     q_refs, (key_ref, value_ref) = refs[:count_y], refs[count_y : count_y + 2]
     o_refs = refs[count_y + 2 : 2 * count_y + 2]
-    query_ref, acc_ref, max_ref = refs[2 * count_y + 2 :]
+    query_ref, acc_ref, max_ref, score_ref = refs[2 * count_y + 2 :]
     z, y, core = own_ref[0] // 8, own_ref[0] // 2 % 4, own_ref[0] % 2
     rows = q_refs[0].shape[2]
-    line = lax.broadcasted_iota(jnp.int32, (HEAD_ROWS - HD, rows), 0)
+    column = lax.broadcasted_iota(jnp.int32, (rows, HEAD_ROWS - HD), 1)
     for number, ref in enumerate(q_refs):
         for slot in range(2):
+            packed = ref[slot].astype(F32) * HD ** (-0.5)
+            both = jnp.concatenate([packed[:, :128], packed[:, 128:]], axis=0)
             for r in range(2):
-                picks = jnp.where((line >= 3 * r) & (line < 3 * r + 3), -1.0, 0.0).astype(F32)
-                heads = ref[slot, r * HD : (r + 1) * HD, :].astype(F32)
-                query_ref[2 * number + slot, r] = jnp.concatenate([heads, picks], axis=0).astype(
-                    BF16
-                )
+                picks = jnp.where((column >= 3 * r) & (column < 3 * r + 3), -1.0, 0.0)
+                query_ref[slot, pl.ds((2 * number + r) * rows, rows), :] = jnp.concatenate(
+                    [both[:, r * HD : (r + 1) * HD], picks.astype(F32)], axis=1
+                ).astype(BF16)
     low = jnp.minimum(z, 7 - z)
     offset = 2 * y + core
+
+    blocks = range(0, 2 * count_y * rows, TALL)
 
     def run_half(high, carry):
         count = jnp.where(high == 1, 7 - low, low)
         slot = jnp.where(count == z, 0, 1)
-        acc_ref[...] = jnp.zeros_like(acc_ref)
-        max_ref[...] = jnp.full_like(max_ref, MASKED)
-
-        def one_slab(slab, masked):
-            keys = key_ref[slab]
-            values = value_ref[slab]
-            for number, shift in enumerate(steps):
-                for r in range(2):
-                    scores = jnp.dot(
-                        keys, query_ref[2 * number + slot, r], preferred_element_type=F32
-                    )
-                    if masked:
-                        line = lax.broadcasted_iota(jnp.int32, scores.shape, 0)
-                        key_at = line + jnp.where(
-                            line < rows, offset * rows, (7 - offset) * rows - rows
-                        )
-                        own = 2 * lax.rem(y + shift + 4, 4) + core
-                        own = jnp.where(slot == 0, own, 7 - own)
-                        query_at = own * rows + lax.broadcasted_iota(jnp.int32, scores.shape, 1)
-                        scores = jnp.where(key_at <= query_at, scores, MASKED)
-                    old = max_ref[number, r]
-                    new = jnp.maximum(old, jnp.max(scores, axis=0, keepdims=True))
-                    weights = jnp.exp(scores - new[0:1]).astype(BF16)
-                    max_ref[number, r] = new
-                    acc_ref[number, r] = acc_ref[number, r] * jnp.exp(old - new)[0:1] + jnp.dot(
-                        values, weights, preferred_element_type=F32
-                    )
-
-        def open_slab(slab, carry):
-            one_slab(slab, False)
+        for block in blocks:
+            at = pl.ds(block, TALL)
+            scores = jnp.dot(query_ref[slot, at, :], key_ref[count], preferred_element_type=F32)
+            lane = lax.broadcasted_iota(jnp.int32, scores.shape, 1)
+            key_at = lane + jnp.where(lane < rows, offset * rows, (7 - offset) * rows - rows)
+            row = block + lax.broadcasted_iota(jnp.int32, scores.shape, 0)
+            owns = [2 * lax.rem(y + shift + 4, 4) + core for shift in steps]
+            owns = [jnp.where(slot == 0, own, 7 - own) for own in owns]
+            own = jnp.where(row < 2 * rows, owns[0], owns[-1])
+            scores = jnp.where(key_at <= own * rows + row % rows, scores, MASKED)
+            score_ref[0, at, :] = scores
+            max_ref[at, :] = jnp.broadcast_to(jnp.max(scores, axis=1, keepdims=True), (TALL, 128))
+            acc_ref[at, :] = jnp.zeros((TALL, 128), F32)
+
+        def add_slab(slab, held, block):
+            at = pl.ds(block, TALL)
+            highest = jnp.concatenate([max_ref[at, :]] * 4, axis=1)
+            weights = jnp.exp(score_ref[held, at, :] - highest).astype(BF16)
+            acc_ref[at, :] += jnp.dot(weights, value_ref[slab], preferred_element_type=F32)
+
+        def next_slab(turn, carry):
+            slab = count - turn
+            held = lax.rem(turn, 2)
+            peaks = []
+            for block in blocks:
+                at = pl.ds(block, TALL)
+                scores = jnp.dot(
+                    query_ref[slot, at, :], key_ref[slab - 1], preferred_element_type=F32
+                )
+                score_ref[1 - held, at, :] = scores
+                highest = jnp.concatenate([max_ref[at, :]] * 4, axis=1)
+                peaks.append(jnp.max(scores - highest))
+                add_slab(slab, held, block)
+
+            @pl.when(functools.reduce(jnp.maximum, peaks) > 60.0)
+            def _():
+                for block in blocks:
+                    at = pl.ds(block, TALL)
+                    old = max_ref[at, :]
+                    top = jnp.max(score_ref[1 - held, at, :], axis=1, keepdims=True)
+                    new = jnp.maximum(old, top)
+                    acc_ref[at, :] = acc_ref[at, :] * jnp.exp(old - new)
+                    max_ref[at, :] = new
+
             return carry
 
-        lax.fori_loop(0, count, open_slab, 0)
-        one_slab(count, True)
-        blank = jnp.zeros((HEAD_ROWS - HD - 3, rows), F32)
+        lax.fori_loop(0, count, next_slab, 0)
+        for block in blocks:
+            add_slab(0, lax.rem(count, 2), block)
+        lane = lax.broadcasted_iota(jnp.int32, (2 * rows, 128), 1)
         for number in range(count_y):
-            for r in range(2):
-                total = acc_ref[number, r]
-                weight = total[HD : HD + 1]
-                stats = pieces_of(max_ref[number, r][0:1] + jnp.log(weight))
-                o_refs[number][slot, pl.ds(r * HEAD_ROWS, HEAD_ROWS), :] = jnp.concatenate(
-                    [total[:HD] / weight, *stats, blank], axis=0
-                ).astype(BF16)
+            at = pl.ds(number * 2 * rows, 2 * rows)
+            total = acc_ref[at, :]
+            weight = total[:, HD : HD + 1]
+            first, second, third = pieces_of(max_ref[at, :] + jnp.log(weight))
+            stats = jnp.where(lane < 80, first, jnp.where(lane < 96, second, third))
+            o_refs[number][slot] = jnp.where(lane < HD, total / weight, stats).astype(BF16)
         return carry
 
     lax.fori_loop(0, 2, run_half, 0)
+
+
+TALL = 1024
 
 
 def attention(own, steps, query_parts, keys, values):
     rows = query_parts[0].shape[2]
     count_y = len(steps)
-    shape = (2, 2 * HEAD_ROWS, rows)
+    shape = (2, 2 * rows, 128)
     operands = (*query_parts, keys, values)
     return pl.pallas_call(
         functools.partial(attention_body, steps=steps),
@@ -208,9 +229,10 @@
             in_specs=[whole(x.shape) for x in operands],
             out_specs=[whole(shape)] * count_y,
             scratch_shapes=[
-                pltpu.VMEM((2 * count_y, 2, HEAD_ROWS, rows), BF16),
-                pltpu.VMEM((count_y, 2, HEAD_ROWS, rows), F32),
-                pltpu.VMEM((count_y, 2, 8, rows), F32),
+                pltpu.VMEM((2, 2 * count_y * rows, HEAD_ROWS), BF16),
+                pltpu.VMEM((2 * count_y * rows, 128), F32),
+                pltpu.VMEM((2 * count_y * rows, 128), F32),
+                pltpu.VMEM((2, 2 * count_y * rows, 2 * rows), F32),
             ],
         ),
         out_shape=[jax.ShapeDtypeStruct(shape, BF16)] * count_y,
@@ -222,27 +244,22 @@
 
 
 def merge_body(a, b, c, d, keep_ref, send_ref):
+    rows = keep_ref.shape[0]
     for slot, target in enumerate((keep_ref, send_ref)):
-        heads = []
-        for r in range(2):
-            block = pl.ds(r * HEAD_ROWS, HEAD_ROWS)
-            parts = [ref[slot, block, :].astype(F32) for ref in (a, b, c, d)]
-            logs = [x[HD : HD + 1] + x[HD + 1 : HD + 2] + x[HD + 2 : HD + 3] for x in parts]
-            highest = functools.reduce(jnp.maximum, logs)
-            shares = [jnp.exp(x - highest) for x in logs]
-            total = functools.reduce(jnp.add, shares)
-            mixed = functools.reduce(
-                jnp.add, [x[:HD] * share for x, share in zip(parts, shares)]
-            )
-            heads.append(mixed / total)
-        target[...] = jnp.concatenate(heads, axis=0).T.astype(BF16)
+        parts = [ref[slot].astype(F32) for ref in (a, b, c, d)]
+        logs = [x[:, 64:65] + x[:, 80:81] + x[:, 96:97] for x in parts]
+        highest = functools.reduce(jnp.maximum, logs)
+        shares = [jnp.exp(x - highest) for x in logs]
+        total = functools.reduce(jnp.add, shares)
+        mixed = functools.reduce(jnp.add, [x * share for x, share in zip(parts, shares)]) / total
+        target[...] = jnp.concatenate([mixed[:rows, :HD], mixed[rows:, :HD]], axis=1).astype(BF16)
 
 
 def merge(parts):
-    rows = parts[0].shape[2]
+    rows = parts[0].shape[1] // 2
     return pl.pallas_call(
         merge_body,
-        out_shape=[jax.ShapeDtypeStruct((rows, 2 * HD), BF16)] * 2,
+        out_shape=[jax.ShapeDtypeStruct((rows, 128), BF16)] * 2,
         name="merge",
     )(*parts)
 

time: 240 us -> 234 us (0.975)
  Pallas kernels: 65.3 us -> 57 us
  waiting for transfers between devices: 57.4 us -> 59.9 us
    pallas_call x2, Pallas kernels: 34.5 us -> 24.7 us  [attention(): pl.pallas_call(functools.partial(attention_body, steps=steps), grid_spec=...]
  transfers between devices with their start and end apart: 31 -> 31, of which waited for: 12 -> 12; matrix products, arithmetic and copies ran while one was open for 1% -> 1% of each run, Pallas kernels for 22% -> 19%
where the time goes in v3:
time: 234 us; the launch traced here: 232 us
  starting transfers between devices  62.2 us (27%)
  waiting for transfers between devices  59.9 us (26%)
  Pallas kernels  57 us (24%)
  blocking collectives  41.3 us (18%)
  local copies, waits for them, and re-layouts  8.7 us (4%)
    all_to_all x1, blocking collectives, over_ep(): lax.all_to_all(x.reshape(size, -1, wide), 'ep', split_axis=0, concat_axis...  41.3 us
    pallas_call x2, Pallas kernels, attention(): pl.pallas_call(functools.partial(attention_body, steps=steps), grid_spec=...  24.7 us
    ppermute x4, waiting for transfers between devices, near(): return (lax.ppermute(x, 'tp', up_ring), lax.ppermute(x, 'tp', down_ring))  22.1 us
    all_to_all x1, starting transfers between devices, over_ep(): lax.all_to_all(x.reshape(size, -1, wide), 'ep', split_axis=0, concat_axis...  12.3 us
    ppermute x2, waiting for transfers between devices, far(): lax.ppermute(low, 'tp', up_ring)  9.88 us
    unnamed x74, local copies, waits for them, and re-layouts  8.58 us
    ppermute x4, starting transfers between devices, per_device(): lax.ppermute(own_keys, 'ep', along_z(shift, size))  8.1 us
    ppermute x3, waiting for transfers between devices, per_device(): lax.ppermute(product, 'tp', ring)  8.08 us
  transfers between devices with their start and end apart: 31, of which 12 were waited for; matrix products, arithmetic and copies ran while one was open for 1% of the time, Pallas kernels for 19%

profile of v3, /device:TPU:1, one launch (start us, length us, event | category | flops | bytes accessed | tf_op | source)
XLA Modules:
  0.0 231.7 jit_solution(13055401601517040251)
XLA Ops:
  0.6 3.1 %dispatch.1 = bf16[1024,512]{1,0:T(8,128)(2,1)} custom-call(s32[1]{0:T(128)} %bitcast.1.tp_ref.index_ref, bf16[256,2048]{1,0:T(8,128)(2,1)} %part_ref.1, bf16[256,2048]{1,0:T(8,128)(2,1)} %part_ref.1, f32[1,2048]{1,0:T(1,128)} %bitcast.28, s32[2,256]{1,0:T(2,128)} %bitcast.29), custom_call_target="tpu_custom_call" | custom-call | tf_op jit(solution)/shard_map/dispatch/pallas_call | solution.py:341
  3.7 41.3 %all_to_all.10 = bf16[64,16,512]{2,1,0:T(8,128)(2,1)S(1)} all-to-all(bf16[64,16,512]{2,1,0:T(8,128)(2,1)} %bitcast.19), channel_id=1, replica_groups=mesh['ep'=64,'tp'=4] {'ep'}, dimensions={0} | all-to-all | bytes 2097152 | tf_op jit(solution)/shard_map/all_to_all | solution.py:547
  47.7 22.1 %collective-permute-done.19.b = bf16[1024,512]{1,0:T(8,128)(2,1)S(1)} collective-permute-done((bf16[1024,512]{1,0:T(8,128)(2,1)S(1)}, bf16[1024,512]{1,0:T(8,128)(2,1)S(1)}, u32[]{:S(2)}, u32[]{:S(2)}) %collective-permute-start.19) | collective-permute-done | bytes 1048608 | tf_op jit(solution)/shard_map/ppermute | solution.py:553
  70.0 2.7 %collective-permute-start.22 = (bf16[512,512]{1,0:T(8,128)(2,1)S(1)}, bf16[512,512]{1,0:T(8,128)(2,1)S(1)}, u32[]{:S(2)}, u32[]{:S(2)}) collective-permute-start(bf16[512,512]{1,0:T(8,128)(2,1)S(1)} %slice.35), channel_id=1, source_target_pairs={{0,3},{1,0},{2,1},{3,2},{4,7},{5,4},{6,5},{7,6},{8,11},{9,8},{10,9... | collective-permute-start | bytes 1572872 | tf_op jit(solution)/shard_map/ppermute | solution.py:558
  72.7 9.9 %collective-permute-done.21.d = bf16[512,512]{1,0:T(8,128)(2,1)S(1)} collective-permute-done((bf16[512,512]{1,0:T(8,128)(2,1)S(1)}, bf16[512,512]{1,0:T(8,128)(2,1)S(1)}, u32[]{:S(2)}, u32[]{:S(2)}) %collective-permute-start.21) | collective-permute-done | bytes 524320 | tf_op jit(solution)/shard_map/ppermute | solution.py:558
  83.6 6.3 %up_projections.1.a = bf16[1024,256]{1,0:T(8,128)(2,1)} custom-call(s32[1]{0:T(128)} %bitcast.1.tp_ref.index_ref, bf16[1024,512]{1,0:T(8,128)(2,1)} %bitcast.23, bf16[1024,512]{1,0:T(8,128)(2,1)} %copy-done.14, bf16[1024,512]{1,0:T(8,128)(2,1)} %copy-done.15, bf16[512,512]{1,0:T(8,128)(2,1)} %copy-done.29, bf16[512,512]{1,0:T(8,128)(2,1)} %copy-done.30, ...), custom_call_target="tpu_custom_call" | custom-call | flops 2200000000 | bytes 6800000 | tf_op jit(solution)/shard_map/up_projections/pallas_call | solution.py:425
  89.9 2.7 %collective-permute-start.24 = (bf16[1024,256]{1,0:T(8,128)(2,1)}, bf16[1024,256]{1,0:T(8,128)(2,1)S(1)}, u32[]{:S(2)}, u32[]{:S(2)}) collective-permute-start(bf16[1024,256]{1,0:T(8,128)(2,1)} %up_projections.1.a), channel_id=1, source_target_pairs={{0,3},{1,0},{2,1},{3,2},{4,7},{5,4},{6,5},{7,6},{8,11},{9,8},{10,9... | collective-permute-start | bytes 1572872 | tf_op jit(solution)/shard_map/ppermute | solution.py:553
  96.5 5.9 %collective-permute-start = (bf16[272,256]{1,0:T(8,128)(2,1)}, bf16[272,256]{1,0:T(8,128)(2,1)S(1)}, u32[]{:S(2)}, u32[]{:S(2)}) collective-permute-start(bf16[272,256]{1,0:T(8,128)(2,1)} %get-tuple-element.20), channel_id=1, source_target_pairs={{0,252},{4,248},{8,244},{12,240},{16,236},{20,232},{24,228},{28,22... | collective-permute-start | bytes 417800 | tf_op jit(solution)/shard_map/ppermute | solution.py:561
  102.4 2.9 %collective-permute-start.28 = (bf16[256,512]{1,0:T(8,128)(2,1)S(1)}, bf16[256,512]{1,0:T(8,128)(2,1)S(1)}, u32[]{:S(2)}, u32[]{:S(2)}) collective-permute-start(bf16[256,512]{1,0:T(8,128)(2,1)S(1)} %copy-done.32), channel_id=1, source_target_pairs={{0,3},{1,0},{2,1},{3,2},{4,7},{5,4},{6,5},{7,6},{8,11},{9,8},{10,9... | collective-permute-start | bytes 786440 | tf_op jit(solution)/shard_map/ppermute | solution.py:583
  105.3 2.4 %collective-permute-done = bf16[272,256]{1,0:T(8,128)(2,1)S(1)} collective-permute-done((bf16[272,256]{1,0:T(8,128)(2,1)}, bf16[272,256]{1,0:T(8,128)(2,1)S(1)}, u32[]{:S(2)}, u32[]{:S(2)}) %collective-permute-start) | collective-permute-done | bytes 139296 | tf_op jit(solution)/shard_map/ppermute | solution.py:561
  110.1 4.0 %collective-permute-start.5 = (bf16[2,144,256]{2,1,0:T(8,128)(2,1)S(1)}, bf16[2,144,256]{2,1,0:T(8,128)(2,1)S(1)}, u32[]{:S(2)}, u32[]{:S(2)}) collective-permute-start(bf16[2,144,256]{2,1,0:T(8,128)(2,1)S(1)} %pad_maximum_fusion.refs_0_), channel_id=1, source_target_pairs={{0,192},{4,196},{8,200},{12,204},{16,208},{20,212},{24,216},{28,22... | collective-permute-start | bytes 442376 | tf_op jit(solution)/shard_map/ppermute | solution.py:572
  114.1 2.7 %collective-permute-start.3 = (bf16[2,144,256]{2,1,0:T(8,128)(2,1)S(1)}, bf16[2,144,256]{2,1,0:T(8,128)(2,1)S(1)}, u32[]{:S(2)}, u32[]{:S(2)}) collective-permute-start(bf16[2,144,256]{2,1,0:T(8,128)(2,1)S(1)} %pad_maximum_fusion.refs_0_), channel_id=1, source_target_pairs={{0,224},{4,228},{8,232},{12,236},{16,240},{20,244},{24,248},{28,25... | collective-permute-start | bytes 442376 | tf_op jit(solution)/shard_map/ppermute | solution.py:572
  122.8 3.1 %collective-permute-start.9 = (bf16[1,144,256]{2,1,0:T(8,128)(2,1)S(1)}, bf16[1,144,256]{2,1,0:T(8,128)(2,1)S(1)}, u32[]{:S(2)}, u32[]{:S(2)}) collective-permute-start(bf16[1,144,256]{2,1,0:T(8,128)(2,1)S(1)} %slice.33), channel_id=1, source_target_pairs={{0,192},{4,196},{8,200},{12,204},{16,208},{20,212},{24,216},{28,22... | collective-permute-start | bytes 221192 | tf_op jit(solution)/shard_map/ppermute | solution.py:577
  125.9 2.0 collective-permute-done.8.refs_7_
  128.2 2.8 %collective-permute-start.7 = (bf16[2,144,256]{2,1,0:T(8,128)(2,1)S(1)}, bf16[2,144,256]{2,1,0:T(8,128)(2,1)S(1)}, u32[]{:S(2)}, u32[]{:S(2)}) collective-permute-start(bf16[2,144,256]{2,1,0:T(8,128)(2,1)S(1)} %collective-permute-done.5.refs_4_), channel_id=1, source_target_pairs={{0,224},{4,228},{8,232},{12,236},{16,240},{20,244},{24,248},{28,25... | collective-permute-start | bytes 442376 | tf_op jit(solution)/shard_map/ppermute | solution.py:575
  131.1 3.0 %collective-permute-done.6.refs_5_ = bf16[2,144,256]{2,1,0:T(8,128)(2,1)S(1)} collective-permute-done((bf16[2,144,256]{2,1,0:T(8,128)(2,1)S(1)}, bf16[2,144,256]{2,1,0:T(8,128)(2,1)S(1)}, u32[]{:S(2)}, u32[]{:S(2)}) %collective-permute-start.6) | collective-permute-done | bytes 147488 | tf_op jit(solution)/shard_map/ppermute | solution.py:574
  137.7 2.9 %assemble.1 = (bf16[8,80,512]{2,1,0:T(8,128)(2,1)}, bf16[8,512,128]{2,1,0:T(8,128)(2,1)}) custom-call(s32[1]{0:T(128)} %bitcast.own_ref, bf16[2,144,256]{2,1,0:T(8,128)(2,1)} %copy-done.4, bf16[2,144,256]{2,1,0:T(8,128)(2,1)} %copy-done.19, bf16[2,144,256]{2,1,0:T(8,128)(2,1)} %copy-done.20, bf16[2,144,256]{2,1,0:T(8,128)(2,1)} %copy-done.6, ...), custom_call_target="tpu_custom_call" | custom-call | tf_op jit(solution)/shard_map/assemble/pallas_call | solution.py:116
  142.8 5.0 %down_projection.1 = bf16[1024,512]{1,0:T(8,128)(2,1)} custom-call(s32[1]{0:T(128)} %bitcast.1.tp_ref.index_ref, bf16[1024,256]{1,0:T(8,128)(2,1)} %up_projections.1.a, bf16[1024,256]{1,0:T(8,128)(2,1)} %copy-done.1, bf16[1024,256]{1,0:T(8,128)(2,1)} %copy-done.2, bf16[512,256]{1,0:T(8,128)(2,1)} %copy-done.11, bf16[512,256]{1,0:T(8,128)(2,1)} %copy-done.12, ...), custom_call_target="tpu_custom_call" | custom-call | flops 1100000000 | bytes 4200000 | tf_op jit(solution)/shard_map/down_projection/pallas_call | solution.py:456
  147.8 12.3 %all-to-all-start.1 = ((bf16[64,16,512]{2,1,0:T(8,128)(2,1)}), bf16[64,16,512]{2,1,0:T(8,128)(2,1)S(1)}, u32[]{:S(2)}, u32[]{:S(2)}) async-start(bf16[64,16,512]{2,1,0:T(8,128)(2,1)} %bitcast.18), calls=%async_computation.1 | async-start | bytes 2097152 | tf_op jit(solution)/shard_map/all_to_all | solution.py:547
  160.9 12.5 %attention.3 = (bf16[2,512,128]{2,1,0:T(8,128)(2,1)}, bf16[2,512,128]{2,1,0:T(8,128)(2,1)}) custom-call(s32[1]{0:T(128)} %bitcast.own_ref, bf16[2,128,256]{2,1,0:T(8,128)(2,1)} %copy-done.33, bf16[2,128,256]{2,1,0:T(8,128)(2,1)} %copy-done.34, bf16[8,80,512]{2,1,0:T(8,128)(2,1)} %get-tuple-element.21.refs_2_, bf16[8,512,128]{2,1,0:T(8,128)(2,1)} %get-tuple-element.22.refs_3_), custom_call_target="tpu_custom_call" | custom-call | flops 10000000000 | bytes 2000000 | tf_op jit(solution)/shard_map/attention/pallas_call | solution.py:224
  173.3 2.6 %collective-permute-start.12 = (bf16[2,512,128]{2,1,0:T(8,128)(2,1)}, bf16[2,512,128]{2,1,0:T(8,128)(2,1)S(1)}, u32[]{:S(2)}, u32[]{:S(2)}) collective-permute-start(bf16[2,512,128]{2,1,0:T(8,128)(2,1)} %get-tuple-element.24), channel_id=1, source_target_pairs={{0,24},{4,28},{8,0},{12,4},{16,8},{20,12},{24,16},{28,20},{32,56},... | collective-permute-start | bytes 786440 | tf_op jit(solution)/shard_map/ppermute | solution.py:599
  177.1 12.3 %attention.2 = (bf16[2,512,128]{2,1,0:T(8,128)(2,1)}, bf16[2,512,128]{2,1,0:T(8,128)(2,1)}) custom-call(s32[1]{0:T(128)} %bitcast.own_ref, bf16[2,128,256]{2,1,0:T(8,128)(2,1)} %copy-done.35, bf16[2,128,256]{2,1,0:T(8,128)(2,1)} %copy-done.23, bf16[8,80,512]{2,1,0:T(8,128)(2,1)} %get-tuple-element.21.refs_2_, bf16[8,512,128]{2,1,0:T(8,128)(2,1)} %get-tuple-element.22.refs_3_), custom_call_target="tpu_custom_call" | custom-call | flops 10000000000 | bytes 2000000 | tf_op jit(solution)/shard_map/attention/pallas_call | solution.py:224
  190.0 7.8 %collective-permute-done.13.c = bf16[2,512,128]{2,1,0:T(8,128)(2,1)S(1)} collective-permute-done((bf16[2,512,128]{2,1,0:T(8,128)(2,1)}, bf16[2,512,128]{2,1,0:T(8,128)(2,1)S(1)}, u32[]{:S(2)}, u32[]{:S(2)}) %collective-permute-start.13) | collective-permute-done | bytes 262176 | tf_op jit(solution)/shard_map/ppermute | solution.py:599
  198.5 3.4 %merge.1 = (bf16[256,128]{1,0:T(8,128)(2,1)}, bf16[256,128]{1,0:T(8,128)(2,1)}) custom-call(bf16[2,512,128]{2,1,0:T(8,128)(2,1)} %get-tuple-element.23.a, bf16[2,512,128]{2,1,0:T(8,128)(2,1)} %copy-done.16, bf16[2,512,128]{2,1,0:T(8,128)(2,1)} %copy-done.18, bf16[2,512,128]{2,1,0:T(8,128)(2,1)} %copy-done.17), custom_call_target="tpu_custom_call" | custom-call | tf_op jit(solution)/shard_map/merge/pallas_call | solution.py:260
  201.9 3.8 %collective-permute-start.15 = (bf16[256,128]{1,0:T(8,128)(2,1)}, bf16[256,128]{1,0:T(8,128)(2,1)S(1)}, u32[]{:S(2)}, u32[]{:S(2)}) collective-permute-start(bf16[256,128]{1,0:T(8,128)(2,1)} %get-tuple-element.28), channel_id=1, source_target_pairs={{0,252},{4,248},{8,244},{12,240},{16,236},{20,232},{24,228},{28,22... | collective-permute-start | bytes 196616 | tf_op jit(solution)/shard_map/ppermute | solution.py:615
  205.8 3.4 %collective-permute-done.15.back_ref = bf16[256,128]{1,0:T(8,128)(2,1)S(1)} collective-permute-done((bf16[256,128]{1,0:T(8,128)(2,1)}, bf16[256,128]{1,0:T(8,128)(2,1)S(1)}, u32[]{:S(2)}, u32[]{:S(2)}) %collective-permute-start.15) | collective-permute-done | bytes 65568 | tf_op jit(solution)/shard_map/ppermute | solution.py:615
  209.8 2.9 %project.1 = (bf16[64,2048]{1,0:T(8,128)(2,1)}, bf16[64,2048]{1,0:T(8,128)(2,1)}, bf16[64,2048]{1,0:T(8,128)(2,1)}, bf16[64,2048]{1,0:T(8,128)(2,1)}) custom-call(s32[1]{0:T(128)} %bitcast.own_ref, s32[1]{0:T(128)} %bitcast.1.tp_ref.index_ref, bf16[256,128]{1,0:T(8,128)(2,1)} %get-tuple-element.27.keep_ref, bf16[256,128]{1,0:T(8,128)(2,1)} %copy-done.26, ...), custom_call_target="tpu_custom_call" | custom-call | tf_op jit(solution)/shard_map/project/pallas_call | solution.py:282
  216.1 2.0 way_back.1.slot_ref
  218.9 2.2 collective-permute-done.16
  221.1 3.7 %collective-permute-done.17 = bf16[64,2048]{1,0:T(8,128)(2,1)S(1)} collective-permute-done((bf16[64,2048]{1,0:T(8,128)(2,1)}, bf16[64,2048]{1,0:T(8,128)(2,1)S(1)}, u32[]{:S(2)}, u32[]{:S(2)}) %collective-permute-start.17) | collective-permute-done | bytes 262176 | tf_op jit(solution)/shard_map/ppermute | solution.py:618
  224.8 2.2 collective-permute-done.18
  228.9 2.8 %combine.1 = bf16[256,512]{1,0:T(8,128)(2,1)} custom-call(s32[256,2]{1,0:T(8,128)} %way_back.1.slot_ref, f32[256,2]{1,0:T(8,128)} %copy.15.weight_ref, bf16[1024,512]{1,0:T(8,128)(2,1)} %bitcast.20), custom_call_target="tpu_custom_call" | custom-call | tf_op jit(solution)/shard_map/combine/pallas_call | solution.py:517
  (126 shorter events, 32.3 us)
Async XLA Ops:
  45.0 25.0 %copy-start.3 = (bf16[64,16,512]{2,1,0:T(8,128)(2,1)}, bf16[64,16,512]{2,1,0:T(8,128)(2,1)S(1)}, u32[]{:S(2)}) copy-start(bf16[64,16,512]{2,1,0:T(8,128)(2,1)S(1)} %all_to_all.10) | copy-start | bytes 3145732
  45.0 24.8 %collective-permute-start.19 = (bf16[1024,512]{1,0:T(8,128)(2,1)S(1)}, bf16[1024,512]{1,0:T(8,128)(2,1)S(1)}, u32[]{:S(2)}, u32[]{:S(2)}) collective-permute-start(bf16[1024,512]{1,0:T(8,128)(2,1)S(1)} %bitcast.21), channel_id=1, source_target_pairs={{0,1},{1,2},{2,3},{3,0},{4,5},{5,6},{6,7},{7,4},{8,9},{9,10},{10,1... | collective-permute-start | bytes 3145736 | tf_op jit(solution)/shard_map/ppermute | solution.py:553
  46.2 23.7 %collective-permute-start.20 = (bf16[1024,512]{1,0:T(8,128)(2,1)S(1)}, bf16[1024,512]{1,0:T(8,128)(2,1)S(1)}, u32[]{:S(2)}, u32[]{:S(2)}) collective-permute-start(bf16[1024,512]{1,0:T(8,128)(2,1)S(1)} %bitcast.22), channel_id=1, source_target_pairs={{0,3},{1,0},{2,1},{3,2},{4,7},{5,4},{6,5},{7,6},{8,11},{9,8},{10,9... | collective-permute-start | bytes 3145736 | tf_op jit(solution)/shard_map/ppermute | solution.py:553
  69.8 12.8 %collective-permute-start.21 = (bf16[512,512]{1,0:T(8,128)(2,1)S(1)}, bf16[512,512]{1,0:T(8,128)(2,1)S(1)}, u32[]{:S(2)}, u32[]{:S(2)}) collective-permute-start(bf16[512,512]{1,0:T(8,128)(2,1)S(1)} %slice.34), channel_id=1, source_target_pairs={{0,1},{1,2},{2,3},{3,0},{4,5},{5,6},{6,7},{7,4},{8,9},{9,10},{10,1... | collective-permute-start | bytes 1572872 | tf_op jit(solution)/shard_map/ppermute | solution.py:558
  70.0 12.6 %collective-permute-start.22 = (bf16[512,512]{1,0:T(8,128)(2,1)S(1)}, bf16[512,512]{1,0:T(8,128)(2,1)S(1)}, u32[]{:S(2)}, u32[]{:S(2)}) collective-permute-start(bf16[512,512]{1,0:T(8,128)(2,1)S(1)} %slice.35), channel_id=1, source_target_pairs={{0,3},{1,0},{2,1},{3,2},{4,7},{5,4},{6,5},{7,6},{8,11},{9,8},{10,9... | collective-permute-start | bytes 1572872 | tf_op jit(solution)/shard_map/ppermute | solution.py:558
  89.9 24.1 %collective-permute-start.23 = (bf16[1024,256]{1,0:T(8,128)(2,1)}, bf16[1024,256]{1,0:T(8,128)(2,1)S(1)}, u32[]{:S(2)}, u32[]{:S(2)}) collective-permute-start(bf16[1024,256]{1,0:T(8,128)(2,1)} %up_projections.1.a), channel_id=1, source_target_pairs={{0,1},{1,2},{2,3},{3,0},{4,5},{5,6},{6,7},{7,4},{8,9},{9,10},{10,1... | collective-permute-start | bytes 1572872 | tf_op jit(solution)/shard_map/ppermute | solution.py:553
  89.9 24.1 %collective-permute-start.24 = (bf16[1024,256]{1,0:T(8,128)(2,1)}, bf16[1024,256]{1,0:T(8,128)(2,1)S(1)}, u32[]{:S(2)}, u32[]{:S(2)}) collective-permute-start(bf16[1024,256]{1,0:T(8,128)(2,1)} %up_projections.1.a), channel_id=1, source_target_pairs={{0,3},{1,0},{2,1},{3,2},{4,7},{5,4},{6,5},{7,6},{8,11},{9,8},{10,9... | collective-permute-start | bytes 1572872 | tf_op jit(solution)/shard_map/ppermute | solution.py:553
  94.6 15.5 %collective-permute-start.27 = (bf16[256,512]{1,0:T(8,128)(2,1)}, bf16[256,512]{1,0:T(8,128)(2,1)S(1)}, u32[]{:S(2)}, u32[]{:S(2)}) collective-permute-start(bf16[256,512]{1,0:T(8,128)(2,1)} %get-tuple-element.33), channel_id=1, source_target_pairs={{0,1},{1,2},{2,3},{3,0},{4,5},{5,6},{6,7},{7,4},{8,9},{9,10},{10,1... | collective-permute-start | bytes 786440 | tf_op jit(solution)/shard_map/ppermute | solution.py:583
  96.5 11.2 %collective-permute-start = (bf16[272,256]{1,0:T(8,128)(2,1)}, bf16[272,256]{1,0:T(8,128)(2,1)S(1)}, u32[]{:S(2)}, u32[]{:S(2)}) collective-permute-start(bf16[272,256]{1,0:T(8,128)(2,1)} %get-tuple-element.20), channel_id=1, source_target_pairs={{0,252},{4,248},{8,244},{12,240},{16,236},{20,232},{24,228},{28,22... | collective-permute-start | bytes 417800 | tf_op jit(solution)/shard_map/ppermute | solution.py:561
  102.4 14.4 %collective-permute-start.28 = (bf16[256,512]{1,0:T(8,128)(2,1)S(1)}, bf16[256,512]{1,0:T(8,128)(2,1)S(1)}, u32[]{:S(2)}, u32[]{:S(2)}) collective-permute-start(bf16[256,512]{1,0:T(8,128)(2,1)S(1)} %copy-done.32), channel_id=1, source_target_pairs={{0,3},{1,0},{2,1},{3,2},{4,7},{5,4},{6,5},{7,6},{8,11},{9,8},{10,9... | collective-permute-start | bytes 786440 | tf_op jit(solution)/shard_map/ppermute | solution.py:583
  108.6 10.1 %collective-permute-start.4 = (bf16[2,144,256]{2,1,0:T(8,128)(2,1)S(1)}, bf16[2,144,256]{2,1,0:T(8,128)(2,1)S(1)}, u32[]{:S(2)}, u32[]{:S(2)}) collective-permute-start(bf16[2,144,256]{2,1,0:T(8,128)(2,1)S(1)} %pad_maximum_fusion.refs_0_), channel_id=1, source_target_pairs={{0,64},{4,68},{8,72},{12,76},{16,80},{20,84},{24,88},{28,92},{32,9... | collective-permute-start | bytes 442376 | tf_op jit(solution)/shard_map/ppermute | solution.py:572
  110.1 9.5 %collective-permute-start.5 = (bf16[2,144,256]{2,1,0:T(8,128)(2,1)S(1)}, bf16[2,144,256]{2,1,0:T(8,128)(2,1)S(1)}, u32[]{:S(2)}, u32[]{:S(2)}) collective-permute-start(bf16[2,144,256]{2,1,0:T(8,128)(2,1)S(1)} %pad_maximum_fusion.refs_0_), channel_id=1, source_target_pairs={{0,192},{4,196},{8,200},{12,204},{16,208},{20,212},{24,216},{28,22... | collective-permute-start | bytes 442376 | tf_op jit(solution)/shard_map/ppermute | solution.py:572
  114.0 8.3 %collective-permute-start.2 = (bf16[2,144,256]{2,1,0:T(8,128)(2,1)S(1)}, bf16[2,144,256]{2,1,0:T(8,128)(2,1)S(1)}, u32[]{:S(2)}, u32[]{:S(2)}) collective-permute-start(bf16[2,144,256]{2,1,0:T(8,128)(2,1)S(1)} %pad_maximum_fusion.refs_0_), channel_id=1, source_target_pairs={{0,32},{4,36},{8,40},{12,44},{16,48},{20,52},{24,56},{28,60},{32,6... | collective-permute-start | bytes 442376 | tf_op jit(solution)/shard_map/ppermute | solution.py:572
  114.1 8.7 %collective-permute-start.3 = (bf16[2,144,256]{2,1,0:T(8,128)(2,1)S(1)}, bf16[2,144,256]{2,1,0:T(8,128)(2,1)S(1)}, u32[]{:S(2)}, u32[]{:S(2)}) collective-permute-start(bf16[2,144,256]{2,1,0:T(8,128)(2,1)S(1)} %pad_maximum_fusion.refs_0_), channel_id=1, source_target_pairs={{0,224},{4,228},{8,232},{12,236},{16,240},{20,244},{24,248},{28,25... | collective-permute-start | bytes 442376 | tf_op jit(solution)/shard_map/ppermute | solution.py:572
  117.7 22.9 %collective-permute-start.29 = (bf16[256,512]{1,0:T(8,128)(2,1)S(1)}, bf16[256,512]{1,0:T(8,128)(2,1)S(1)}, u32[]{:S(2)}, u32[]{:S(2)}) collective-permute-start(bf16[256,512]{1,0:T(8,128)(2,1)S(1)} %copy-done.31), channel_id=1, source_target_pairs={{0,2},{1,3},{2,0},{3,1},{4,6},{5,7},{6,4},{7,5},{8,10},{9,11},{10,... | collective-permute-start | bytes 786440 | tf_op jit(solution)/shard_map/ppermute | solution.py:583
  118.7 22.7 %collective-permute-start.25 = (bf16[512,256]{1,0:T(8,128)(2,1)S(1)}, bf16[512,256]{1,0:T(8,128)(2,1)S(1)}, u32[]{:S(2)}, u32[]{:S(2)}) collective-permute-start(bf16[512,256]{1,0:T(8,128)(2,1)S(1)} %slice.36), channel_id=1, source_target_pairs={{0,1},{1,2},{2,3},{3,0},{4,5},{5,6},{6,7},{7,4},{8,9},{9,10},{10,1... | collective-permute-start | bytes 786440 | tf_op jit(solution)/shard_map/ppermute | solution.py:558
  119.6 21.8 %collective-permute-start.26 = (bf16[512,256]{1,0:T(8,128)(2,1)S(1)}, bf16[512,256]{1,0:T(8,128)(2,1)S(1)}, u32[]{:S(2)}, u32[]{:S(2)}) collective-permute-start(bf16[512,256]{1,0:T(8,128)(2,1)S(1)} %slice.37), channel_id=1, source_target_pairs={{0,3},{1,0},{2,1},{3,2},{4,7},{5,4},{6,5},{7,6},{8,11},{9,8},{10,9... | collective-permute-start | bytes 786440 | tf_op jit(solution)/shard_map/ppermute | solution.py:558
  122.3 5.6 %collective-permute-start.8 = (bf16[1,144,256]{2,1,0:T(8,128)(2,1)S(1)}, bf16[1,144,256]{2,1,0:T(8,128)(2,1)S(1)}, u32[]{:S(2)}, u32[]{:S(2)}) collective-permute-start(bf16[1,144,256]{2,1,0:T(8,128)(2,1)S(1)} %slice.32), channel_id=1, source_target_pairs={{0,64},{4,68},{8,72},{12,76},{16,80},{20,84},{24,88},{28,92},{32,9... | collective-permute-start | bytes 221192 | tf_op jit(solution)/shard_map/ppermute | solution.py:576
  122.8 5.4 %collective-permute-start.9 = (bf16[1,144,256]{2,1,0:T(8,128)(2,1)S(1)}, bf16[1,144,256]{2,1,0:T(8,128)(2,1)S(1)}, u32[]{:S(2)}, u32[]{:S(2)}) collective-permute-start(bf16[1,144,256]{2,1,0:T(8,128)(2,1)S(1)} %slice.33), channel_id=1, source_target_pairs={{0,192},{4,196},{8,200},{12,204},{16,208},{20,212},{24,216},{28,22... | collective-permute-start | bytes 221192 | tf_op jit(solution)/shard_map/ppermute | solution.py:577
  127.9 6.2 %collective-permute-start.6 = (bf16[2,144,256]{2,1,0:T(8,128)(2,1)S(1)}, bf16[2,144,256]{2,1,0:T(8,128)(2,1)S(1)}, u32[]{:S(2)}, u32[]{:S(2)}) collective-permute-start(bf16[2,144,256]{2,1,0:T(8,128)(2,1)S(1)} %collective-permute-done.4.refs_3_), channel_id=1, source_target_pairs={{0,32},{4,36},{8,40},{12,44},{16,48},{20,52},{24,56},{28,60},{32,6... | collective-permute-start | bytes 442376 | tf_op jit(solution)/shard_map/ppermute | solution.py:574
  128.2 7.5 %collective-permute-start.7 = (bf16[2,144,256]{2,1,0:T(8,128)(2,1)S(1)}, bf16[2,144,256]{2,1,0:T(8,128)(2,1)S(1)}, u32[]{:S(2)}, u32[]{:S(2)}) collective-permute-start(bf16[2,144,256]{2,1,0:T(8,128)(2,1)S(1)} %collective-permute-done.5.refs_4_), channel_id=1, source_target_pairs={{0,224},{4,228},{8,232},{12,236},{16,240},{20,244},{24,248},{28,25... | collective-permute-start | bytes 442376 | tf_op jit(solution)/shard_map/ppermute | solution.py:575
  134.1 26.1 %collective-permute-start.10 = (bf16[2,128,256]{2,1,0:T(8,128)(2,1)S(1)}, bf16[2,128,256]{2,1,0:T(8,128)(2,1)S(1)}, u32[]{:S(2)}, u32[]{:S(2)}) collective-permute-start(bf16[2,128,256]{2,1,0:T(8,128)(2,1)S(1)} %pad_maximum_fusion.1.refs_1_), channel_id=1, source_target_pairs={{0,16},{4,20},{8,24},{12,28},{16,0},{20,4},{24,8},{28,12},{32,48},... | collective-permute-start | bytes 393224 | tf_op jit(solution)/shard_map/ppermute | solution.py:569
  135.8 24.4 %collective-permute-start.11 = (bf16[2,128,256]{2,1,0:T(8,128)(2,1)S(1)}, bf16[2,128,256]{2,1,0:T(8,128)(2,1)S(1)}, u32[]{:S(2)}, u32[]{:S(2)}) collective-permute-start(bf16[2,128,256]{2,1,0:T(8,128)(2,1)S(1)} %pad_maximum_fusion.1.refs_1_), channel_id=1, source_target_pairs={{0,8},{4,12},{8,16},{12,20},{16,24},{20,28},{24,0},{28,4},{32,40},... | collective-permute-start | bytes 393224 | tf_op jit(solution)/shard_map/ppermute | solution.py:569
  140.6 35.9 %collective-permute-start.1 = (bf16[2,128,256]{2,1,0:T(8,128)(2,1)S(1)}, bf16[2,128,256]{2,1,0:T(8,128)(2,1)S(1)}, u32[]{:S(2)}, u32[]{:S(2)}) collective-permute-start(bf16[2,128,256]{2,1,0:T(8,128)(2,1)S(1)} %pad_maximum_fusion.1.refs_1_), channel_id=1, source_target_pairs={{0,24},{4,28},{8,0},{12,4},{16,8},{20,12},{24,16},{28,20},{32,56},... | collective-permute-start | bytes 393224 | tf_op jit(solution)/shard_map/ppermute | solution.py:569
  147.8 80.0 %all-to-all-start.1 = ((bf16[64,16,512]{2,1,0:T(8,128)(2,1)}), bf16[64,16,512]{2,1,0:T(8,128)(2,1)S(1)}, u32[]{:S(2)}, u32[]{:S(2)}) async-start(bf16[64,16,512]{2,1,0:T(8,128)(2,1)} %bitcast.18), calls=%async_computation.1 | async-start | bytes 2097152 | tf_op jit(solution)/shard_map/all_to_all | solution.py:547
  173.3 16.7 %collective-permute-start.12 = (bf16[2,512,128]{2,1,0:T(8,128)(2,1)}, bf16[2,512,128]{2,1,0:T(8,128)(2,1)S(1)}, u32[]{:S(2)}, u32[]{:S(2)}) collective-permute-start(bf16[2,512,128]{2,1,0:T(8,128)(2,1)} %get-tuple-element.24), channel_id=1, source_target_pairs={{0,24},{4,28},{8,0},{12,4},{16,8},{20,12},{24,16},{28,20},{32,56},... | collective-permute-start | bytes 786440 | tf_op jit(solution)/shard_map/ppermute | solution.py:599
  175.9 14.1 %collective-permute-start.14 = (bf16[2,512,128]{2,1,0:T(8,128)(2,1)}, bf16[2,512,128]{2,1,0:T(8,128)(2,1)S(1)}, u32[]{:S(2)}, u32[]{:S(2)}) collective-permute-start(bf16[2,512,128]{2,1,0:T(8,128)(2,1)} %get-tuple-element.26), channel_id=1, source_target_pairs={{0,16},{4,20},{8,24},{12,28},{16,0},{20,4},{24,8},{28,12},{32,48},... | collective-permute-start | bytes 786440 | tf_op jit(solution)/shard_map/ppermute | solution.py:599
  189.4 8.4 %collective-permute-start.13 = (bf16[2,512,128]{2,1,0:T(8,128)(2,1)}, bf16[2,512,128]{2,1,0:T(8,128)(2,1)S(1)}, u32[]{:S(2)}, u32[]{:S(2)}) collective-permute-start(bf16[2,512,128]{2,1,0:T(8,128)(2,1)} %get-tuple-element.25), channel_id=1, source_target_pairs={{0,8},{4,12},{8,16},{12,20},{16,24},{20,28},{24,0},{28,4},{32,40},... | collective-permute-start | bytes 786440 | tf_op jit(solution)/shard_map/ppermute | solution.py:599
  201.9 7.2 %collective-permute-start.15 = (bf16[256,128]{1,0:T(8,128)(2,1)}, bf16[256,128]{1,0:T(8,128)(2,1)S(1)}, u32[]{:S(2)}, u32[]{:S(2)}) collective-permute-start(bf16[256,128]{1,0:T(8,128)(2,1)} %get-tuple-element.28), channel_id=1, source_target_pairs={{0,252},{4,248},{8,244},{12,240},{16,236},{20,232},{24,228},{28,22... | collective-permute-start | bytes 196616 | tf_op jit(solution)/shard_map/ppermute | solution.py:615
  212.6 8.5 %collective-permute-start.16 = (bf16[64,2048]{1,0:T(8,128)(2,1)}, bf16[64,2048]{1,0:T(8,128)(2,1)S(1)}, u32[]{:S(2)}, u32[]{:S(2)}) collective-permute-start(bf16[64,2048]{1,0:T(8,128)(2,1)} %get-tuple-element.30), channel_id=1, source_target_pairs={{0,1},{1,2},{2,3},{3,0},{4,5},{5,6},{6,7},{7,4},{8,9},{9,10},{10,1... | collective-permute-start | bytes 786440 | tf_op jit(solution)/shard_map/ppermute | solution.py:618
  212.6 12.2 %collective-permute-start.17 = (bf16[64,2048]{1,0:T(8,128)(2,1)}, bf16[64,2048]{1,0:T(8,128)(2,1)S(1)}, u32[]{:S(2)}, u32[]{:S(2)}) collective-permute-start(bf16[64,2048]{1,0:T(8,128)(2,1)} %get-tuple-element.31), channel_id=1, source_target_pairs={{0,2},{1,3},{2,0},{3,1},{4,6},{5,7},{6,4},{7,5},{8,10},{9,11},{10,... | collective-permute-start | bytes 786440 | tf_op jit(solution)/shard_map/ppermute | solution.py:618
  214.3 12.7 %collective-permute-start.18 = (bf16[64,2048]{1,0:T(8,128)(2,1)}, bf16[64,2048]{1,0:T(8,128)(2,1)S(1)}, u32[]{:S(2)}, u32[]{:S(2)}) collective-permute-start(bf16[64,2048]{1,0:T(8,128)(2,1)} %get-tuple-element.32), channel_id=1, source_target_pairs={{0,3},{1,0},{2,1},{3,2},{4,7},{5,4},{6,5},{7,6},{8,11},{9,8},{10,9... | collective-permute-start | bytes 786440 | tf_op jit(solution)/shard_map/ppermute | solution.py:618
  (35 other events, 219.7 us)

commit v4 on v3

--- a/solution.py
+++ b/solution.py
@@ -151,19 +151,27 @@
     def run_half(high, carry):
         count = jnp.where(high == 1, 7 - low, low)
         slot = jnp.where(count == z, 0, 1)
-        for block in blocks:
-            at = pl.ds(block, TALL)
+        owns = [2 * lax.rem(y + shift + 4, 4) + core for shift in steps]
+        owns = [jnp.where(slot == 0, own, 7 - own) for own in owns]
+
+        def own_slab(block, carry):
+            at = pl.ds(pl.multiple_of(block * 2 * rows, 2 * rows), 2 * rows)
             scores = jnp.dot(query_ref[slot, at, :], key_ref[count], preferred_element_type=F32)
             lane = lax.broadcasted_iota(jnp.int32, scores.shape, 1)
             key_at = lane + jnp.where(lane < rows, offset * rows, (7 - offset) * rows - rows)
-            row = block + lax.broadcasted_iota(jnp.int32, scores.shape, 0)
-            owns = [2 * lax.rem(y + shift + 4, 4) + core for shift in steps]
-            owns = [jnp.where(slot == 0, own, 7 - own) for own in owns]
-            own = jnp.where(row < 2 * rows, owns[0], owns[-1])
-            scores = jnp.where(key_at <= own * rows + row % rows, scores, MASKED)
+            own = owns[0]
+            for number in range(1, count_y):
+                own = jnp.where(block < number, own, owns[number])
+            row = lax.broadcasted_iota(jnp.int32, scores.shape, 0)
+            query_at = own * rows + jnp.where(row < rows, row, row - rows)
+            scores = jnp.where(key_at <= query_at, scores, MASKED)
             score_ref[0, at, :] = scores
-            max_ref[at, :] = jnp.broadcast_to(jnp.max(scores, axis=1, keepdims=True), (TALL, 128))
-            acc_ref[at, :] = jnp.zeros((TALL, 128), F32)
+            top = jnp.max(scores, axis=1, keepdims=True)
+            max_ref[at, :] = jnp.broadcast_to(top, (2 * rows, 128))
+            acc_ref[at, :] = jnp.zeros((2 * rows, 128), F32)
+            return carry
+
+        lax.fori_loop(0, count_y, own_slab, 0)
 
         def add_slab(slab, held, block):
             at = pl.ds(block, TALL)
@@ -187,13 +195,16 @@
 
             @pl.when(functools.reduce(jnp.maximum, peaks) > 60.0)
             def _():
-                for block in blocks:
-                    at = pl.ds(block, TALL)
+                def raise_rows(block, carry):
+                    at = pl.ds(pl.multiple_of(block * rows, rows), rows)
                     old = max_ref[at, :]
                     top = jnp.max(score_ref[1 - held, at, :], axis=1, keepdims=True)
                     new = jnp.maximum(old, top)
                     acc_ref[at, :] = acc_ref[at, :] * jnp.exp(old - new)
                     max_ref[at, :] = new
+                    return carry
+
+                lax.fori_loop(0, 2 * count_y, raise_rows, 0)
 
             return carry
 
@@ -383,18 +394,6 @@
     )(experts)
 
 
-def pick_parts(index_ref, refs, steps):
-    own, previous, following, far_low, far_high = refs
-    low = pl.program_id(0) < steps // 2
-    tp = index_ref[0]
-    return (
-        (tp, own[...]),
-        (lax.rem(tp + 3, 4), previous[...]),
-        (lax.rem(tp + 1, 4), following[...]),
-        (lax.rem(tp + 2, 4), jnp.where(low, far_low[...], far_high[...])),
-    )
-
-
 def part_specs(tall, wide, steps):
     block = tall // steps
     half = steps // 2
@@ -408,9 +407,15 @@
     ]
 
 
-def up_body(index_ref, a, b, c, d, e, gate_ref, up_ref, out_ref, *, steps):
+def up_body(index_ref, own_ref, *refs, steps):
+    halves, (gate_ref, up_ref, out_ref) = refs[:6], refs[6:]
+    low = pl.program_id(0) < steps // 2
+    parts = [(index_ref[0], own_ref[...])]
+    for number, shift in enumerate((3, 1, 2)):
+        rows = jnp.where(low, halves[2 * number][...], halves[2 * number + 1][...])
+        parts.append((lax.rem(index_ref[0] + shift, 4), rows))
     gate = up = None
-    for number, rows in pick_parts(index_ref, (a, b, c, d, e), steps):
+    for number, rows in parts:
         to_gate = jnp.dot(rows, gate_ref[number], preferred_element_type=F32)
         to_up = jnp.dot(rows, up_ref[number], preferred_element_type=F32)
         gate = to_gate if gate is None else gate + to_gate
@@ -427,7 +432,8 @@
         grid_spec=pltpu.PrefetchScalarGridSpec(
             num_scalar_prefetch=1,
             grid=(steps,),
-            in_specs=part_specs(tall, wide, steps)
+            in_specs=part_specs(tall, wide, steps)[:1]
+            + part_specs(tall, wide, steps)[3:] * 3
             + [whole((tp, wide, hidden)), whole((tp, wide, hidden))],
             out_specs=pl.BlockSpec((tall // steps, hidden), lambda s, own: (s, 0)),
         ),
@@ -583,8 +589,19 @@
         lax.ppermute(cut, "tp", ring) for cut, ring in zip(cuts, (up_ring, down_ring, far_ring))
     ]
     slots = way_back(experts, size)
-    x_near = [near(rows) for rows in arrived]
-    x_far = [far(pair) for pair in x_near]
+    x_parts = []
+    for rows in arrived:
+        half = rows.shape[0] // 2
+        low, high = lax.optimization_barrier((rows[:half], rows[half:]))
+        previous_low = lax.ppermute(low, "tp", up_ring)
+        following_high = lax.ppermute(high, "tp", down_ring)
+        previous_high = lax.ppermute(high, "tp", up_ring)
+        following_low = lax.ppermute(low, "tp", down_ring)
+        far_low = lax.ppermute(previous_low, "tp", up_ring)
+        far_high = lax.ppermute(following_high, "tp", down_ring)
+        x_parts.append(
+            (rows, previous_low, previous_high, following_low, following_high, far_low, far_high)
+        )
     partial = {}
     for picks in ((3, 1), (2, 0)):
         done = attention(
@@ -603,7 +620,7 @@
         hidden.append(
             up_projections(
                 tp_index,
-                (arrived[number],) + x_near[number] + x_far[number],
+                x_parts[number],
                 w_gate[0],
                 w_up[0],
                 tp,

time: 234 us -> 234 us (level)
  waiting for transfers between devices: 59.9 us -> 57.2 us
    ppermute x0 -> x6, waiting for transfers between devices: none -> 28 us  [the longest x1 11.2 us: per_device(): far_low = lax.ppermute(previous_low, 'tp', up_ring)]
    ppermute x4 -> x2, waiting for transfers between devices: 22.1 us -> 0.01 us  [near(): return (lax.ppermute(x, 'tp', up_ring), lax.ppermute(x, 'tp', down_ring))]
    ppermute x2 -> x1, waiting for transfers between devices: 9.88 us -> 0.01 us  [far(): lax.ppermute(low, 'tp', up_ring)]
    ppermute x0 -> x6, starting transfers between devices: none -> 8.02 us  [the longest x1 2.67 us: per_device(): following_low = lax.ppermute(low, 'tp', down_ring)]
    ppermute x2 -> x1, starting transfers between devices: 4.49 us -> 1.37 us  [far(): lax.ppermute(high, 'tp', down_ring)]
    ppermute x4 -> x2, starting transfers between devices: 5.35 us -> 2.68 us  [near(): return (lax.ppermute(x, 'tp', up_ring), lax.ppermute(x, 'tp', down_ring))]
    unnamed x74 -> x78, local copies, waits for them, and re-layouts: 8.58 us -> 10.1 us
  transfers between devices with their start and end apart: 31 -> 33, of which waited for: 12 -> 13; matrix products, arithmetic and copies ran while one was open for 1% -> 1% of each run, Pallas kernels for 19% -> 20%
where the time goes in v4:
time: 234 us; the launch traced here: 231 us
  starting transfers between devices  61.6 us (26%)
  Pallas kernels  58.2 us (25%)
  waiting for transfers between devices  57.2 us (24%)
  blocking collectives  41.3 us (18%)
  local copies, waits for them, and re-layouts  10.2 us (4%)
    all_to_all x1, blocking collectives, over_ep(): lax.all_to_all(x.reshape(size, -1, wide), 'ep', split_axis=0, concat_axis...  41.3 us
    pallas_call x2, Pallas kernels, attention(): pl.pallas_call(functools.partial(attention_body, steps=steps), grid_spec=...  25.8 us
    ppermute x1, waiting for transfers between devices, per_device(): far_low = lax.ppermute(previous_low, 'tp', up_ring)  11.2 us
    all_to_all x1, starting transfers between devices, over_ep(): lax.all_to_all(x.reshape(size, -1, wide), 'ep', split_axis=0, concat_axis...  10.9 us
    unnamed x78, local copies, waits for them, and re-layouts  10.1 us
    ppermute x1, waiting for transfers between devices, per_device(): previous_high = lax.ppermute(high, 'tp', up_ring)  8.55 us
    ppermute x1, waiting for transfers between devices, per_device(): previous_low = lax.ppermute(low, 'tp', up_ring)  8.19 us
    ppermute x4, starting transfers between devices, per_device(): lax.ppermute(own_keys, 'ep', along_z(shift, size))  8 us
  transfers between devices with their start and end apart: 33, of which 13 were waited for; matrix products, arithmetic and copies ran while one was open for 1% of the time, Pallas kernels for 20%

profile of v4, /device:TPU:1, one launch (start us, length us, event | category | flops | bytes accessed | tf_op | source)
XLA Modules:
  0.0 231.2 jit_solution(2683752308256584327)
XLA Ops:
  0.6 3.1 %dispatch.1 = bf16[1024,512]{1,0:T(8,128)(2,1)} custom-call(s32[1]{0:T(128)} %bitcast.1.tp_ref.index_ref, bf16[256,2048]{1,0:T(8,128)(2,1)} %part_ref.1, bf16[256,2048]{1,0:T(8,128)(2,1)} %part_ref.1, f32[1,2048]{1,0:T(1,128)} %bitcast.32, s32[2,256]{1,0:T(2,128)} %bitcast.33), custom_call_target="tpu_custom_call" | custom-call | tf_op jit(solution)/shard_map/dispatch/pallas_call | solution.py:352
  3.7 41.3 %all_to_all.10 = bf16[64,16,512]{2,1,0:T(8,128)(2,1)S(1)} all-to-all(bf16[64,16,512]{2,1,0:T(8,128)(2,1)} %bitcast.21), channel_id=1, replica_groups=mesh['ep'=64,'tp'=4] {'ep'}, dimensions={0} | all-to-all | bytes 2097152 | tf_op jit(solution)/shard_map/all_to_all | solution.py:553
  48.7 2.7 %collective-permute-start.21 = (bf16[512,512]{1,0:T(8,128)(2,1)S(1)}, bf16[512,512]{1,0:T(8,128)(2,1)S(1)}, u32[]{:S(2)}, u32[]{:S(2)}) collective-permute-start(bf16[512,512]{1,0:T(8,128)(2,1)S(1)} %bitcast.29), channel_id=1, source_target_pairs={{0,3},{1,0},{2,1},{3,2},{4,7},{5,4},{6,5},{7,6},{8,11},{9,8},{10,9... | collective-permute-start | bytes 1572872 | tf_op jit(solution)/shard_map/ppermute | solution.py:599
  51.4 8.2 %collective-permute-done.19.refs_0_ = bf16[512,512]{1,0:T(8,128)(2,1)S(1)} collective-permute-done((bf16[512,512]{1,0:T(8,128)(2,1)S(1)}, bf16[512,512]{1,0:T(8,128)(2,1)S(1)}, u32[]{:S(2)}, u32[]{:S(2)}) %collective-permute-start.19) | collective-permute-done | bytes 524320 | tf_op jit(solution)/shard_map/ppermute | solution.py:596
  59.6 2.7 %collective-permute-start.24 = (bf16[512,512]{1,0:T(8,128)(2,1)S(1)}, bf16[512,512]{1,0:T(8,128)(2,1)S(1)}, u32[]{:S(2)}, u32[]{:S(2)}) collective-permute-start(bf16[512,512]{1,0:T(8,128)(2,1)S(1)} %collective-permute-done.22.refs_3_), channel_id=1, source_target_pairs={{0,3},{1,0},{2,1},{3,2},{4,7},{5,4},{6,5},{7,6},{8,11},{9,8},{10,9... | collective-permute-start | bytes 1572872 | tf_op jit(solution)/shard_map/ppermute | solution.py:601
  62.2 8.5 %collective-permute-done.20.refs_1_ = bf16[512,512]{1,0:T(8,128)(2,1)S(1)} collective-permute-done((bf16[512,512]{1,0:T(8,128)(2,1)S(1)}, bf16[512,512]{1,0:T(8,128)(2,1)S(1)}, u32[]{:S(2)}, u32[]{:S(2)}) %collective-permute-start.20) | collective-permute-done | bytes 524320 | tf_op jit(solution)/shard_map/ppermute | solution.py:598
  70.8 11.2 %collective-permute-done.23.refs_4_ = bf16[512,512]{1,0:T(8,128)(2,1)S(1)} collective-permute-done((bf16[512,512]{1,0:T(8,128)(2,1)S(1)}, bf16[512,512]{1,0:T(8,128)(2,1)S(1)}, u32[]{:S(2)}, u32[]{:S(2)}) %collective-permute-start.23) | collective-permute-done | bytes 524320 | tf_op jit(solution)/shard_map/ppermute | solution.py:600
  83.0 6.5 %up_projections.1.a = bf16[1024,256]{1,0:T(8,128)(2,1)} custom-call(s32[1]{0:T(128)} %bitcast.1.tp_ref.index_ref, bf16[1024,512]{1,0:T(8,128)(2,1)} %bitcast.23, bf16[512,512]{1,0:T(8,128)(2,1)} %copy-done.27, bf16[512,512]{1,0:T(8,128)(2,1)} %copy-done.29, bf16[512,512]{1,0:T(8,128)(2,1)} %copy-done.30, bf16[512,512]{1,0:T(8,128)(2,1)} %copy-done.28, ...), custom_call_target="tpu_custom_call" | custom-call | flops 2200000000 | bytes 6800000 | tf_op jit(solution)/shard_map/up_projections/pallas_call | solution.py:430
  96.1 4.3 %collective-permute-start = (bf16[272,256]{1,0:T(8,128)(2,1)}, bf16[272,256]{1,0:T(8,128)(2,1)S(1)}, u32[]{:S(2)}, u32[]{:S(2)}) collective-permute-start(bf16[272,256]{1,0:T(8,128)(2,1)} %get-tuple-element.22), channel_id=1, source_target_pairs={{0,252},{4,248},{8,244},{12,240},{16,236},{20,232},{24,228},{28,22... | collective-permute-start | bytes 417800 | tf_op jit(solution)/shard_map/ppermute | solution.py:567
  100.4 2.9 %collective-permute-start.30 = (bf16[256,512]{1,0:T(8,128)(2,1)S(1)}, bf16[256,512]{1,0:T(8,128)(2,1)S(1)}, u32[]{:S(2)}, u32[]{:S(2)}) collective-permute-start(bf16[256,512]{1,0:T(8,128)(2,1)S(1)} %copy-done.34), channel_id=1, source_target_pairs={{0,3},{1,0},{2,1},{3,2},{4,7},{5,4},{6,5},{7,6},{8,11},{9,8},{10,9... | collective-permute-start | bytes 786440 | tf_op jit(solution)/shard_map/ppermute | solution.py:589
  103.3 2.8 %collective-permute-done = bf16[272,256]{1,0:T(8,128)(2,1)S(1)} collective-permute-done((bf16[272,256]{1,0:T(8,128)(2,1)}, bf16[272,256]{1,0:T(8,128)(2,1)S(1)}, u32[]{:S(2)}, u32[]{:S(2)}) %collective-permute-start) | collective-permute-done | bytes 139296 | tf_op jit(solution)/shard_map/ppermute | solution.py:567
  108.1 5.2 %collective-permute-start.5 = (bf16[2,144,256]{2,1,0:T(8,128)(2,1)S(1)}, bf16[2,144,256]{2,1,0:T(8,128)(2,1)S(1)}, u32[]{:S(2)}, u32[]{:S(2)}) collective-permute-start(bf16[2,144,256]{2,1,0:T(8,128)(2,1)S(1)} %pad_maximum_fusion.refs_0_), channel_id=1, source_target_pairs={{0,192},{4,196},{8,200},{12,204},{16,208},{20,212},{24,216},{28,22... | collective-permute-start | bytes 442376 | tf_op jit(solution)/shard_map/ppermute | solution.py:578
  113.4 2.6 %collective-permute-start.3 = (bf16[2,144,256]{2,1,0:T(8,128)(2,1)S(1)}, bf16[2,144,256]{2,1,0:T(8,128)(2,1)S(1)}, u32[]{:S(2)}, u32[]{:S(2)}) collective-permute-start(bf16[2,144,256]{2,1,0:T(8,128)(2,1)S(1)} %pad_maximum_fusion.refs_0_), channel_id=1, source_target_pairs={{0,224},{4,228},{8,232},{12,236},{16,240},{20,244},{24,248},{28,25... | collective-permute-start | bytes 442376 | tf_op jit(solution)/shard_map/ppermute | solution.py:578
  120.4 2.0 collective-permute-done.2.refs_1_
  122.4 3.6 %collective-permute-start.9 = (bf16[1,144,256]{2,1,0:T(8,128)(2,1)S(1)}, bf16[1,144,256]{2,1,0:T(8,128)(2,1)S(1)}, u32[]{:S(2)}, u32[]{:S(2)}) collective-permute-start(bf16[1,144,256]{2,1,0:T(8,128)(2,1)S(1)} %slice.41), channel_id=1, source_target_pairs={{0,192},{4,196},{8,200},{12,204},{16,208},{20,212},{24,216},{28,22... | collective-permute-start | bytes 221192 | tf_op jit(solution)/shard_map/ppermute | solution.py:583
  128.1 2.9 %collective-permute-start.7 = (bf16[2,144,256]{2,1,0:T(8,128)(2,1)S(1)}, bf16[2,144,256]{2,1,0:T(8,128)(2,1)S(1)}, u32[]{:S(2)}, u32[]{:S(2)}) collective-permute-start(bf16[2,144,256]{2,1,0:T(8,128)(2,1)S(1)} %collective-permute-done.5.refs_4_), channel_id=1, source_target_pairs={{0,224},{4,228},{8,232},{12,236},{16,240},{20,244},{24,248},{28,25... | collective-permute-start | bytes 442376 | tf_op jit(solution)/shard_map/ppermute | solution.py:581
  131.1 2.6 %collective-permute-done.6.refs_5_ = bf16[2,144,256]{2,1,0:T(8,128)(2,1)S(1)} collective-permute-done((bf16[2,144,256]{2,1,0:T(8,128)(2,1)S(1)}, bf16[2,144,256]{2,1,0:T(8,128)(2,1)S(1)}, u32[]{:S(2)}, u32[]{:S(2)}) %collective-permute-start.6) | collective-permute-done | bytes 147488 | tf_op jit(solution)/shard_map/ppermute | solution.py:580
  135.8 2.8 %assemble.1 = (bf16[8,80,512]{2,1,0:T(8,128)(2,1)}, bf16[8,512,128]{2,1,0:T(8,128)(2,1)}) custom-call(s32[1]{0:T(128)} %bitcast.own_ref, bf16[2,144,256]{2,1,0:T(8,128)(2,1)} %copy-done.4, bf16[2,144,256]{2,1,0:T(8,128)(2,1)} %copy-done.17, bf16[2,144,256]{2,1,0:T(8,128)(2,1)} %copy-done.18, bf16[2,144,256]{2,1,0:T(8,128)(2,1)} %copy-done.6, ...), custom_call_target="tpu_custom_call" | custom-call | tf_op jit(solution)/shard_map/assemble/pallas_call | solution.py:116
  138.7 2.1 collective-permute-start.1
  142.2 5.0 %down_projection.1 = bf16[1024,512]{1,0:T(8,128)(2,1)} custom-call(s32[1]{0:T(128)} %bitcast.1.tp_ref.index_ref, bf16[1024,256]{1,0:T(8,128)(2,1)} %up_projections.1.a, bf16[1024,256]{1,0:T(8,128)(2,1)} %copy-done.2, bf16[1024,256]{1,0:T(8,128)(2,1)} %copy-done.3, bf16[512,256]{1,0:T(8,128)(2,1)} %copy-done.11, bf16[512,256]{1,0:T(8,128)(2,1)} %copy-done.12, ...), custom_call_target="tpu_custom_call" | custom-call | flops 1100000000 | bytes 4200000 | tf_op jit(solution)/shard_map/down_projection/pallas_call | solution.py:462
  147.2 10.9 %all-to-all-start.1 = ((bf16[64,16,512]{2,1,0:T(8,128)(2,1)}), bf16[64,16,512]{2,1,0:T(8,128)(2,1)S(1)}, u32[]{:S(2)}, u32[]{:S(2)}) async-start(bf16[64,16,512]{2,1,0:T(8,128)(2,1)} %bitcast.20), calls=%async_computation.1 | async-start | bytes 2097152 | tf_op jit(solution)/shard_map/all_to_all | solution.py:553
  158.8 13.1 %attention.3 = (bf16[2,512,128]{2,1,0:T(8,128)(2,1)}, bf16[2,512,128]{2,1,0:T(8,128)(2,1)}) custom-call(s32[1]{0:T(128)} %bitcast.own_ref, bf16[2,128,256]{2,1,0:T(8,128)(2,1)} %copy-done.35, bf16[2,128,256]{2,1,0:T(8,128)(2,1)} %copy-done.36, bf16[8,80,512]{2,1,0:T(8,128)(2,1)} %get-tuple-element.23.refs_2_, bf16[8,512,128]{2,1,0:T(8,128)(2,1)} %get-tuple-element.24.refs_3_), custom_call_target="tpu_custom_call" | custom-call | flops 10000000000 | bytes 2000000 | tf_op jit(solution)/shard_map/attention/pallas_call | solution.py:235
  172.0 2.6 %collective-permute-start.12 = (bf16[2,512,128]{2,1,0:T(8,128)(2,1)}, bf16[2,512,128]{2,1,0:T(8,128)(2,1)S(1)}, u32[]{:S(2)}, u32[]{:S(2)}) collective-permute-start(bf16[2,512,128]{2,1,0:T(8,128)(2,1)} %get-tuple-element.26), channel_id=1, source_target_pairs={{0,24},{4,28},{8,0},{12,4},{16,8},{20,12},{24,16},{28,20},{32,56},... | collective-permute-start | bytes 786440 | tf_op jit(solution)/shard_map/ppermute | solution.py:616
  175.8 12.6 %attention.2 = (bf16[2,512,128]{2,1,0:T(8,128)(2,1)}, bf16[2,512,128]{2,1,0:T(8,128)(2,1)}) custom-call(s32[1]{0:T(128)} %bitcast.own_ref, bf16[2,128,256]{2,1,0:T(8,128)(2,1)} %copy-done.37, bf16[2,128,256]{2,1,0:T(8,128)(2,1)} %copy-done.21, bf16[8,80,512]{2,1,0:T(8,128)(2,1)} %get-tuple-element.23.refs_2_, bf16[8,512,128]{2,1,0:T(8,128)(2,1)} %get-tuple-element.24.refs_3_), custom_call_target="tpu_custom_call" | custom-call | flops 10000000000 | bytes 2000000 | tf_op jit(solution)/shard_map/attention/pallas_call | solution.py:235
  189.0 7.7 %collective-permute-done.13.c = bf16[2,512,128]{2,1,0:T(8,128)(2,1)S(1)} collective-permute-done((bf16[2,512,128]{2,1,0:T(8,128)(2,1)}, bf16[2,512,128]{2,1,0:T(8,128)(2,1)S(1)}, u32[]{:S(2)}, u32[]{:S(2)}) %collective-permute-start.13) | collective-permute-done | bytes 262176 | tf_op jit(solution)/shard_map/ppermute | solution.py:616
  197.5 3.4 %merge.1 = (bf16[256,128]{1,0:T(8,128)(2,1)}, bf16[256,128]{1,0:T(8,128)(2,1)}) custom-call(bf16[2,512,128]{2,1,0:T(8,128)(2,1)} %get-tuple-element.25.a, bf16[2,512,128]{2,1,0:T(8,128)(2,1)} %copy-done.14, bf16[2,512,128]{2,1,0:T(8,128)(2,1)} %copy-done.16, bf16[2,512,128]{2,1,0:T(8,128)(2,1)} %copy-done.15), custom_call_target="tpu_custom_call" | custom-call | tf_op jit(solution)/shard_map/merge/pallas_call | solution.py:271
  200.9 3.6 %collective-permute-start.15 = (bf16[256,128]{1,0:T(8,128)(2,1)}, bf16[256,128]{1,0:T(8,128)(2,1)S(1)}, u32[]{:S(2)}, u32[]{:S(2)}) collective-permute-start(bf16[256,128]{1,0:T(8,128)(2,1)} %get-tuple-element.30), channel_id=1, source_target_pairs={{0,252},{4,248},{8,244},{12,240},{16,236},{20,232},{24,228},{28,22... | collective-permute-start | bytes 196616 | tf_op jit(solution)/shard_map/ppermute | solution.py:632
  204.5 3.6 %collective-permute-done.15.back_ref = bf16[256,128]{1,0:T(8,128)(2,1)S(1)} collective-permute-done((bf16[256,128]{1,0:T(8,128)(2,1)}, bf16[256,128]{1,0:T(8,128)(2,1)S(1)}, u32[]{:S(2)}, u32[]{:S(2)}) %collective-permute-start.15) | collective-permute-done | bytes 65568 | tf_op jit(solution)/shard_map/ppermute | solution.py:632
  208.7 2.9 %project.1 = (bf16[64,2048]{1,0:T(8,128)(2,1)}, bf16[64,2048]{1,0:T(8,128)(2,1)}, bf16[64,2048]{1,0:T(8,128)(2,1)}, bf16[64,2048]{1,0:T(8,128)(2,1)}) custom-call(s32[1]{0:T(128)} %bitcast.own_ref, s32[1]{0:T(128)} %bitcast.1.tp_ref.index_ref, bf16[256,128]{1,0:T(8,128)(2,1)} %get-tuple-element.29.keep_ref, bf16[256,128]{1,0:T(8,128)(2,1)} %copy-done.24, ...), custom_call_target="tpu_custom_call" | custom-call | tf_op jit(solution)/shard_map/project/pallas_call | solution.py:293
  219.6 4.7 %collective-permute-done.17 = bf16[64,2048]{1,0:T(8,128)(2,1)S(1)} collective-permute-done((bf16[64,2048]{1,0:T(8,128)(2,1)}, bf16[64,2048]{1,0:T(8,128)(2,1)S(1)}, u32[]{:S(2)}, u32[]{:S(2)}) %collective-permute-start.17) | collective-permute-done | bytes 262176 | tf_op jit(solution)/shard_map/ppermute | solution.py:635
  224.3 2.3 collective-permute-done.18
  228.4 2.8 %combine.1 = bf16[256,512]{1,0:T(8,128)(2,1)} custom-call(s32[256,2]{1,0:T(8,128)} %way_back.1.slot_ref, f32[256,2]{1,0:T(8,128)} %copy.15.weight_ref, bf16[1024,512]{1,0:T(8,128)(2,1)} %bitcast.22), custom_call_target="tpu_custom_call" | custom-call | tf_op jit(solution)/shard_map/combine/pallas_call | solution.py:523
  (133 shorter events, 36.9 us)
Async XLA Ops:
  46.0 13.5 %collective-permute-start.19 = (bf16[512,512]{1,0:T(8,128)(2,1)S(1)}, bf16[512,512]{1,0:T(8,128)(2,1)S(1)}, u32[]{:S(2)}, u32[]{:S(2)}) collective-permute-start(bf16[512,512]{1,0:T(8,128)(2,1)S(1)} %bitcast.28), channel_id=1, source_target_pairs={{0,1},{1,2},{2,3},{3,0},{4,5},{5,6},{6,7},{7,4},{8,9},{9,10},{10,1... | collective-permute-start | bytes 1572872 | tf_op jit(solution)/shard_map/ppermute | solution.py:596
  47.2 12.3 %collective-permute-start.22 = (bf16[512,512]{1,0:T(8,128)(2,1)S(1)}, bf16[512,512]{1,0:T(8,128)(2,1)S(1)}, u32[]{:S(2)}, u32[]{:S(2)}) collective-permute-start(bf16[512,512]{1,0:T(8,128)(2,1)S(1)} %bitcast.30), channel_id=1, source_target_pairs={{0,3},{1,0},{2,1},{3,2},{4,7},{5,4},{6,5},{7,6},{8,11},{9,8},{10,9... | collective-permute-start | bytes 1572872 | tf_op jit(solution)/shard_map/ppermute | solution.py:597
  48.7 22.1 %collective-permute-start.20 = (bf16[512,512]{1,0:T(8,128)(2,1)S(1)}, bf16[512,512]{1,0:T(8,128)(2,1)S(1)}, u32[]{:S(2)}, u32[]{:S(2)}) collective-permute-start(bf16[512,512]{1,0:T(8,128)(2,1)S(1)} %bitcast.31), channel_id=1, source_target_pairs={{0,1},{1,2},{2,3},{3,0},{4,5},{5,6},{6,7},{7,4},{8,9},{9,10},{10,1... | collective-permute-start | bytes 1572872 | tf_op jit(solution)/shard_map/ppermute | solution.py:598
  48.7 22.1 %collective-permute-start.21 = (bf16[512,512]{1,0:T(8,128)(2,1)S(1)}, bf16[512,512]{1,0:T(8,128)(2,1)S(1)}, u32[]{:S(2)}, u32[]{:S(2)}) collective-permute-start(bf16[512,512]{1,0:T(8,128)(2,1)S(1)} %bitcast.29), channel_id=1, source_target_pairs={{0,3},{1,0},{2,1},{3,2},{4,7},{5,4},{6,5},{7,6},{8,11},{9,8},{10,9... | collective-permute-start | bytes 1572872 | tf_op jit(solution)/shard_map/ppermute | solution.py:599
  59.6 22.5 %collective-permute-start.23 = (bf16[512,512]{1,0:T(8,128)(2,1)S(1)}, bf16[512,512]{1,0:T(8,128)(2,1)S(1)}, u32[]{:S(2)}, u32[]{:S(2)}) collective-permute-start(bf16[512,512]{1,0:T(8,128)(2,1)S(1)} %collective-permute-done.19.refs_0_), channel_id=1, source_target_pairs={{0,1},{1,2},{2,3},{3,0},{4,5},{5,6},{6,7},{7,4},{8,9},{9,10},{10,1... | collective-permute-start | bytes 1572872 | tf_op jit(solution)/shard_map/ppermute | solution.py:600
  59.6 22.5 %collective-permute-start.24 = (bf16[512,512]{1,0:T(8,128)(2,1)S(1)}, bf16[512,512]{1,0:T(8,128)(2,1)S(1)}, u32[]{:S(2)}, u32[]{:S(2)}) collective-permute-start(bf16[512,512]{1,0:T(8,128)(2,1)S(1)} %collective-permute-done.22.refs_3_), channel_id=1, source_target_pairs={{0,3},{1,0},{2,1},{3,2},{4,7},{5,4},{6,5},{7,6},{8,11},{9,8},{10,9... | collective-permute-start | bytes 1572872 | tf_op jit(solution)/shard_map/ppermute | solution.py:601
  89.6 23.8 %collective-permute-start.25 = (bf16[1024,256]{1,0:T(8,128)(2,1)}, bf16[1024,256]{1,0:T(8,128)(2,1)S(1)}, u32[]{:S(2)}, u32[]{:S(2)}) collective-permute-start(bf16[1024,256]{1,0:T(8,128)(2,1)} %up_projections.1.a), channel_id=1, source_target_pairs={{0,1},{1,2},{2,3},{3,0},{4,5},{5,6},{6,7},{7,4},{8,9},{9,10},{10,1... | collective-permute-start | bytes 1572872 | tf_op jit(solution)/shard_map/ppermute | solution.py:559
  90.3 23.2 %collective-permute-start.26 = (bf16[1024,256]{1,0:T(8,128)(2,1)}, bf16[1024,256]{1,0:T(8,128)(2,1)S(1)}, u32[]{:S(2)}, u32[]{:S(2)}) collective-permute-start(bf16[1024,256]{1,0:T(8,128)(2,1)} %up_projections.1.a), channel_id=1, source_target_pairs={{0,3},{1,0},{2,1},{3,2},{4,7},{5,4},{6,5},{7,6},{8,11},{9,8},{10,9... | collective-permute-start | bytes 1572872 | tf_op jit(solution)/shard_map/ppermute | solution.py:559
  94.2 13.8 %collective-permute-start.29 = (bf16[256,512]{1,0:T(8,128)(2,1)}, bf16[256,512]{1,0:T(8,128)(2,1)S(1)}, u32[]{:S(2)}, u32[]{:S(2)}) collective-permute-start(bf16[256,512]{1,0:T(8,128)(2,1)} %get-tuple-element.37), channel_id=1, source_target_pairs={{0,1},{1,2},{2,3},{3,0},{4,5},{5,6},{6,7},{7,4},{8,9},{9,10},{10,1... | collective-permute-start | bytes 786440 | tf_op jit(solution)/shard_map/ppermute | solution.py:589
  96.1 10.0 %collective-permute-start = (bf16[272,256]{1,0:T(8,128)(2,1)}, bf16[272,256]{1,0:T(8,128)(2,1)S(1)}, u32[]{:S(2)}, u32[]{:S(2)}) collective-permute-start(bf16[272,256]{1,0:T(8,128)(2,1)} %get-tuple-element.22), channel_id=1, source_target_pairs={{0,252},{4,248},{8,244},{12,240},{16,236},{20,232},{24,228},{28,22... | collective-permute-start | bytes 417800 | tf_op jit(solution)/shard_map/ppermute | solution.py:567
  100.4 15.7 %collective-permute-start.30 = (bf16[256,512]{1,0:T(8,128)(2,1)S(1)}, bf16[256,512]{1,0:T(8,128)(2,1)S(1)}, u32[]{:S(2)}, u32[]{:S(2)}) collective-permute-start(bf16[256,512]{1,0:T(8,128)(2,1)S(1)} %copy-done.34), channel_id=1, source_target_pairs={{0,3},{1,0},{2,1},{3,2},{4,7},{5,4},{6,5},{7,6},{8,11},{9,8},{10,9... | collective-permute-start | bytes 786440 | tf_op jit(solution)/shard_map/ppermute | solution.py:589
  107.0 10.7 %collective-permute-start.4 = (bf16[2,144,256]{2,1,0:T(8,128)(2,1)S(1)}, bf16[2,144,256]{2,1,0:T(8,128)(2,1)S(1)}, u32[]{:S(2)}, u32[]{:S(2)}) collective-permute-start(bf16[2,144,256]{2,1,0:T(8,128)(2,1)S(1)} %pad_maximum_fusion.refs_0_), channel_id=1, source_target_pairs={{0,64},{4,68},{8,72},{12,76},{16,80},{20,84},{24,88},{28,92},{32,9... | collective-permute-start | bytes 442376 | tf_op jit(solution)/shard_map/ppermute | solution.py:578
  108.1 10.9 %collective-permute-start.5 = (bf16[2,144,256]{2,1,0:T(8,128)(2,1)S(1)}, bf16[2,144,256]{2,1,0:T(8,128)(2,1)S(1)}, u32[]{:S(2)}, u32[]{:S(2)}) collective-permute-start(bf16[2,144,256]{2,1,0:T(8,128)(2,1)S(1)} %pad_maximum_fusion.refs_0_), channel_id=1, source_target_pairs={{0,192},{4,196},{8,200},{12,204},{16,208},{20,212},{24,216},{28,22... | collective-permute-start | bytes 442376 | tf_op jit(solution)/shard_map/ppermute | solution.py:578
  113.3 9.1 %collective-permute-start.2 = (bf16[2,144,256]{2,1,0:T(8,128)(2,1)S(1)}, bf16[2,144,256]{2,1,0:T(8,128)(2,1)S(1)}, u32[]{:S(2)}, u32[]{:S(2)}) collective-permute-start(bf16[2,144,256]{2,1,0:T(8,128)(2,1)S(1)} %pad_maximum_fusion.refs_0_), channel_id=1, source_target_pairs={{0,32},{4,36},{8,40},{12,44},{16,48},{20,52},{24,56},{28,60},{32,6... | collective-permute-start | bytes 442376 | tf_op jit(solution)/shard_map/ppermute | solution.py:578
  113.4 9.0 %collective-permute-start.3 = (bf16[2,144,256]{2,1,0:T(8,128)(2,1)S(1)}, bf16[2,144,256]{2,1,0:T(8,128)(2,1)S(1)}, u32[]{:S(2)}, u32[]{:S(2)}) collective-permute-start(bf16[2,144,256]{2,1,0:T(8,128)(2,1)S(1)} %pad_maximum_fusion.refs_0_), channel_id=1, source_target_pairs={{0,224},{4,228},{8,232},{12,236},{16,240},{20,244},{24,248},{28,25... | collective-permute-start | bytes 442376 | tf_op jit(solution)/shard_map/ppermute | solution.py:578
  117.0 21.7 %collective-permute-start.31 = (bf16[256,512]{1,0:T(8,128)(2,1)S(1)}, bf16[256,512]{1,0:T(8,128)(2,1)S(1)}, u32[]{:S(2)}, u32[]{:S(2)}) collective-permute-start(bf16[256,512]{1,0:T(8,128)(2,1)S(1)} %copy-done.33), channel_id=1, source_target_pairs={{0,2},{1,3},{2,0},{3,1},{4,6},{5,7},{6,4},{7,5},{8,10},{9,11},{10,... | collective-permute-start | bytes 786440 | tf_op jit(solution)/shard_map/ppermute | solution.py:589
  117.7 23.2 %collective-permute-start.27 = (bf16[512,256]{1,0:T(8,128)(2,1)S(1)}, bf16[512,256]{1,0:T(8,128)(2,1)S(1)}, u32[]{:S(2)}, u32[]{:S(2)}) collective-permute-start(bf16[512,256]{1,0:T(8,128)(2,1)S(1)} %slice.44), channel_id=1, source_target_pairs={{0,1},{1,2},{2,3},{3,0},{4,5},{5,6},{6,7},{7,4},{8,9},{9,10},{10,1... | collective-permute-start | bytes 786440 | tf_op jit(solution)/shard_map/ppermute | solution.py:564
  119.0 21.8 %collective-permute-start.28 = (bf16[512,256]{1,0:T(8,128)(2,1)S(1)}, bf16[512,256]{1,0:T(8,128)(2,1)S(1)}, u32[]{:S(2)}, u32[]{:S(2)}) collective-permute-start(bf16[512,256]{1,0:T(8,128)(2,1)S(1)} %slice.45), channel_id=1, source_target_pairs={{0,3},{1,0},{2,1},{3,2},{4,7},{5,4},{6,5},{7,6},{8,11},{9,8},{10,9... | collective-permute-start | bytes 786440 | tf_op jit(solution)/shard_map/ppermute | solution.py:564
  122.4 5.6 %collective-permute-start.8 = (bf16[1,144,256]{2,1,0:T(8,128)(2,1)S(1)}, bf16[1,144,256]{2,1,0:T(8,128)(2,1)S(1)}, u32[]{:S(2)}, u32[]{:S(2)}) collective-permute-start(bf16[1,144,256]{2,1,0:T(8,128)(2,1)S(1)} %slice.40), channel_id=1, source_target_pairs={{0,64},{4,68},{8,72},{12,76},{16,80},{20,84},{24,88},{28,92},{32,9... | collective-permute-start | bytes 221192 | tf_op jit(solution)/shard_map/ppermute | solution.py:582
  122.4 5.7 %collective-permute-start.9 = (bf16[1,144,256]{2,1,0:T(8,128)(2,1)S(1)}, bf16[1,144,256]{2,1,0:T(8,128)(2,1)S(1)}, u32[]{:S(2)}, u32[]{:S(2)}) collective-permute-start(bf16[1,144,256]{2,1,0:T(8,128)(2,1)S(1)} %slice.41), channel_id=1, source_target_pairs={{0,192},{4,196},{8,200},{12,204},{16,208},{20,212},{24,216},{28,22... | collective-permute-start | bytes 221192 | tf_op jit(solution)/shard_map/ppermute | solution.py:583
  128.1 7.1 %collective-permute-start.7 = (bf16[2,144,256]{2,1,0:T(8,128)(2,1)S(1)}, bf16[2,144,256]{2,1,0:T(8,128)(2,1)S(1)}, u32[]{:S(2)}, u32[]{:S(2)}) collective-permute-start(bf16[2,144,256]{2,1,0:T(8,128)(2,1)S(1)} %collective-permute-done.5.refs_4_), channel_id=1, source_target_pairs={{0,224},{4,228},{8,232},{12,236},{16,240},{20,244},{24,248},{28,25... | collective-permute-start | bytes 442376 | tf_op jit(solution)/shard_map/ppermute | solution.py:581
  133.6 24.5 %collective-permute-start.10 = (bf16[2,128,256]{2,1,0:T(8,128)(2,1)S(1)}, bf16[2,128,256]{2,1,0:T(8,128)(2,1)S(1)}, u32[]{:S(2)}, u32[]{:S(2)}) collective-permute-start(bf16[2,128,256]{2,1,0:T(8,128)(2,1)S(1)} %pad_maximum_fusion.1.refs_1_), channel_id=1, source_target_pairs={{0,16},{4,20},{8,24},{12,28},{16,0},{20,4},{24,8},{28,12},{32,48},... | collective-permute-start | bytes 393224 | tf_op jit(solution)/shard_map/ppermute | solution.py:575
  135.2 23.0 %collective-permute-start.11 = (bf16[2,128,256]{2,1,0:T(8,128)(2,1)S(1)}, bf16[2,128,256]{2,1,0:T(8,128)(2,1)S(1)}, u32[]{:S(2)}, u32[]{:S(2)}) collective-permute-start(bf16[2,128,256]{2,1,0:T(8,128)(2,1)S(1)} %pad_maximum_fusion.1.refs_1_), channel_id=1, source_target_pairs={{0,8},{4,12},{8,16},{12,20},{16,24},{20,28},{24,0},{28,4},{32,40},... | collective-permute-start | bytes 393224 | tf_op jit(solution)/shard_map/ppermute | solution.py:575
  138.7 36.4 %collective-permute-start.1 = (bf16[2,128,256]{2,1,0:T(8,128)(2,1)S(1)}, bf16[2,128,256]{2,1,0:T(8,128)(2,1)S(1)}, u32[]{:S(2)}, u32[]{:S(2)}) collective-permute-start(bf16[2,128,256]{2,1,0:T(8,128)(2,1)S(1)} %pad_maximum_fusion.1.refs_1_), channel_id=1, source_target_pairs={{0,24},{4,28},{8,0},{12,4},{16,8},{20,12},{24,16},{28,20},{32,56},... | collective-permute-start | bytes 393224 | tf_op jit(solution)/shard_map/ppermute | solution.py:575
  147.2 80.2 %all-to-all-start.1 = ((bf16[64,16,512]{2,1,0:T(8,128)(2,1)}), bf16[64,16,512]{2,1,0:T(8,128)(2,1)S(1)}, u32[]{:S(2)}, u32[]{:S(2)}) async-start(bf16[64,16,512]{2,1,0:T(8,128)(2,1)} %bitcast.20), calls=%async_computation.1 | async-start | bytes 2097152 | tf_op jit(solution)/shard_map/all_to_all | solution.py:553
  172.0 17.0 %collective-permute-start.12 = (bf16[2,512,128]{2,1,0:T(8,128)(2,1)}, bf16[2,512,128]{2,1,0:T(8,128)(2,1)S(1)}, u32[]{:S(2)}, u32[]{:S(2)}) collective-permute-start(bf16[2,512,128]{2,1,0:T(8,128)(2,1)} %get-tuple-element.26), channel_id=1, source_target_pairs={{0,24},{4,28},{8,0},{12,4},{16,8},{20,12},{24,16},{28,20},{32,56},... | collective-permute-start | bytes 786440 | tf_op jit(solution)/shard_map/ppermute | solution.py:616
  174.5 14.5 %collective-permute-start.14 = (bf16[2,512,128]{2,1,0:T(8,128)(2,1)}, bf16[2,512,128]{2,1,0:T(8,128)(2,1)S(1)}, u32[]{:S(2)}, u32[]{:S(2)}) collective-permute-start(bf16[2,512,128]{2,1,0:T(8,128)(2,1)} %get-tuple-element.28), channel_id=1, source_target_pairs={{0,16},{4,20},{8,24},{12,28},{16,0},{20,4},{24,8},{28,12},{32,48},... | collective-permute-start | bytes 786440 | tf_op jit(solution)/shard_map/ppermute | solution.py:616
  188.4 8.3 %collective-permute-start.13 = (bf16[2,512,128]{2,1,0:T(8,128)(2,1)}, bf16[2,512,128]{2,1,0:T(8,128)(2,1)S(1)}, u32[]{:S(2)}, u32[]{:S(2)}) collective-permute-start(bf16[2,512,128]{2,1,0:T(8,128)(2,1)} %get-tuple-element.27), channel_id=1, source_target_pairs={{0,8},{4,12},{8,16},{12,20},{16,24},{20,28},{24,0},{28,4},{32,40},... | collective-permute-start | bytes 786440 | tf_op jit(solution)/shard_map/ppermute | solution.py:616
  200.9 7.2 %collective-permute-start.15 = (bf16[256,128]{1,0:T(8,128)(2,1)}, bf16[256,128]{1,0:T(8,128)(2,1)S(1)}, u32[]{:S(2)}, u32[]{:S(2)}) collective-permute-start(bf16[256,128]{1,0:T(8,128)(2,1)} %get-tuple-element.30), channel_id=1, source_target_pairs={{0,252},{4,248},{8,244},{12,240},{16,236},{20,232},{24,228},{28,22... | collective-permute-start | bytes 196616 | tf_op jit(solution)/shard_map/ppermute | solution.py:632
  211.6 8.0 %collective-permute-start.16 = (bf16[64,2048]{1,0:T(8,128)(2,1)}, bf16[64,2048]{1,0:T(8,128)(2,1)S(1)}, u32[]{:S(2)}, u32[]{:S(2)}) collective-permute-start(bf16[64,2048]{1,0:T(8,128)(2,1)} %get-tuple-element.32), channel_id=1, source_target_pairs={{0,1},{1,2},{2,3},{3,0},{4,5},{5,6},{6,7},{7,4},{8,9},{9,10},{10,1... | collective-permute-start | bytes 786440 | tf_op jit(solution)/shard_map/ppermute | solution.py:635
  213.1 11.2 %collective-permute-start.17 = (bf16[64,2048]{1,0:T(8,128)(2,1)}, bf16[64,2048]{1,0:T(8,128)(2,1)S(1)}, u32[]{:S(2)}, u32[]{:S(2)}) collective-permute-start(bf16[64,2048]{1,0:T(8,128)(2,1)} %get-tuple-element.33), channel_id=1, source_target_pairs={{0,2},{1,3},{2,0},{3,1},{4,6},{5,7},{6,4},{7,5},{8,10},{9,11},{10,... | collective-permute-start | bytes 786440 | tf_op jit(solution)/shard_map/ppermute | solution.py:635
  213.5 13.0 %collective-permute-start.18 = (bf16[64,2048]{1,0:T(8,128)(2,1)}, bf16[64,2048]{1,0:T(8,128)(2,1)S(1)}, u32[]{:S(2)}, u32[]{:S(2)}) collective-permute-start(bf16[64,2048]{1,0:T(8,128)(2,1)} %get-tuple-element.34), channel_id=1, source_target_pairs={{0,3},{1,0},{2,1},{3,2},{4,7},{5,4},{6,5},{7,6},{8,11},{9,8},{10,9... | collective-permute-start | bytes 786440 | tf_op jit(solution)/shard_map/ppermute | solution.py:635
  (39 other events, 262.6 us)
